TPU v7x, 256 devices: a whole 4x4x8 slice. The times are simulated.
256 devices in a mesh: ep: 64 (over z, x, core), tp: 4 (over y).
Axes of the slice: x: 4, y: 4, z: 8, core: 2. Of those that a mesh axis runs over, the one named last changes fastest.
Arguments:
- tokens: bfloat16 [1024, 2048], P('ep'), may hold values from -6 to 6
- attn_gain: float32 [2048], replicated, may hold values from 0.1 to 1.9
- query_weight: bfloat16 [2048, 2048], P('ep', 'tp'), may hold values from -0.125 to 0.125
- key_weight: bfloat16 [2048, 512], P('ep', 'tp'), may hold values from -0.125 to 0.125
- value_weight: bfloat16 [2048, 512], P('ep', 'tp'), may hold values from -0.125 to 0.125
- break_bias: float32 [16], P('tp'), may hold values from -14 to -8
- cache_keys: bfloat16 [1024, 4, 1024, 128], P('ep', 'tp'), may hold values from -18 to 18
- cache_values: bfloat16 [1024, 4, 1024, 128], P('ep', 'tp'), may hold values from -6 to 6
- lengths: int32 [1024], P('ep'), may hold values from 1 to 1024, 524288 in all
- out_weight: bfloat16 [2048, 2048], P('tp', 'ep'), may hold values from -0.25 to 0.25
- ffn_gain: float32 [2048], replicated, may hold values from 0.1 to 1.9
- branch_gate: bfloat16 [2048], replicated, may hold values from -0.125 to 0.125
- dense_gate: bfloat16 [2048, 8192], P('tp', 'ep'), may hold values from -0.125 to 0.125
- dense_up: bfloat16 [2048, 8192], P('tp', 'ep'), may hold values from -0.125 to 0.125
- dense_down: bfloat16 [8192, 2048], P('ep', 'tp'), may hold values from -0.0625 to 0.0625
- route_ids: int32 [1024, 4], P('ep'), may hold values from 0 to 63, all different within a row; in each aligned block of 16 rows (0 to 15, 16 to 31, ...) at most 2 rows name the same one
- route_weights: float32 [1024, 4], P('ep'), may hold values from 0.1 to 1
- expert_gate: bfloat16 [64, 2048, 1024], P('ep', None, 'tp'), may hold values from -0.4375 to 0.4375
- expert_up: bfloat16 [64, 2048, 1024], P('ep', None, 'tp'), may hold values from -0.4375 to 0.4375
- expert_down: bfloat16 [64, 1024, 2048], P('ep', 'tp'), may hold values from -0.01953125 to 0.01953125
Outputs:
- layer_out: bfloat16 [1024, 2048], P('ep', 'tp')
- new_keys: bfloat16 [1024, 512], P('ep', 'tp')
- new_values: bfloat16 [1024, 512], P('ep', 'tp')
Inputs may be any that keep to these rules, and one draw needn't show every extreme that they name: `route_ids`: each row names 4 different experts. Among the rows of one device no expert is named more than 2 times, a bound that some block reaches. Sequence b's cache holds keys at positions below lengths[b]; some sequence fills its whole cache.
All inputs are finite; a program needn't handle non-finite values. No bound on the sum of `lengths` on one device may be relied on, other than what follows from the above.
Results may differ from a plain program's by a relative error of at most 0.011.
Values may be sent and summed in bfloat16 or wider, within the bound.
No kernel may reach another device: no remote copies, remote signals or barrier semaphores. Data moves between devices by JAX's collectives and lax.ppermute only.
A program may use at most 64 MiB of HBM per device.

v0:
```python
import jax
import jax.numpy as jnp
from jax import lax
from jax.sharding import Mesh
from jax.sharding import PartitionSpec as P

EP = ("ep_0", "ep_1", "ep_2")


norm_eps = 1e-05
clamp_limit = 7.0
swish_alpha = 1.702


def in_one_piece(arrays, axis, dim, along):
    widths = [a.shape[along] for a in arrays]
    both = jnp.concatenate(arrays, axis=along)
    whole = lax.all_gather(both, axis, axis=dim, tiled=True)
    return tuple(jnp.split(whole, [sum(widths[:k]) for k in range(1, len(widths))], axis=along))


def laid_out(blocks, dim):
    dims = list(blocks.shape[1:])
    dims[dim] *= blocks.shape[0]
    return jnp.moveaxis(blocks, 0, dim).reshape(dims)


def from_everyone(shard, axis):
    count = lax.axis_size(axis)
    return lax.all_to_all(
        jnp.broadcast_to(shard[None], (count, *shard.shape)), axis, 0, 0, tiled=True
    )


def gather_directly(shard, axis, dim):
    return laid_out(from_everyone(shard, axis), dim)


def over_copies(shard, axis):
    everything = from_everyone(shard, axis)
    return jnp.sum(everything, axis=0)


def split_up(shard, dim, count):
    before, after = (shard.shape[:dim], shard.shape[dim + 1 :])
    return jnp.moveaxis(shard.reshape(*before, count, -1, *after), dim, 0)


def summed_on_arrival(shard, axis, dim):
    blocks = split_up(shard, dim, lax.axis_size(axis))
    arrived = lax.all_to_all(blocks, axis, split_axis=0, concat_axis=0, tiled=True)
    return arrived.astype(jnp.float32).sum(axis=0)


def all_blocks(shard, axes, sequence):
    blocks = shard[None]
    for k in sequence:
        blocks = lax.all_gather(blocks, axes[k], axis=0, tiled=True)
    current = [lax.axis_size(axes[k]) for k in reversed(sequence)]
    blocks = blocks.reshape(*current, *shard.shape)
    turned = sorted(range(len(sequence)), key=lambda place: sequence[len(sequence) - 1 - place])
    return blocks.transpose(*turned, *range(len(sequence), blocks.ndim)).reshape(-1, *shard.shape)


def gathered_by_axis(shard, axes, sequence, dim):
    return laid_out(all_blocks(shard, axes, sequence), dim)


def of_everyone(shard, axis):
    return from_everyone(shard, axis).astype(jnp.float32).sum(axis=0)


def rms_scale(values, gain):
    return values * lax.rsqrt(jnp.mean(values * values, axis=-1, keepdims=True) + norm_eps) * gain


def clamped_unit(gate_pre, up_pre):
    gate_c = jnp.minimum(gate_pre, clamp_limit)
    up_c = jnp.clip(up_pre, -clamp_limit, clamp_limit)
    return (up_c + 1.0) * gate_c * jax.nn.sigmoid(swish_alpha * gate_c)


def slot_ranks(flat_ids, expert_count):
    one_hot = (flat_ids[..., None] == jnp.arange(expert_count, dtype=jnp.int32)).astype(jnp.int32)
    earlier = jnp.cumsum(one_hot, axis=-2) - one_hot
    return jnp.sum(earlier * one_hot, axis=-1)


def body(
    tokens,
    attn_gain,
    query_weight,
    key_weight,
    value_weight,
    break_bias,
    cache_keys,
    cache_values,
    lengths,
    out_weight,
    ffn_gain,
    branch_gate,
    dense_gate,
    dense_up,
    dense_down,
    route_ids,
    route_weights,
    expert_gate,
    expert_up,
    expert_down,
):
    ep_count = lax.axis_size(EP)
    tp_count = lax.axis_size("tp")
    seq_count, model_width = tokens.shape
    top_count = route_ids.shape[1]
    local_experts = expert_gate.shape[0]
    expert_count = ep_count * local_experts
    capacity = 2 * seq_count * top_count // expert_count
    slice_width = model_width // tp_count
    tp_start = lax.axis_index("tp") * slice_width
    q_columns = query_weight.shape[1]
    normed = rms_scale(tokens.astype(jnp.float32), attn_gain).astype(jnp.bfloat16)
    pieces = in_one_piece((query_weight, key_weight, value_weight), EP, 0, 1)
    query_sum = jnp.dot(normed, pieces[0], preferred_element_type=jnp.float32)
    key_sum = jnp.dot(normed, pieces[1], preferred_element_type=jnp.float32)
    value_sum = jnp.dot(normed, pieces[2], preferred_element_type=jnp.float32)
    queries = query_sum.astype(jnp.bfloat16)
    new_keys = key_sum.astype(jnp.bfloat16)
    new_values = value_sum.astype(jnp.bfloat16)
    kv_local = cache_keys.shape[1]
    cache_span = cache_keys.shape[2]
    head_dim = cache_keys.shape[3]
    group_size = q_columns // (kv_local * head_dim)
    query_heads = queries.reshape(seq_count, kv_local, group_size, head_dim)
    scores = jnp.einsum(
        "sgrd,sgld->sgrl", query_heads, cache_keys, preferred_element_type=jnp.float32
    )
    scores = (
        scores * head_dim ** (-0.5) + break_bias.reshape(kv_local, group_size)[None, :, :, None]
    )
    positions = lax.broadcasted_iota(jnp.int32, (1, 1, 1, cache_span), 3)
    inside = positions < lengths[:, None, None, None]
    log_keep = jnp.where(inside, jax.nn.log_sigmoid(-scores), 0.0)
    between = lax.cumsum(log_keep, axis=3, reverse=True) - log_keep
    weights = jnp.where(inside, jnp.exp(jax.nn.log_sigmoid(scores) + between), 0.0).astype(
        jnp.bfloat16
    )
    attended = jnp.einsum(
        "sgrl,sgld->sgrd", weights, cache_values, preferred_element_type=jnp.float32
    )
    attended = attended.astype(jnp.bfloat16).reshape(seq_count, q_columns)
    partial_out = jnp.dot(
        attended, gather_directly(out_weight, EP, 1), preferred_element_type=jnp.float32
    )
    mixed_rows = over_copies(partial_out, "tp").astype(jnp.bfloat16)
    resid = tokens.astype(jnp.float32) + mixed_rows.astype(jnp.float32)
    normed2 = rms_scale(resid, ffn_gain).astype(jnp.bfloat16)
    flat_ids = route_ids.reshape(seq_count * top_count)
    slots = (flat_ids * capacity + slot_ranks(flat_ids, expert_count)).reshape(seq_count, top_count)
    dispatch = (
        slots[None, :, :] == jnp.arange(expert_count * capacity, dtype=jnp.int32)[:, None, None]
    )
    dispatch = jnp.any(dispatch, axis=2).astype(jnp.bfloat16)
    outgoing = jnp.dot(dispatch, normed2, preferred_element_type=jnp.float32).astype(jnp.bfloat16)
    outgoing = outgoing.reshape(ep_count, local_experts, capacity, model_width)
    buffer = lax.all_to_all(outgoing, EP, split_axis=0, concat_axis=0, tiled=True)
    gate_pre = jnp.einsum("sxcd,xdw->sxcw", buffer, expert_gate, preferred_element_type=jnp.float32)
    up_pre = jnp.einsum("sxcd,xdw->sxcw", buffer, expert_up, preferred_element_type=jnp.float32)
    activation = clamped_unit(gate_pre, up_pre).astype(jnp.bfloat16)
    partial_rows = jnp.einsum(
        "sxcw,xwd->sxcd", activation, expert_down, preferred_element_type=jnp.float32
    )
    results = summed_on_arrival(partial_rows.astype(jnp.bfloat16), "tp", 3).astype(jnp.bfloat16)
    returned = lax.all_to_all(results, EP, split_axis=0, concat_axis=0, tiled=True)
    returned = returned.reshape(expert_count * capacity, slice_width)
    picked = returned[slots].astype(jnp.float32)
    moe_own = jnp.sum(picked * route_weights[:, :, None], axis=1)
    own_slice = lax.dynamic_slice_in_dim(normed2, tp_start, slice_width, 1)
    piece_rows = gathered_by_axis(own_slice, EP, (1, 0, 2), 0)
    dense_pre = jnp.concatenate(
        [
            jnp.dot(piece_rows, dense_gate, preferred_element_type=jnp.float32),
            jnp.dot(piece_rows, dense_up, preferred_element_type=jnp.float32),
        ],
        axis=1,
    )
    pre_sum = of_everyone(dense_pre.astype(jnp.bfloat16), "tp").astype(jnp.float32)
    dense_cols = dense_gate.shape[1]
    hidden_units = (jax.nn.silu(pre_sum[:, :dense_cols]) * pre_sum[:, dense_cols:]).astype(
        jnp.bfloat16
    )
    dense_block = jnp.dot(hidden_units, dense_down, preferred_element_type=jnp.float32)
    combined = summed_on_arrival(dense_block.astype(jnp.bfloat16), EP, 0)
    resid_own = lax.dynamic_slice_in_dim(resid, tp_start, slice_width, 1)
    branch_own = jax.nn.sigmoid(jnp.dot(normed2, branch_gate, preferred_element_type=jnp.float32))
    layer_sum = resid_own + moe_own + branch_own[:, None] * combined
    return (layer_sum.astype(jnp.bfloat16), new_keys, new_values)


def solution(mesh):
    split = Mesh(mesh.devices.reshape(8, 4, 2, mesh.shape["tp"]), ("ep_0", "ep_1", "ep_2", "tp"))
    return jax.shard_map(
        body,
        mesh=split,
        in_specs=(
            P(EP, None),
            P(),
            P(EP, "tp"),
            P(EP, "tp"),
            P(EP, "tp"),
            P("tp"),
            P(EP, "tp", None, None),
            P(EP, "tp", None, None),
            P(EP),
            P("tp", EP),
            P(),
            P(),
            P("tp", EP),
            P("tp", EP),
            P(EP, "tp"),
            P(EP, None),
            P(EP, None),
            P(EP, None, "tp"),
            P(EP, None, "tp"),
            P(EP, "tp", None),
        ),
        out_specs=(P(EP, "tp"), P(EP, "tp"), P(EP, "tp")),
        check_vma=False,
    )
```

profile of v0, /device:TPU:1, one launch (start us, length us, event | category | flops | bytes accessed | tf_op | source)
XLA Modules:
  0.0 362.7 jit_solution(4714251275176345074)
XLA Ops:
  7.2 1.5 pad_maximum_fusion.1
  8.8 2.4 broadcast_in_dim.25
  11.2 13.1 %all-to-all-start = ((bf16[64,512,32]{1,2,0:T(8,128)(2,1)}), bf16[64,512,32]{1,2,0:T(8,128)(2,1)S(1)}, u32[]{:S(2)}, u32[]{:S(2)}) async-start(bf16[64,512,32]{1,2,0:T(8,128)(2,1)} %broadcast_in_dim.25), calls=%async_computation | async-start | bytes 4194304 | tf_op jit(solution)/shard_map/all_to_all | solution.py:30
  24.9 70.4 %all-gather.4.cloned.1.call-done = bf16[2048,768]{1,0:T(8,128)(2,1)} async-done(((bf16[32,768]{1,0:T(8,128)(2,1)}), bf16[2048,768]{1,0:T(8,128)(2,1)}) %all-gather.4.cloned.1.call-update) | async-done | bytes 3145744 | tf_op jit(solution)/shard_map/all_gather | solution.py:18
  95.3 2.0 fusion.16
  97.4 4.1 %fusion.46 = (f32[16,4,1024]{2,1,0:T(4,128)S(1)}, f32[16,4,1024]{2,1,0:T(4,128)}) fusion(pred[16,1024]{1,0:T(8,128)(4,1)S(1)} %iota_compare_fusion, f32[4]{0:T(128)S(1)} %copy-done.11, bf16[16,4,128]{2,1,0:T(4,128)(2,1)S(1)} %reshape.195, bf16[16,1,1024,128]{3,2,1,0:T(8,128)(2,1)} %param.26), kind=kOutput, calls=%fused_computation.52 | convolution fusion | flops 17432576 | bytes 4751376 | tf_op jit(solution)/shard_map/sgrd,sgld->sgrl/dot_general | solution.py:134
  101.5 0.8 reshape.197
  102.3 79.8 %reduce-window.6 = f32[16,1,4,8,128]{4,3,2,1,0:T(8,128)S(1)} reduce-window(f32[16,1,4,8,128]{4,3,2,1,0:T(8,128)} %bitcast.95, f32[]{:T(128)} %constant.16.clone.1), window={size=1x1x1x1x128 pad=0_0x0_0x0_0x0_0x0_127}, to_apply=%region_1.2 | reduce-window | flops 8323072 | bytes 524292 | tf_op jit(solution)/shard_map/reduce-window
  182.1 0.8 reshape.198
  182.9 0.3 copy.61
  183.4 0.8 reshape.201
  184.2 3.5 fusion.19
  187.7 0.6 fusion.65
  188.4 0.8 broadcast_in_dim.26
  189.2 4.4 %all-to-all-start.1 = ((f32[4,16,2048]{2,1,0:T(8,128)}), f32[4,16,2048]{2,1,0:T(8,128)S(1)}, u32[]{:S(2)}, u32[]{:S(2)}) async-start(f32[4,16,2048]{2,1,0:T(8,128)} %broadcast_in_dim.26), calls=%async_computation.1 | async-start | bytes 1048576 | tf_op jit(solution)/shard_map/all_to_all | solution.py:30
  193.6 0.2 select_reduce_fusion
  194.0 8.6 %all-to-all-done.1 = f32[4,16,2048]{2,1,0:T(8,128)S(1)} async-done(((f32[4,16,2048]{2,1,0:T(8,128)}), f32[4,16,2048]{2,1,0:T(8,128)S(1)}, u32[]{:S(2)}, u32[]{:S(2)}) %all-to-all-start.1) | async-done | bytes 524320 | tf_op jit(solution)/shard_map/all_to_all | solution.py:30
  202.9 0.3 convolution_convert_fusion.1
  203.2 1.2 reshape.205
  204.4 7.8 %all-to-all-start.2 = ((bf16[64,1,2,2048]{3,2,1,0:T(2,128)(2,1)}), bf16[64,1,2,2048]{3,2,1,0:T(2,128)(2,1)S(1)}, u32[]{:S(2)}, u32[]{:S(2)}) async-start(bf16[64,1,2,2048]{3,2,1,0:T(2,128)(2,1)} %bitcast.7), calls=%async_computation.2 | async-start | bytes 1048576 | tf_op jit(solution)/shard_map/all_to_all | solution.py:165
  212.3 10.4 %all-gather = bf16[64,512]{1,0:T(8,128)(2,1)S(1)} all-gather(bf16[16,512]{1,0:T(8,128)(2,1)S(1)} %constant_dynamic-slice_fusion), channel_id=2, replica_groups=mesh['ep_0'=8,'ep_1'=4,'ep_2'=2,'tp'=4] {'ep_1'}, dimensions={0}, use_global_device_ids=true | all-gather | bytes 81920 | tf_op jit(solution)/shard_map/all_gather | solution.py:58
  222.7 22.8 %all_gather.14 = bf16[32,16,512]{2,1,0:T(8,128)(2,1)} all-gather(bf16[4,16,512]{2,1,0:T(8,128)(2,1)S(1)} %bitcast.98), channel_id=1, replica_groups=mesh['ep_0'=8,'ep_1'=4,'ep_2'=2,'tp'=4] {'ep_0'}, dimensions={0}, use_global_device_ids=true | all-gather | bytes 589824 | tf_op jit(solution)/shard_map/all_gather | solution.py:58
  245.5 1.6 convolution_minimum_fusion
  247.1 0.8 convolution_convert_fusion
  247.9 0.9 copy.91
  248.8 3.5 all-to-all-start.3
  252.2 13.7 %all-gather.6.cloned.1.call-done = bf16[64,16,512]{2,1,0:T(8,128)(2,1)} async-done(((bf16[32,16,512]{2,1,0:T(8,128)(2,1)}), bf16[64,16,512]{2,1,0:T(8,128)(2,1)}) %all-gather.6.cloned.1.call-update) | async-done | bytes 1048592 | tf_op jit(solution)/shard_map/all_gather | solution.py:58
  266.0 1.3 copy.72
  267.3 0.5 convolution_convert_fusion.3
  267.8 0.5 convolution_convert_fusion.4
  268.3 0.2 copy.73
  268.6 1.5 broadcast_in_dim.29
  270.1 3.7 %all-to-all-start.5 = ((bf16[4,1024,256]{2,1,0:T(8,128)(2,1)}), bf16[4,1024,256]{2,1,0:T(8,128)(2,1)S(1)}, u32[]{:S(2)}, u32[]{:S(2)}) async-start(bf16[4,1024,256]{2,1,0:T(8,128)(2,1)} %broadcast_in_dim.29), calls=%async_computation.5 | async-start | bytes 4194304 | tf_op jit(solution)/shard_map/all_to_all | solution.py:30
  273.8 1.1 reduce_sum.84
  274.9 0.8 copy.70
  275.7 24.0 %all-to-all-done.5 = bf16[4,1024,256]{2,1,0:T(8,128)(2,1)S(1)} async-done(((bf16[4,1024,256]{2,1,0:T(8,128)(2,1)}), bf16[4,1024,256]{2,1,0:T(8,128)(2,1)S(1)}, u32[]{:S(2)}, u32[]{:S(2)}) %all-to-all-start.5) | async-done | bytes 2097184 | tf_op jit(solution)/shard_map/all_to_all | solution.py:30
  299.7 11.3 %all-to-all-start.4 = ((bf16[64,1,2,512]{3,2,1,0:T(2,128)(2,1)}), bf16[64,1,2,512]{3,2,1,0:T(2,128)(2,1)S(1)}, u32[]{:S(2)}, u32[]{:S(2)}) async-start(bf16[64,1,2,512]{3,2,1,0:T(2,128)(2,1)} %copy.70), calls=%async_computation.4 | async-start | bytes 262144 | tf_op jit(solution)/shard_map/all_to_all | solution.py:173
  311.1 0.3 convert_reduce_fusion
  311.4 2.3 convolution_convert_fusion.2
  313.8 8.4 %all-to-all-done.4 = bf16[64,1,2,512]{3,2,1,0:T(2,128)(2,1)S(1)} async-done(((bf16[64,1,2,512]{3,2,1,0:T(2,128)(2,1)}), bf16[64,1,2,512]{3,2,1,0:T(2,128)(2,1)S(1)}, u32[]{:S(2)}, u32[]{:S(2)}) %all-to-all-start.4) | async-done | bytes 131104 | tf_op jit(solution)/shard_map/all_to_all | solution.py:173
  322.2 4.5 %all-to-all-start.6 = ((bf16[64,16,512]{2,1,0:T(8,128)(2,1)}), bf16[64,16,512]{2,1,0:T(8,128)(2,1)S(1)}, u32[]{:S(2)}, u32[]{:S(2)}) async-start(bf16[64,16,512]{2,1,0:T(8,128)(2,1)} %bitcast.25), calls=%async_computation.6 | async-start | bytes 2097152 | tf_op jit(solution)/shard_map/all_to_all | solution.py:51
  326.9 1.9 convolution_convert_fusion.5
  328.8 1.9 convolution_convert_fusion.6
  330.9 0.7 gather_fusion
  331.6 0.1 multiply_reduce_fusion
  331.8 23.2 %all-to-all-done.6 = bf16[64,16,512]{2,1,0:T(8,128)(2,1)S(1)} async-done(((bf16[64,16,512]{2,1,0:T(8,128)(2,1)}), bf16[64,16,512]{2,1,0:T(8,128)(2,1)S(1)}, u32[]{:S(2)}, u32[]{:S(2)}) %all-to-all-start.6) | async-done | bytes 1048608 | tf_op jit(solution)/shard_map/all_to_all | solution.py:51
  355.0 0.2 convert_reduce_fusion.1
  355.1 0.7 add_convert_fusion
  (70 shorter events, 2.1 us)
Async XLA Ops:
  7.2 239.9 %copy-start = (bf16[1,256,2048]{2,1,0:T(8,128)(2,1)S(1)}, bf16[1,256,2048]{2,1,0:T(8,128)(2,1)}, u32[]{:S(2)}) copy-start(bf16[1,256,2048]{2,1,0:T(8,128)(2,1)} %param.39) | copy-start | bytes 3145732
  7.2 88.2 %all-gather.4.cloned.1.call-start = ((), (), s32[]{:S(2)}) async-start(), calls=%async_computation.7 | async-start | bytes 3194880 | tf_op jit(solution)/shard_map/all_gather | solution.py:18
  8.7 15.6 %copy-start.9 = (s32[16,4]{0,1:T(4,128)S(1)}, s32[16,4]{0,1:T(4,128)}, u32[]{:S(2)}) copy-start(s32[16,4]{0,1:T(4,128)} %param.35) | copy-start | bytes 772
  8.7 15.9 %copy-start.3 = (bf16[16,2048]{1,0:T(8,128)(2,1)S(1)}, bf16[16,2048]{1,0:T(8,128)(2,1)}, u32[]{:S(2)}) copy-start(bf16[16,2048]{1,0:T(8,128)(2,1)} %param.20) | copy-start | bytes 196612
  8.8 16.0 %copy-start.12 = (s32[16]{0:T(128)S(1)}, s32[16]{0:T(128)}, u32[]{:S(2)}) copy-start(s32[16]{0:T(128)} %param.28) | copy-start | bytes 196
  8.8 86.6 %copy-start.13 = (f32[2048]{0:T(1024)S(1)}, f32[2048]{0:T(1024)}, u32[]{:S(2)}) copy-start(f32[2048]{0:T(1024)} %param.21) | copy-start | bytes 24580
  11.2 86.2 %copy-start.11 = (f32[4]{0:T(128)S(1)}, f32[4]{0:T(128)}, u32[]{:S(2)}) copy-start(f32[4]{0:T(128)} %param.25) | copy-start | bytes 52
  11.2 176.5 %all-to-all-start = ((bf16[64,512,32]{1,2,0:T(8,128)(2,1)}), bf16[64,512,32]{1,2,0:T(8,128)(2,1)S(1)}, u32[]{:S(2)}, u32[]{:S(2)}) async-start(bf16[64,512,32]{1,2,0:T(8,128)(2,1)} %broadcast_in_dim.25), calls=%async_computation | async-start | bytes 4194304 | tf_op jit(solution)/shard_map/all_to_all | solution.py:30
  24.8 70.5 %copy-start.15 = (f32[16]{0:T(128)}, f32[16]{0:T(128)S(1)}, u32[]{:S(2)}) copy-start(f32[16]{0:T(128)S(1)} %add_rsqrt_fusion.1) | copy-start | bytes 196
  24.9 76.6 %copy-start.6 = (pred[16,1024]{1,0:T(8,128)(4,1)}, pred[16,1024]{1,0:T(8,128)(4,1)S(1)}, u32[]{:S(2)}) copy-start(pred[16,1024]{1,0:T(8,128)(4,1)S(1)} %iota_compare_fusion) | copy-start | bytes 49156
  187.7 15.1 %copy-start.7 = (f32[2048]{0:T(1024)S(1)}, f32[2048]{0:T(1024)}, u32[]{:S(2)}) copy-start(f32[2048]{0:T(1024)} %param.30) | copy-start | bytes 24580
  189.2 13.4 %all-to-all-start.1 = ((f32[4,16,2048]{2,1,0:T(8,128)}), f32[4,16,2048]{2,1,0:T(8,128)S(1)}, u32[]{:S(2)}, u32[]{:S(2)}) async-start(f32[4,16,2048]{2,1,0:T(8,128)} %broadcast_in_dim.26), calls=%async_computation.1 | async-start | bytes 1048576 | tf_op jit(solution)/shard_map/all_to_all | solution.py:30
  202.6 44.5 %copy-start.2 = (bf16[1,2048,256]{2,1,0:T(8,128)(2,1)S(1)}, bf16[1,2048,256]{2,1,0:T(8,128)(2,1)}, u32[]{:S(2)}) copy-start(bf16[1,2048,256]{2,1,0:T(8,128)(2,1)} %param.38) | copy-start | bytes 3145732
  204.4 41.1 %all-to-all-start.2 = ((bf16[64,1,2,2048]{3,2,1,0:T(2,128)(2,1)}), bf16[64,1,2,2048]{3,2,1,0:T(2,128)(2,1)S(1)}, u32[]{:S(2)}, u32[]{:S(2)}) async-start(bf16[64,1,2,2048]{3,2,1,0:T(2,128)(2,1)} %bitcast.7), calls=%async_computation.2 | async-start | bytes 1048576 | tf_op jit(solution)/shard_map/all_to_all | solution.py:165
  212.2 53.8 %all-gather.6.cloned.1.call-start = ((), (), s32[]{:S(2)}) async-start(), calls=%async_computation.8 | async-start | bytes 1572864 | tf_op jit(solution)/shard_map/all_gather | solution.py:58
  247.9 19.4 %copy-start.4 = (bf16[512,128]{1,0:T(8,128)(2,1)S(1)}, bf16[512,128]{1,0:T(8,128)(2,1)}, u32[]{:S(2)}) copy-start(bf16[512,128]{1,0:T(8,128)(2,1)} %param.33) | copy-start | bytes 393220
  247.9 19.9 %copy-start.5 = (bf16[512,128]{1,0:T(8,128)(2,1)S(1)}, bf16[512,128]{1,0:T(8,128)(2,1)}, u32[]{:S(2)}) copy-start(bf16[512,128]{1,0:T(8,128)(2,1)} %param.32) | copy-start | bytes 393220
  248.8 19.8 %all-to-all-start.3 = ((bf16[4,64,1,2,512]{4,1,3,2,0:T(8,128)(2,1)}), bf16[4,64,1,2,512]{4,1,3,2,0:T(8,128)(2,1)S(1)}, u32[]{:S(2)}, u32[]{:S(2)}) async-start(bf16[4,64,1,2,512]{4,1,3,2,0:T(8,128)(2,1)} %bitcast.88), calls=%async_computation.3 | async-start | bytes 1048576 | tf_op jit(solution)/shard_map/all_to_all | solution.py:51
  268.5 1.5 copy-start.1
  270.1 29.7 %all-to-all-start.5 = ((bf16[4,1024,256]{2,1,0:T(8,128)(2,1)}), bf16[4,1024,256]{2,1,0:T(8,128)(2,1)S(1)}, u32[]{:S(2)}, u32[]{:S(2)}) async-start(bf16[4,1024,256]{2,1,0:T(8,128)(2,1)} %broadcast_in_dim.29), calls=%async_computation.5 | async-start | bytes 4194304 | tf_op jit(solution)/shard_map/all_to_all | solution.py:30
  299.7 22.4 %all-to-all-start.4 = ((bf16[64,1,2,512]{3,2,1,0:T(2,128)(2,1)}), bf16[64,1,2,512]{3,2,1,0:T(2,128)(2,1)S(1)}, u32[]{:S(2)}, u32[]{:S(2)}) async-start(bf16[64,1,2,512]{3,2,1,0:T(2,128)(2,1)} %copy.70), calls=%async_computation.4 | async-start | bytes 262144 | tf_op jit(solution)/shard_map/all_to_all | solution.py:173
  311.4 15.3 %copy-start.8 = (bf16[2048]{0:T(1024)(128)(2,1)S(1)}, bf16[2048]{0:T(1024)(128)(2,1)}, u32[]{:S(2)}) copy-start(bf16[2048]{0:T(1024)(128)(2,1)} %param.31) | copy-start | bytes 12292
  311.4 15.3 %copy-start.10 = (f32[16,4]{0,1:T(4,128)S(1)}, f32[16,4]{0,1:T(4,128)}, u32[]{:S(2)}) copy-start(f32[16,4]{0,1:T(4,128)} %param.36) | copy-start | bytes 772
  311.4 15.5 %copy-start.14 = (f32[2048]{0:T(1024)S(1)}, f32[2048]{0:T(1024)}, u32[]{:S(2)}) copy-start(f32[2048]{0:T(1024)} %param.21) | copy-start | bytes 24580
  311.4 15.5 %copy-start.16 = (f32[16]{0:T(128)S(1)}, f32[16]{0:T(128)}, u32[]{:S(2)}) copy-start(f32[16]{0:T(128)} %copy-done.15) | copy-start | bytes 196
  322.2 32.8 %all-to-all-start.6 = ((bf16[64,16,512]{2,1,0:T(8,128)(2,1)}), bf16[64,16,512]{2,1,0:T(8,128)(2,1)S(1)}, u32[]{:S(2)}, u32[]{:S(2)}) async-start(bf16[64,16,512]{2,1,0:T(8,128)(2,1)} %bitcast.25), calls=%async_computation.6 | async-start | bytes 2097152 | tf_op jit(solution)/shard_map/all_to_all | solution.py:51
Sparse Core Ops, SparseCore 0:
  10.7 84.5 all-gather.3
  245.6 20.3 all-gather.5
where the time goes:
time: 364 us; the launch traced here: 363 us
  waiting for transfers between devices  148 us (41%)
  other arithmetic  84.7 us (23%)
  starting transfers between devices  48.4 us (13%)
  blocking collectives  33.2 us (9%)
  matrix products  20.1 us (6%)
  between operations  14.5 us (4%)
  local copies, waits for them, and re-layouts  13.4 us (4%)
    another operation x2, other arithmetic  79.8 us
    all_gather x1, waiting for transfers between devices, in_one_piece(): whole = lax.all_gather(both, axis, axis=dim, tiled=True)  70.4 us
    all_gather x2, blocking collectives, all_blocks(): blocks = lax.all_gather(blocks, axes[k], axis=0, tiled=True)  33.2 us
    all_to_all x3, waiting for transfers between devices, from_everyone(): lax.all_to_all(jnp.broadcast_to(shard[None], (count, *shard.shape)), axis...  32.6 us
    all_to_all x2, waiting for transfers between devices, summed_on_arrival(): lax.all_to_all(blocks, axis, split_axis=0, concat_axis=0, tiled=True)  23.2 us
    all_to_all x3, starting transfers between devices, from_everyone(): lax.all_to_all(jnp.broadcast_to(shard[None], (count, *shard.shape)), axis...  21.2 us
    all_gather x1, waiting for transfers between devices, all_blocks(): blocks = lax.all_gather(blocks, axes[k], axis=0, tiled=True)  13.7 us
    all_to_all x1, starting transfers between devices, body(): lax.all_to_all(results, EP, split_axis=0, concat_axis=0, tiled=True)  11.3 us
  transfers between devices with their start and end apart: 9, of which 6 were waited for; matrix products, arithmetic and copies ran while one was open for 31% of the time, Pallas kernels for 0%

commit v1 on v0

v1 whole, which is shorter than its diff:
```python
import functools
import jax
import jax.numpy as jnp
from jax import lax
from jax.experimental import pallas as pl
from jax.experimental.pallas import tpu as pltpu
from jax.sharding import Mesh
from jax.sharding import PartitionSpec as P

EP = ("z", "x", "c")
ZX = ("z", "x")

norm_eps = 1e-05
clamp_limit = 7.0
swish_alpha = 1.702
f32 = jnp.float32
bf16 = jnp.bfloat16


def rms_scale(values, gain):
    return values * lax.rsqrt(jnp.mean(values * values, axis=-1, keepdims=True) + norm_eps) * gain


def clamped_unit(gate_pre, up_pre):
    gate_c = jnp.minimum(gate_pre, clamp_limit)
    up_c = jnp.clip(up_pre, -clamp_limit, clamp_limit)
    return (up_c + 1.0) * gate_c * jax.nn.sigmoid(swish_alpha * gate_c)


def exchange(blocks, axes):
    return lax.all_to_all(blocks, axes, 0, 0, tiled=True)


def to_everyone(shard, axes):
    count = lax.axis_size(axes)
    return exchange(jnp.broadcast_to(shard[None], (count, *shard.shape)), axes)


def other_core(values):
    return lax.ppermute(values, "c", [(0, 1), (1, 0)])


def attention_kernel(per_step, group, span, lengths_ref, q_ref, bias_ref, k_ref, v_ref, o_ref):
    step = pl.program_id(0)
    head_dim = k_ref.shape[-1]
    scores = []
    for i in range(per_step):
        q = q_ref[i]
        scores.append(
            lax.dot_general(
                q, k_ref[i, 0], (((1,), (1,)), ((), ())), preferred_element_type=f32
            )
        )
    z = jnp.concatenate(scores, axis=0) * head_dim ** (-0.5) + bias_ref[:, 0:1]
    rows = z.shape[0]
    row_group = lax.broadcasted_iota(jnp.int32, (rows, 1), 0) // group
    length = jnp.zeros((rows, 1), jnp.int32)
    for i in range(per_step):
        length = jnp.where(row_group == i, lengths_ref[step * per_step + i], length)
    inside = lax.broadcasted_iota(jnp.int32, (rows, span), 1) < length
    tail = jnp.log1p(jnp.exp(-jnp.abs(z)))
    keep = jnp.where(inside, -jnp.maximum(z, 0.0) - tail, 0.0)
    take = jnp.minimum(z, 0.0) - tail
    lane = lax.broadcasted_iota(jnp.int32, (rows, 128), 1)
    chunks = span // 128
    after = jnp.zeros((rows, 1), f32)
    betweens = [None] * chunks
    for c in range(chunks - 1, -1, -1):
        own = keep[:, c * 128 : (c + 1) * 128]
        total = own
        shift = 1
        while shift < 128:
            moved = pltpu.roll(total, 128 - shift, 1)
            total = total + jnp.where(lane < 128 - shift, moved, 0.0)
            shift *= 2
        betweens[c] = total - own + after
        after = after + total[:, 0:1]
    between = jnp.concatenate(betweens, axis=1)
    weights = jnp.where(inside, jnp.exp(take + between), 0.0).astype(bf16)
    for i in range(per_step):
        o_ref[i] = jnp.dot(
            weights[i * group : (i + 1) * group], v_ref[i, 0], preferred_element_type=f32
        ).astype(bf16)


def attention(queries, bias, keys, values, lengths):
    seqs, _, span, head_dim = keys.shape
    heads = queries.shape[1] // head_dim
    group = 8
    per_step = 4
    q = queries.reshape(seqs, heads, head_dim)
    q = jnp.pad(q, ((0, 0), (0, group - heads), (0, 0)))
    b = jnp.pad(bias, (0, group - heads))
    b = jnp.broadcast_to(jnp.tile(b, per_step)[:, None], (per_step * group, 128))
    out = pl.pallas_call(
        functools.partial(attention_kernel, per_step, group, span),
        grid_spec=pltpu.PrefetchScalarGridSpec(
            num_scalar_prefetch=1,
            grid=(seqs // per_step,),
            in_specs=[
                pl.BlockSpec((per_step, group, head_dim), lambda i, n: (i, 0, 0)),
                pl.BlockSpec((per_step * group, 128), lambda i, n: (0, 0)),
                pl.BlockSpec((per_step, 1, span, head_dim), lambda i, n: (i, 0, 0, 0)),
                pl.BlockSpec((per_step, 1, span, head_dim), lambda i, n: (i, 0, 0, 0)),
            ],
            out_specs=pl.BlockSpec((per_step, group, head_dim), lambda i, n: (i, 0, 0)),
        ),
        out_shape=jax.ShapeDtypeStruct((seqs, group, head_dim), bf16),
        name="attention",
    )(lengths, q, b, keys, values)
    return out[:, :heads].reshape(seqs, heads * head_dim)


def body(
    tokens,
    attn_gain,
    query_weight,
    key_weight,
    value_weight,
    break_bias,
    cache_keys,
    cache_values,
    lengths,
    out_weight,
    ffn_gain,
    branch_gate,
    dense_gate,
    dense_up,
    dense_down,
    route_ids,
    route_weights,
    expert_gate,
    expert_up,
    expert_down,
):
    nz, nx, nt = lax.axis_size("z"), lax.axis_size("x"), lax.axis_size("tp")
    nzx = nz * nx
    seqs, width = tokens.shape
    experts = nzx * 2
    cap = 2
    slice_width = width // nt
    tp_start = lax.axis_index("tp") * slice_width
    q_cols, k_cols = query_weight.shape[1], key_weight.shape[1]

    w_own = jnp.concatenate([query_weight, key_weight, value_weight], axis=1)
    normed = rms_scale(tokens.astype(f32), attn_gain).astype(bf16)
    w_part = to_everyone(w_own, ("x", "c")).reshape(-1, w_own.shape[1])
    feats = jnp.moveaxis(normed.reshape(seqs, nz, width // nz), 1, 0)
    feats = exchange(feats, "z").reshape(nz * seqs, width // nz)

    ow = to_everyone(out_weight.T, "z")
    ow = to_everyone(ow.reshape(-1, ow.shape[2]), "x")
    ow = ow.reshape(nx, nz, -1, ow.shape[2])
    ow_other = other_core(ow)

    eid = jnp.arange(experts, dtype=jnp.int32)
    hit = route_ids[:, :, None] == eid
    chosen = jnp.any(hit, axis=1)
    weight = jnp.sum(jnp.where(hit, route_weights[:, :, None], 0.0), axis=1)
    count = chosen.astype(jnp.int32)
    rank = jnp.cumsum(count, axis=0) - count
    row = jnp.arange(seqs, dtype=f32)[:, None]
    meta = []
    for s in range(cap):
        here = chosen & (rank == s)
        meta.append(jnp.sum(jnp.where(here, row, 0.0), axis=0))
        meta.append(jnp.sum(jnp.where(here, weight, 0.0), axis=0))
    meta = jnp.stack(meta, axis=1)
    meta = jnp.pad(meta, ((0, 0), (0, 128 - 2 * cap)))[:, None, :]
    meta = exchange(meta, EP)[:, 0, : 2 * cap].reshape(nzx, 2, cap, 2)
    core = lax.axis_index("c")
    meta = jnp.where(core == 0, meta, meta[:, ::-1])
    meta = jnp.moveaxis(meta, 1, 0)
    slot_rows = meta[..., 0].astype(jnp.int32)
    block_at = jnp.arange(2 * nzx, dtype=jnp.int32).reshape(2, nzx, 1) * seqs
    slot_rows = (slot_rows + block_at).reshape(-1)
    slot_weights = meta[..., 1].reshape(-1)
    slot_count = 2 * nzx * cap
    all_rows = 2 * nzx * seqs
    onehot = (slot_rows[:, None] == jnp.arange(all_rows, dtype=jnp.int32)[None, :]).astype(bf16)

    partial = jnp.dot(feats, w_part, preferred_element_type=f32).astype(bf16)
    partial = exchange(partial.reshape(nz, seqs, -1), "z")
    qkv = jnp.sum(partial.astype(f32), axis=0).astype(bf16)
    queries = qkv[:, :q_cols]
    new_keys = qkv[:, q_cols : q_cols + k_cols]
    new_values = qkv[:, q_cols + k_cols :]

    attended = attention(queries, break_bias, cache_keys, cache_values, lengths)

    both = jnp.stack(
        [jnp.where(core == 0, ow, ow_other), jnp.where(core == 0, ow_other, ow)], axis=2
    )
    both = jnp.moveaxis(both, 0, 1).reshape(width, -1)
    partial_out = lax.dot_general(
        attended, both, (((1,), (1,)), ((), ())), preferred_element_type=f32
    )
    mixed = to_everyone(partial_out.astype(bf16), "tp").astype(f32).sum(axis=0).astype(bf16)
    resid = tokens.astype(f32) + mixed.astype(f32)
    normed2 = rms_scale(resid, ffn_gain).astype(bf16)

    own_slice = lax.dynamic_slice_in_dim(normed2, tp_start, slice_width, 1)
    mine = to_everyone(own_slice, ZX)
    other = other_core(mine)
    rows_x = jnp.concatenate([mine, other], axis=0).reshape(all_rows, slice_width)

    gate_slice = lax.dynamic_slice_in_dim(branch_gate, tp_start, slice_width, 0)
    gu = jnp.concatenate([dense_gate, dense_up], axis=1)
    dense_pre = jnp.dot(rows_x, gu, preferred_element_type=f32).astype(bf16)
    branch_pre = jnp.dot(rows_x, gate_slice, preferred_element_type=f32)
    slot_x = jnp.dot(onehot, rows_x, preferred_element_type=f32).astype(bf16)
    quarter = all_rows // nt
    half = slice_width // 2
    slot_fold = jnp.concatenate([slot_x[:, :half], slot_x[:, half:]], axis=0)
    m1 = jnp.concatenate(
        [
            dense_pre.reshape(nt, quarter, 2 * dense_gate.shape[1]),
            jnp.broadcast_to(slot_fold[None], (nt, *slot_fold.shape)),
        ],
        axis=2,
    )
    tailrow = jnp.pad(
        branch_pre.astype(bf16).reshape(nt, 1, quarter), ((0, 0), (0, 15), (0, half * 2 - quarter))
    )
    m1 = exchange(jnp.concatenate([m1, tailrow], axis=1), "tp")
    pre = m1[:, :quarter, :half].astype(f32).sum(axis=0)
    cols = dense_gate.shape[1]
    branch = jax.nn.sigmoid(m1[:, quarter, :quarter].astype(f32).sum(axis=0))
    hidden = (jax.nn.silu(pre[:, :cols]) * pre[:, cols:] * branch[:, None]).astype(bf16)
    sx = m1[:, :quarter, half:]
    sx = jnp.concatenate([sx[:, :slot_count], sx[:, slot_count:]], axis=2)
    sx = jnp.moveaxis(sx, 0, 1).reshape(slot_count, width)
    gate_pre = jnp.dot(sx, expert_gate[0], preferred_element_type=f32)
    up_pre = jnp.dot(sx, expert_up[0], preferred_element_type=f32)
    act = clamped_unit(gate_pre, up_pre).astype(bf16)
    out_rows = jnp.dot(act, expert_down[0], preferred_element_type=f32).astype(bf16)
    out_rows = jnp.moveaxis(out_rows.reshape(slot_count, nt, slice_width), 1, 0)
    hid_fold = jnp.concatenate([hidden[:slot_count], hidden[slot_count:]], axis=1)
    m2 = jnp.concatenate(
        [out_rows, jnp.broadcast_to(hid_fold[None], (nt, *hid_fold.shape))], axis=2
    )
    m2 = exchange(m2, "tp")
    moe_rows = m2[:, :, :slice_width].astype(f32).sum(axis=0)
    moe_rows = (moe_rows * slot_weights[:, None]).astype(bf16)
    hid = m2[:, :, slice_width:]
    hid = jnp.concatenate([hid[:, :, :cols], hid[:, :, cols:]], axis=1).reshape(all_rows, cols)
    lhs = jnp.concatenate([hid, onehot.T], axis=1)
    rhs = jnp.concatenate([dense_down, moe_rows], axis=0)
    block = jnp.dot(lhs, rhs, preferred_element_type=f32).astype(bf16)
    block = block.reshape(2, nzx, seqs, slice_width)
    from_other = other_core(block[1])
    block = (block[0].astype(f32) + from_other.astype(f32)).astype(bf16)
    combined = exchange(block, ZX).astype(f32).sum(axis=0)
    resid_own = lax.dynamic_slice_in_dim(resid, tp_start, slice_width, 1)
    return ((resid_own + combined).astype(bf16), new_keys, new_values)


def solution(mesh):
    shape = (mesh.shape["ep"] // 8, 4, 2, mesh.shape["tp"])
    split = Mesh(mesh.devices.reshape(shape), ("z", "x", "c", "tp"))
    return jax.shard_map(
        body,
        mesh=split,
        in_specs=(
            P(EP, None),
            P(),
            P(EP, "tp"),
            P(EP, "tp"),
            P(EP, "tp"),
            P("tp"),
            P(EP, "tp", None, None),
            P(EP, "tp", None, None),
            P(EP),
            P("tp", EP),
            P(),
            P(),
            P("tp", EP),
            P("tp", EP),
            P(EP, "tp"),
            P(EP, None),
            P(EP, None),
            P(EP, None, "tp"),
            P(EP, None, "tp"),
            P(EP, "tp", None),
        ),
        out_specs=(P(EP, "tp"), P(EP, "tp"), P(EP, "tp")),
        check_vma=False,
    )
```

time: 364 us -> 207 us (0.57)
  other arithmetic: 84.7 us -> 4.47 us
  waiting for transfers between devices: 148 us -> 80.6 us
  blocking collectives: 33.2 us -> 48.6 us
  between operations: 14.5 us -> 1.18 us
  matrix products: 20.1 us -> 7.67 us
  Pallas kernels: 0 us -> 8.08 us
  starting transfers between devices: 48.4 us -> 43.5 us
    all_gather x2 -> x0, waiting for transfers between devices: 84.2 us -> none  [the longest x1 70.4 us: in_one_piece(): whole = lax.all_gather(both, axis, axis=dim, tiled=True)]
    another operation x3 -> x2, other arithmetic: 79.9 us -> 0.18 us  [the longest x1 0.14 us: body(): jnp.stack([jnp.where(core == 0, ow, ow_other), jnp.where(core == 0, ow_ot...]
    all_to_all x0 -> x3, blocking collectives: none -> 48.6 us  [exchange(): return lax.all_to_all(blocks, axes, 0, 0, tiled=True)]
    all_gather x2 -> x0, blocking collectives: 33.2 us -> none  [all_blocks(): blocks = lax.all_gather(blocks, axes[k], axis=0, tiled=True)]
    all_to_all x7 -> x8, waiting for transfers between devices: 64.2 us -> 79.1 us  [exchange(): return lax.all_to_all(blocks, axes, 0, 0, tiled=True)]
    dot_general x13 -> x8, matrix products: 20.1 us -> 7.67 us  [the longest x1 2.03 us: body(): jnp.dot(act, expert_down[0], preferred_element_type=f32).astype(bf16)]
    all_to_all x7 -> x8, starting transfers between devices: 48.3 us -> 36.8 us  [exchange(): return lax.all_to_all(blocks, axes, 0, 0, tiled=True)]
    pallas_call x0 -> x1, Pallas kernels: none -> 8.08 us  [attention(): pl.pallas_call(functools.partial(attention_kernel, per_step, group, span)...]
  transfers between devices with their start and end apart: 9 -> 11, of which waited for: 6 -> 9; matrix products, arithmetic and copies ran while one was open for 31% -> 4% of each run, Pallas kernels for 0% -> 4%
where the time goes in v1:
time: 207 us; the launch traced here: 206 us
  waiting for transfers between devices  80.6 us (39%)
  blocking collectives  48.6 us (23%)
  starting transfers between devices  43.5 us (21%)
  local copies, waits for them, and re-layouts  11.7 us (6%)
  Pallas kernels  8.08 us (4%)
  matrix products  7.67 us (4%)
  other arithmetic  4.47 us (2%)
    all_to_all x8, waiting for transfers between devices, exchange(): return lax.all_to_all(blocks, axes, 0, 0, tiled=True)  79.1 us
    all_to_all x3, blocking collectives, exchange(): return lax.all_to_all(blocks, axes, 0, 0, tiled=True)  48.6 us
    all_to_all x8, starting transfers between devices, exchange(): return lax.all_to_all(blocks, axes, 0, 0, tiled=True)  36.8 us
    pallas_call x1, Pallas kernels, attention(): pl.pallas_call(functools.partial(attention_kernel, per_step, group, span)...  8.08 us
    ppermute x3, starting transfers between devices, other_core(): return lax.ppermute(values, 'c', [(0, 1), (1, 0)])  6.71 us
  transfers between devices with their start and end apart: 11, of which 9 were waited for; matrix products, arithmetic and copies ran while one was open for 4% of the time, Pallas kernels for 4%

profile of v1, /device:TPU:1, one launch (start us, length us, event | category | flops | bytes accessed | tf_op | source)
XLA Modules:
  0.0 205.8 jit_solution(1602338724934994806)
XLA Ops:
  0.7 0.9 broadcast_in_dim.58
  1.5 19.3 %all_to_all.55 = bf16[8,32,512]{2,1,0:T(8,128)(2,1)S(1)} all-to-all(bf16[8,32,512]{2,1,0:T(8,128)(2,1)S(1)} %broadcast_in_dim.58), channel_id=1, replica_groups=mesh['z'=8,'x'=4,'c'=2,'tp'=4] {'z'}, dimensions={0} | all-to-all | bytes 524288 | tf_op jit(solution)/shard_map/all_to_all | solution.py:31
  20.8 1.1 broadcast_in_dim.101
  21.9 4.1 %all-to-all-start.4 = ((bf16[4,256,512]{2,1,0:T(8,128)(2,1)}), bf16[4,256,512]{2,1,0:T(8,128)(2,1)S(1)}, u32[]{:S(2)}, u32[]{:S(2)}) async-start(bf16[4,256,512]{2,1,0:T(8,128)(2,1)} %broadcast_in_dim.101), calls=%async_computation.4 | async-start | bytes 2097152 | tf_op jit(solution)/shard_map/all_to_all | solution.py:31
  26.2 12.1 %all-to-all-done.4 = bf16[4,256,512]{2,1,0:T(8,128)(2,1)S(1)} async-done(((bf16[4,256,512]{2,1,0:T(8,128)(2,1)}), bf16[4,256,512]{2,1,0:T(8,128)(2,1)S(1)}, u32[]{:S(2)}, u32[]{:S(2)}) %all-to-all-start.4) | async-done | bytes 1048608 | tf_op jit(solution)/shard_map/all_to_all | solution.py:31
  38.3 3.8 %collective-permute-start = (bf16[4,8,32,512]{3,2,1,0:T(8,128)(2,1)S(1)}, bf16[4,8,32,512]{3,2,1,0:T(8,128)(2,1)S(1)}, u32[]{:S(2)}, u32[]{:S(2)}) collective-permute-start(bf16[4,8,32,512]{3,2,1,0:T(8,128)(2,1)S(1)} %bitcast.79), channel_id=1, source_target_pairs={{0,4},{4,0},{1,5},{5,1},{2,6},{6,2},{3,7},{7,3},{8,12},{12,8},{9,1... | collective-permute-start | bytes 3145736 | tf_op jit(solution)/shard_map/ppermute | solution.py:40
  42.2 0.6 copy.72
  42.9 3.3 %all-to-all-start = ((bf16[8,16,256]{2,1,0:T(8,128)(2,1)}), bf16[8,16,256]{2,1,0:T(8,128)(2,1)S(1)}, u32[]{:S(2)}, u32[]{:S(2)}) async-start(bf16[8,16,256]{2,1,0:T(8,128)(2,1)} %copy.72), calls=%async_computation | async-start | bytes 131072 | tf_op jit(solution)/shard_map/all_to_all | solution.py:31
  46.3 7.3 %all-to-all-done = bf16[8,16,256]{2,1,0:T(8,128)(2,1)S(1)} async-done(((bf16[8,16,256]{2,1,0:T(8,128)(2,1)}), bf16[8,16,256]{2,1,0:T(8,128)(2,1)S(1)}, u32[]{:S(2)}, u32[]{:S(2)}) %all-to-all-start) | async-done | bytes 65568 | tf_op jit(solution)/shard_map/all_to_all | solution.py:31
  53.5 11.7 %all_to_all.56 = bf16[8,32,768]{2,1,0:T(8,128)(2,1)S(1)} all-to-all(bf16[8,32,768]{2,1,0:T(8,128)(2,1)S(1)} %broadcast_in_dim.55), channel_id=1, replica_groups=mesh['z'=8,'x'=4,'c'=2,'tp'=4] {'x','c'}, dimensions={0} | all-to-all | bytes 786432 | tf_op jit(solution)/shard_map/all_to_all | solution.py:31
  65.2 0.9 convolution_convert_fusion.4
  66.1 3.4 %all-to-all-start.2 = ((bf16[8,16,768]{2,1,0:T(8,128)(2,1)}), bf16[8,16,768]{2,1,0:T(8,128)(2,1)S(1)}, u32[]{:S(2)}, u32[]{:S(2)}) async-start(bf16[8,16,768]{2,1,0:T(8,128)(2,1)} %bitcast.3), calls=%async_computation.2 | async-start | bytes 393216 | tf_op jit(solution)/shard_map/all_to_all | solution.py:31
  69.6 8.9 %all-to-all-done.2 = bf16[8,16,768]{2,1,0:T(8,128)(2,1)S(1)} async-done(((bf16[8,16,768]{2,1,0:T(8,128)(2,1)}), bf16[8,16,768]{2,1,0:T(8,128)(2,1)S(1)}, u32[]{:S(2)}, u32[]{:S(2)}) %all-to-all-start.2) | async-done | bytes 196640 | tf_op jit(solution)/shard_map/all_to_all | solution.py:31
  78.6 0.6 pad.16.q_ref
  79.2 0.7 broadcast_in_dim.57.bias_ref
  79.9 8.1 %attention.1 = bf16[16,8,128]{2,1,0:T(8,128)(2,1)} custom-call(s32[16]{0:T(128)} %lengths_ref.1, bf16[16,8,128]{2,1,0:T(8,128)(2,1)} %pad.16.q_ref, f32[32,128]{1,0:T(8,128)} %broadcast_in_dim.57.bias_ref, bf16[16,1,1024,128]{3,2,1,0:T(8,128)(2,1)} %k_ref.1, bf16[16,1,1024,128]{3,2,1,0:T(8,128)(2,1)} %v_ref.1), custom_call_target="tpu_custom_call" | custom-call | tf_op jit(solution)/shard_map/attention/pallas_call | solution.py:95
  88.3 0.2 copy.73
  88.5 0.5 slice-done
  89.0 0.6 convolution_convert_fusion.1
  89.7 0.7 broadcast_in_dim.102
  90.4 4.2 %all-to-all-start.5 = ((bf16[4,16,2048]{2,1,0:T(8,128)(2,1)}), bf16[4,16,2048]{2,1,0:T(8,128)(2,1)S(1)}, u32[]{:S(2)}, u32[]{:S(2)}) async-start(bf16[4,16,2048]{2,1,0:T(8,128)(2,1)} %broadcast_in_dim.102), calls=%async_computation.5 | async-start | bytes 524288 | tf_op jit(solution)/shard_map/all_to_all | solution.py:31
  94.6 0.8 dynamic-slice
  95.3 4.8 %all-to-all-done.5 = bf16[4,16,2048]{2,1,0:T(8,128)(2,1)S(1)} async-done(((bf16[4,16,2048]{2,1,0:T(8,128)(2,1)}), bf16[4,16,2048]{2,1,0:T(8,128)(2,1)S(1)}, u32[]{:S(2)}, u32[]{:S(2)}) %all-to-all-start.5) | async-done | bytes 262176 | tf_op jit(solution)/shard_map/all_to_all | solution.py:31
  100.4 0.9 broadcast_in_dim.103
  101.2 3.9 %all-to-all-start.6 = ((bf16[32,16,512]{2,1,0:T(8,128)(2,1)}), bf16[32,16,512]{2,1,0:T(8,128)(2,1)S(1)}, u32[]{:S(2)}, u32[]{:S(2)}) async-start(bf16[32,16,512]{2,1,0:T(8,128)(2,1)} %broadcast_in_dim.103), calls=%async_computation.6 | async-start | bytes 1048576 | tf_op jit(solution)/shard_map/all_to_all | solution.py:31
  105.5 0.7 copy.74
  106.2 12.2 %all-to-all-done.6 = bf16[32,16,512]{2,1,0:T(8,128)(2,1)S(1)} async-done(((bf16[32,16,512]{2,1,0:T(8,128)(2,1)}), bf16[32,16,512]{2,1,0:T(8,128)(2,1)S(1)}, u32[]{:S(2)}, u32[]{:S(2)}) %all-to-all-start.6) | async-done | bytes 524320 | tf_op jit(solution)/shard_map/all_to_all | solution.py:31
  118.4 10.3 %all-to-all-start.7 = ((f32[64,1,128]{2,1,0:T(1,128)}), f32[64,1,128]{2,1,0:T(1,128)S(1)}, u32[]{:S(2)}, u32[]{:S(2)}) async-start(f32[64,1,128]{2,1,0:T(1,128)} %copy.74), calls=%async_computation.7 | async-start | bytes 65536 | tf_op jit(solution)/shard_map/all_to_all | solution.py:31
  128.9 0.8 dynamic_slice.11
  129.7 0.5 collective-permute-start.1
  130.2 7.9 %all-to-all-done.7 = f32[64,1,128]{2,1,0:T(1,128)S(1)} async-done(((f32[64,1,128]{2,1,0:T(1,128)}), f32[64,1,128]{2,1,0:T(1,128)S(1)}, u32[]{:S(2)}, u32[]{:S(2)}) %all-to-all-start.7) | async-done | bytes 32800 | tf_op jit(solution)/shard_map/all_to_all | solution.py:31
  138.8 0.3 convolution_convert_fusion.5
  139.2 0.4 fusion.54
  139.6 1.4 convolution_convert_fusion.3
  141.1 17.6 %all_to_all.57 = bf16[4,272,512]{2,1,0:T(8,128)(2,1)S(1)} all-to-all(bf16[4,272,512]{2,1,0:T(8,128)(2,1)S(1)} %fusion.5), channel_id=1, replica_groups=mesh['z'=8,'x'=4,'c'=2,'tp'=4] {'tp'}, dimensions={0} | all-to-all | bytes 2228224 | tf_op jit(solution)/shard_map/all_to_all | solution.py:31
  159.2 1.6 convolution_minimum_fusion
  160.8 2.0 convolution_convert_fusion
  163.5 0.9 pad_maximum_fusion.1
  164.4 3.6 %all-to-all-start.9 = ((bf16[4,128,768]{2,1,0:T(8,128)(2,1)}), bf16[4,128,768]{2,1,0:T(8,128)(2,1)S(1)}, u32[]{:S(2)}, u32[]{:S(2)}) async-start(bf16[4,128,768]{2,1,0:T(8,128)(2,1)} %pad_maximum_fusion.1), calls=%async_computation.9 | async-start | bytes 1572864 | tf_op jit(solution)/shard_map/all_to_all | solution.py:31
  168.3 10.5 %all-to-all-done.9 = bf16[4,128,768]{2,1,0:T(8,128)(2,1)S(1)} async-done(((bf16[4,128,768]{2,1,0:T(8,128)(2,1)}), bf16[4,128,768]{2,1,0:T(8,128)(2,1)S(1)}, u32[]{:S(2)}, u32[]{:S(2)}) %all-to-all-start.9) | async-done | bytes 786464 | tf_op jit(solution)/shard_map/all_to_all | solution.py:31
  179.1 0.4 convolution_convert_fusion.2
  179.6 2.5 %collective-permute-start.2 = (bf16[32,16,512]{2,1,0:T(8,128)(2,1)S(1)}, bf16[32,16,512]{2,1,0:T(8,128)(2,1)S(1)}, u32[]{:S(2)}, u32[]{:S(2)}) collective-permute-start(bf16[32,16,512]{2,1,0:T(8,128)(2,1)S(1)} %bitcast.86), channel_id=1, source_target_pairs={{0,4},{4,0},{1,5},{5,1},{2,6},{6,2},{3,7},{7,3},{8,12},{12,8},{9,1... | collective-permute-start | bytes 1572872 | tf_op jit(solution)/shard_map/ppermute | solution.py:40
  182.1 1.5 collective-permute-done.2
  183.6 1.0 fusion.6
  184.6 3.9 %all-to-all-start.10 = ((bf16[32,16,512]{2,1,0:T(8,128)(2,1)}), bf16[32,16,512]{2,1,0:T(8,128)(2,1)S(1)}, u32[]{:S(2)}, u32[]{:S(2)}) async-start(bf16[32,16,512]{2,1,0:T(8,128)(2,1)} %fusion.6), calls=%async_computation.10 | async-start | bytes 1048576 | tf_op jit(solution)/shard_map/all_to_all | solution.py:31
  188.5 1.3 fusion.52
  189.8 15.3 %all-to-all-done.10 = bf16[32,16,512]{2,1,0:T(8,128)(2,1)S(1)} async-done(((bf16[32,16,512]{2,1,0:T(8,128)(2,1)}), bf16[32,16,512]{2,1,0:T(8,128)(2,1)S(1)}, u32[]{:S(2)}, u32[]{:S(2)}) %all-to-all-start.10) | async-done | bytes 524320 | tf_op jit(solution)/shard_map/all_to_all | solution.py:31
  205.2 0.6 add_convert_fusion
  (93 shorter events, 4.0 us)
Async XLA Ops:
  0.6 160.2 %copy-start = (bf16[1,256,2048]{2,1,0:T(8,128)(2,1)S(1)}, bf16[1,256,2048]{2,1,0:T(8,128)(2,1)}, u32[]{:S(2)}) copy-start(bf16[1,256,2048]{2,1,0:T(8,128)(2,1)} %param.39) | copy-start | bytes 3145732
  0.6 25.4 %copy-start.1 = (bf16[16,2048]{1,0:T(8,128)(2,1)S(1)}, bf16[16,2048]{1,0:T(8,128)(2,1)}, u32[]{:S(2)}) copy-start(bf16[16,2048]{1,0:T(8,128)(2,1)} %param.20) | copy-start | bytes 196612
  0.7 41.5 %copy-start.4 = (f32[2048]{0:T(1024)S(1)}, f32[2048]{0:T(1024)}, u32[]{:S(2)}) copy-start(f32[2048]{0:T(1024)} %param.21) | copy-start | bytes 24580
  20.8 25.4 %copy-start.3 = (bf16[32,512]{1,0:T(8,128)(2,1)S(1)}, bf16[32,512]{1,0:T(8,128)(2,1)}, u32[]{:S(2)}) copy-start(bf16[32,512]{1,0:T(8,128)(2,1)} %param.22) | copy-start | bytes 98308
  20.8 25.4 %copy-start.5 = (bf16[32,128]{1,0:T(8,128)(2,1)S(1)}, bf16[32,128]{1,0:T(8,128)(2,1)}, u32[]{:S(2)}) copy-start(bf16[32,128]{1,0:T(8,128)(2,1)} %param.24) | copy-start | bytes 24580
  20.8 25.4 %copy-start.6 = (bf16[32,128]{1,0:T(8,128)(2,1)S(1)}, bf16[32,128]{1,0:T(8,128)(2,1)}, u32[]{:S(2)}) copy-start(bf16[32,128]{1,0:T(8,128)(2,1)} %param.23) | copy-start | bytes 24580
  21.9 47.6 %copy-start.10 = (f32[4]{0:T(128)S(1)}, f32[4]{0:T(128)}, u32[]{:S(2)}) copy-start(f32[4]{0:T(128)} %param.25) | copy-start | bytes 52
  21.9 16.4 %all-to-all-start.4 = ((bf16[4,256,512]{2,1,0:T(8,128)(2,1)}), bf16[4,256,512]{2,1,0:T(8,128)(2,1)S(1)}, u32[]{:S(2)}, u32[]{:S(2)}) async-start(bf16[4,256,512]{2,1,0:T(8,128)(2,1)} %broadcast_in_dim.101), calls=%async_computation.4 | async-start | bytes 2097152 | tf_op jit(solution)/shard_map/all_to_all | solution.py:31
  38.3 49.6 %collective-permute-start = (bf16[4,8,32,512]{3,2,1,0:T(8,128)(2,1)S(1)}, bf16[4,8,32,512]{3,2,1,0:T(8,128)(2,1)S(1)}, u32[]{:S(2)}, u32[]{:S(2)}) collective-permute-start(bf16[4,8,32,512]{3,2,1,0:T(8,128)(2,1)S(1)} %bitcast.79), channel_id=1, source_target_pairs={{0,4},{4,0},{1,5},{5,1},{2,6},{6,2},{3,7},{7,3},{8,12},{12,8},{9,1... | collective-permute-start | bytes 3145736 | tf_op jit(solution)/shard_map/ppermute | solution.py:40
  42.9 10.7 %all-to-all-start = ((bf16[8,16,256]{2,1,0:T(8,128)(2,1)}), bf16[8,16,256]{2,1,0:T(8,128)(2,1)S(1)}, u32[]{:S(2)}, u32[]{:S(2)}) async-start(bf16[8,16,256]{2,1,0:T(8,128)(2,1)} %copy.72), calls=%async_computation | async-start | bytes 131072 | tf_op jit(solution)/shard_map/all_to_all | solution.py:31
  66.1 12.4 %all-to-all-start.2 = ((bf16[8,16,768]{2,1,0:T(8,128)(2,1)}), bf16[8,16,768]{2,1,0:T(8,128)(2,1)S(1)}, u32[]{:S(2)}, u32[]{:S(2)}) async-start(bf16[8,16,768]{2,1,0:T(8,128)(2,1)} %bitcast.3), calls=%async_computation.2 | async-start | bytes 393216 | tf_op jit(solution)/shard_map/all_to_all | solution.py:31
  78.5 9.4 %copy-start.2 = (bf16[16,768]{1,0:T(8,128)(2,1)}, bf16[16,768]{1,0:T(8,128)(2,1)S(1)}, u32[]{:S(2)}) copy-start(bf16[16,768]{1,0:T(8,128)(2,1)S(1)} %reduce_sum.124) | copy-start | bytes 73732
  88.3 0.7 slice-start
  89.7 15.5 %copy-start.7 = (s32[16,4]{0,1:T(4,128)S(1)}, s32[16,4]{0,1:T(4,128)}, u32[]{:S(2)}) copy-start(s32[16,4]{0,1:T(4,128)} %param.35) | copy-start | bytes 772
  89.7 15.7 %copy-start.8 = (f32[16,4]{0,1:T(4,128)S(1)}, f32[16,4]{0,1:T(4,128)}, u32[]{:S(2)}) copy-start(f32[16,4]{0,1:T(4,128)} %param.36) | copy-start | bytes 772
  90.4 9.7 %all-to-all-start.5 = ((bf16[4,16,2048]{2,1,0:T(8,128)(2,1)}), bf16[4,16,2048]{2,1,0:T(8,128)(2,1)S(1)}, u32[]{:S(2)}, u32[]{:S(2)}) async-start(bf16[4,16,2048]{2,1,0:T(8,128)(2,1)} %broadcast_in_dim.102), calls=%async_computation.5 | async-start | bytes 524288 | tf_op jit(solution)/shard_map/all_to_all | solution.py:31
  101.2 17.2 %all-to-all-start.6 = ((bf16[32,16,512]{2,1,0:T(8,128)(2,1)}), bf16[32,16,512]{2,1,0:T(8,128)(2,1)S(1)}, u32[]{:S(2)}, u32[]{:S(2)}) async-start(bf16[32,16,512]{2,1,0:T(8,128)(2,1)} %broadcast_in_dim.103), calls=%async_computation.6 | async-start | bytes 1048576 | tf_op jit(solution)/shard_map/all_to_all | solution.py:31
  118.4 19.7 %all-to-all-start.7 = ((f32[64,1,128]{2,1,0:T(1,128)}), f32[64,1,128]{2,1,0:T(1,128)S(1)}, u32[]{:S(2)}, u32[]{:S(2)}) async-start(f32[64,1,128]{2,1,0:T(1,128)} %copy.74), calls=%async_computation.7 | async-start | bytes 65536 | tf_op jit(solution)/shard_map/all_to_all | solution.py:31
  129.7 9.0 %collective-permute-start.1 = (bf16[32,16,512]{2,1,0:T(8,128)(2,1)S(1)}, bf16[32,16,512]{2,1,0:T(8,128)(2,1)S(1)}, u32[]{:S(2)}, u32[]{:S(2)}) collective-permute-start(bf16[32,16,512]{2,1,0:T(8,128)(2,1)S(1)} %all-to-all-done.6), channel_id=1, source_target_pairs={{0,4},{4,0},{1,5},{5,1},{2,6},{6,2},{3,7},{7,3},{8,12},{12,8},{9,1... | collective-permute-start | bytes 1572872 | tf_op jit(solution)/shard_map/ppermute | solution.py:40
  164.4 14.7 %copy-start.9 = (bf16[128,512]{1,0:T(8,128)(2,1)S(1)}, bf16[128,512]{1,0:T(8,128)(2,1)}, u32[]{:S(2)}) copy-start(bf16[128,512]{1,0:T(8,128)(2,1)} %param.34) | copy-start | bytes 393220
  164.4 14.5 %all-to-all-start.9 = ((bf16[4,128,768]{2,1,0:T(8,128)(2,1)}), bf16[4,128,768]{2,1,0:T(8,128)(2,1)S(1)}, u32[]{:S(2)}, u32[]{:S(2)}) async-start(bf16[4,128,768]{2,1,0:T(8,128)(2,1)} %pad_maximum_fusion.1), calls=%async_computation.9 | async-start | bytes 1572864 | tf_op jit(solution)/shard_map/all_to_all | solution.py:31
  179.6 4.0 %collective-permute-start.2 = (bf16[32,16,512]{2,1,0:T(8,128)(2,1)S(1)}, bf16[32,16,512]{2,1,0:T(8,128)(2,1)S(1)}, u32[]{:S(2)}, u32[]{:S(2)}) collective-permute-start(bf16[32,16,512]{2,1,0:T(8,128)(2,1)S(1)} %bitcast.86), channel_id=1, source_target_pairs={{0,4},{4,0},{1,5},{5,1},{2,6},{6,2},{3,7},{7,3},{8,12},{12,8},{9,1... | collective-permute-start | bytes 1572872 | tf_op jit(solution)/shard_map/ppermute | solution.py:40
  184.6 20.5 %all-to-all-start.10 = ((bf16[32,16,512]{2,1,0:T(8,128)(2,1)}), bf16[32,16,512]{2,1,0:T(8,128)(2,1)S(1)}, u32[]{:S(2)}, u32[]{:S(2)}) async-start(bf16[32,16,512]{2,1,0:T(8,128)(2,1)} %fusion.6), calls=%async_computation.10 | async-start | bytes 1048576 | tf_op jit(solution)/shard_map/all_to_all | solution.py:31

commit v2 on v0

v2 whole, which is shorter than its diff:
```python
import functools
import jax
import jax.numpy as jnp
from jax import lax
from jax.experimental import pallas as pl
from jax.experimental.pallas import tpu as pltpu
from jax.sharding import Mesh
from jax.sharding import PartitionSpec as P

EP = ("z", "x", "c")
ZX = ("z", "x")

norm_eps = 1e-05
clamp_limit = 7.0
swish_alpha = 1.702
f32 = jnp.float32
bf16 = jnp.bfloat16
VM = pl.BlockSpec(memory_space=pltpu.VMEM)
SM = pl.BlockSpec(memory_space=pltpu.SMEM)

NX = 4


def rms_scale(values, gain):
    return values * lax.rsqrt(jnp.mean(values * values, axis=-1, keepdims=True) + norm_eps) * gain


def clamped_unit(gate_pre, up_pre):
    gate_c = jnp.minimum(gate_pre, clamp_limit)
    up_c = jnp.clip(up_pre, -clamp_limit, clamp_limit)
    return (up_c + 1.0) * gate_c * jax.nn.sigmoid(swish_alpha * gate_c)


def exchange(blocks, axes):
    return lax.all_to_all(blocks, axes, 0, 0, tiled=True)


def other_core(values):
    return lax.ppermute(values, "c", [(0, 1), (1, 0)])


def along_x(values, k):
    return lax.ppermute(values, "x", [(i, (i + k) % NX) for i in range(NX)])


def vmem(value):
    return pltpu.with_memory_space_constraint(value, pltpu.VMEM)


def local(kernel, name, outs, args, scratch=(), smem=0, keep=True, cost=None):
    multi = isinstance(outs, (list, tuple))
    if keep:
        outs = jax.tree.map(lambda s: pltpu.VMEM(s.shape, s.dtype), outs)
    args = tuple(args[:smem]) + tuple(vmem(a) for a in args[smem:])
    return pl.pallas_call(
        kernel,
        out_shape=outs,
        in_specs=[SM] * smem + [VM] * (len(args) - smem),
        out_specs=[VM] * len(outs) if multi else VM,
        scratch_shapes=list(scratch),
        compiler_params=pltpu.CompilerParams(vmem_limit_bytes=16 << 20),
        cost_estimate=cost,
        name=name,
    )(*args)


def sds(shape, dtype=bf16):
    return jax.ShapeDtypeStruct(tuple(shape), dtype)


def pick(parts, at):
    out = parts[0]
    for k in range(1, len(parts)):
        out = jnp.where(at == k, parts[k], out)
    return out


def prepare_kernel(nz, tok, gain, qw, kw, vw, owt, ids, rw, wcat, msg):
    qc, kc = qw.shape[1], kw.shape[1]
    wcat[:, :qc] = qw[...]
    wcat[:, qc : qc + kc] = kw[...]
    wcat[:, qc + kc :] = vw[...]
    normed = rms_scale(tok[...].astype(f32), gain[...]).astype(bf16)
    seqs = normed.shape[0]
    lane = lax.broadcasted_iota(jnp.int32, (seqs, 128), 1)
    hi = rw[...].astype(bf16).astype(f32)
    lo = rw[...] - hi
    idf = ids[...].astype(f32)
    top = idf.shape[1]
    meta = jnp.zeros((seqs, 128), f32)
    for k in range(top):
        meta = jnp.where(lane == k, idf[:, k : k + 1], meta)
        meta = jnp.where(lane == top + k, hi[:, k : k + 1], meta)
        meta = jnp.where(lane == 2 * top + k, lo[:, k : k + 1], meta)
    meta = meta.astype(bf16)
    heads = owt.shape[1]
    for z in range(nz):
        msg[z, :, :heads] = owt[...]
        msg[z, :seqs, heads : heads + 128] = meta
        msg[z, seqs:, heads : heads + 128] = meta
        msg[z, :seqs, heads + 128 :] = normed[:, z * 256 : z * 256 + 128]
        msg[z, seqs:, heads + 128 :] = normed[:, z * 256 + 128 : z * 256 + 256]


def project_kernel(at, got, w0, w1, w2, w3, wo, part, owm, w_s, f_s):
    x, c = at[1], at[2]
    nz, depth, wide = got.shape
    seqs = depth // 2
    for k, w in enumerate((w0, w1, w2, w3)):
        place = lax.rem(x + NX - k, NX) * 2
        w_s[pl.ds(pl.multiple_of((place + c) * depth, depth), depth)] = w[...]
        w_s[pl.ds(pl.multiple_of((place + 1 - c) * depth, depth), depth)] = wo[k]
    for z in range(nz):
        f_s[z * seqs : (z + 1) * seqs, :128] = got[z, :seqs, wide - 128 :]
        f_s[z * seqs : (z + 1) * seqs, 128:] = got[z, seqs:, wide - 128 :]
        owm[z] = got[z, :, : wide - 128]
    out = jnp.dot(f_s[...], w_s[...], preferred_element_type=f32).astype(bf16)
    for z in range(nz):
        part[z] = out[z * seqs : (z + 1) * seqs]


def attention_kernel(per_step, lengths, bias, part, k_ref, v_ref, att, nk, nv, q_s, a_s):
    seqs, _, span, head_dim = k_ref.shape
    heads = bias.shape[0]
    group = 8
    q_cols = heads * head_dim
    qkv = jnp.sum(part[...].astype(f32), axis=0)
    nk[...] = qkv[:, q_cols : q_cols + head_dim].astype(bf16)
    nv[...] = qkv[:, q_cols + head_dim :].astype(bf16)
    q_s[...] = jnp.zeros_like(q_s)
    for h in range(heads):
        q_s[:, h, :] = qkv[:, h * head_dim : (h + 1) * head_dim]

    rows = per_step * group
    row = lax.broadcasted_iota(jnp.int32, (rows, 1), 0)
    lane = lax.broadcasted_iota(jnp.int32, (rows, 128), 1)
    position = lax.broadcasted_iota(jnp.int32, (rows, span), 1)
    offset = jnp.zeros((rows, 1), f32)
    for h in range(heads):
        offset = jnp.where(row % group == h, bias[h], offset)

    @pl.loop(0, seqs // per_step)
    def _(step):
        scores = []
        length = jnp.zeros((rows, 1), jnp.int32)
        for i in range(per_step):
            q = q_s[step * per_step + i].astype(bf16)
            scores.append(
                lax.dot_general(
                    q,
                    k_ref[step * per_step + i, 0],
                    (((1,), (1,)), ((), ())),
                    preferred_element_type=f32,
                )
            )
            length = jnp.where(row // group == i, lengths[step * per_step + i], length)
        z = jnp.concatenate(scores, axis=0) * head_dim ** (-0.5) + offset
        inside = position < length
        tail = jnp.log1p(jnp.exp(-jnp.abs(z)))
        keep = jnp.where(inside, -jnp.maximum(z, 0.0) - tail, 0.0)
        take = jnp.minimum(z, 0.0) - tail
        chunks = span // 128
        after = jnp.zeros((rows, 1), f32)
        betweens = [None] * chunks
        for c in range(chunks - 1, -1, -1):
            own = keep[:, c * 128 : (c + 1) * 128]
            total = own
            shift = 1
            while shift < 128:
                moved = pltpu.roll(total, 128 - shift, 1)
                total = total + jnp.where(lane < 128 - shift, moved, 0.0)
                shift *= 2
            betweens[c] = total - own + after
            after = after + total[:, 0:1]
        between = jnp.concatenate(betweens, axis=1)
        weights = jnp.where(inside, jnp.exp(take + between), 0.0).astype(bf16)
        for i in range(per_step):
            a_s[step * per_step + i] = jnp.dot(
                weights[i * group : (i + 1) * group],
                v_ref[step * per_step + i, 0],
                preferred_element_type=f32,
            )

    for h in range(heads):
        att[:, h * head_dim : (h + 1) * head_dim] = a_s[:, h, :].astype(bf16)


def mix_kernel(at, att, *refs):
    mine, others, msg, w_s = refs[:NX], refs[NX : 2 * NX], refs[2 * NX], refs[2 * NX + 1]
    x, c = at[1], at[2]
    nz, depth = mine[0].shape[:2]
    heads = att.shape[1]
    for k in range(NX):
        place = lax.rem(x + NX - k, NX) * 2
        for z in range(nz):
            base = z * NX * 2
            w_s[pl.ds(pl.multiple_of((base + place + c) * depth, depth), depth)] = mine[k][
                z, :, :heads
            ]
            w_s[pl.ds(pl.multiple_of((base + place + 1 - c) * depth, depth), depth)] = others[k][
                z, :, :heads
            ]
    out = lax.dot_general(
        att[...], w_s[...], (((1,), (1,)), ((), ())), preferred_element_type=f32
    ).astype(bf16)
    for t in range(msg.shape[0]):
        msg[t] = out


def slots_kernel(seqs, heads, top, at, *refs):
    pieces = refs[: 2 * NX]
    pickm, him, lom, m_s = refs[2 * NX :]
    x = at[1]
    nz = pieces[0].shape[0]
    half = nz * NX * seqs
    for r in range(2):
        for k in range(NX):
            place = lax.rem(x + NX - k, NX) * seqs
            for z in range(nz):
                start = pl.multiple_of(r * half + z * NX * seqs + place, seqs)
                m_s[pl.ds(start, seqs)] = pieces[r * NX + k][z, :seqs, heads : heads + 128]
    expert = (at[0] * NX + x) * 2 + at[2]
    m = m_s[...].astype(f32)
    rows = m.shape[0]
    lane = lax.broadcasted_iota(jnp.int32, (rows, 128), 1)
    row = lax.broadcasted_iota(jnp.int32, (rows, 128), 0)
    hit = jnp.where((m == expert.astype(f32)) & (lane < top), 1.0, 0.0)
    hi = jnp.sum(hit * pltpu.roll(m, 128 - top, 1), axis=1, keepdims=True)
    lo = jnp.sum(hit * pltpu.roll(m, 128 - 2 * top, 1), axis=1, keepdims=True)
    own = jnp.broadcast_to(jnp.sum(hit, axis=1, keepdims=True), (rows, 128))
    upto = own
    shift = 1
    while shift < seqs:
        upto = upto + jnp.where(row % seqs >= shift, pltpu.roll(upto, shift, 0), 0.0)
        shift *= 2
    slot = (row // seqs) * 2 + (upto - own).astype(jnp.int32)
    here = jnp.where((lane == slot) & (own > 0.5), 1.0, 0.0)
    pickm[...] = here.astype(bf16)
    him[...] = (here * hi).astype(bf16)
    lom[...] = (here * lo).astype(bf16)


def norm_kernel(at, got, tok, gain, msg, res):
    t = at[3]
    mixed = jnp.sum(got[...].astype(f32), axis=0).astype(bf16).astype(f32)
    resid = tok[...].astype(f32) + mixed
    normed = rms_scale(resid, gain[...])
    wide = msg.shape[2]
    parts = resid.shape[1] // wide
    res[...] = pick([resid[:, k * wide : (k + 1) * wide] for k in range(parts)], t)
    own = pick([normed[:, k * wide : (k + 1) * wide] for k in range(parts)], t).astype(bf16)
    for b in range(msg.shape[0]):
        msg[b] = own


def spread_kernel(at, mine, other, dg, du, bg, pickm, msg, x_s, w_s):
    t = at[3]
    nb, seqs, wide = mine.shape
    half = nb * seqs
    cols = dg.shape[1]
    x_s[:half] = mine[...].reshape(half, wide)
    x_s[half:] = other[...].reshape(half, wide)
    w_s[:, :cols] = dg[...]
    w_s[:, cols:] = du[...]
    x = x_s[...]
    pre = jnp.dot(x, w_s[...], preferred_element_type=f32).astype(bf16)
    gate = pick([bg[:, k * wide : (k + 1) * wide] for k in range(bg.shape[1] // wide)], t)
    gate = jnp.broadcast_to(gate.astype(f32), (16, wide)).astype(bf16)
    branch = lax.dot_general(
        gate, x, (((1,), (1,)), ((), ())), preferred_element_type=f32
    ).astype(bf16)
    rows = lax.dot_general(
        pickm[...], x, (((0,), (0,)), ((), ())), preferred_element_type=f32
    ).astype(bf16)
    nt = msg.shape[0]
    quarter = 2 * half // nt
    slots = rows.shape[0]
    fold = wide // 2
    for q in range(nt):
        msg[q, :quarter, :fold] = pre[q * quarter : (q + 1) * quarter]
        msg[q, :slots, fold:] = rows[:, :fold]
        msg[q, slots:quarter, fold:] = rows[:, fold:]
        msg[q, quarter:, :fold] = branch[:, q * quarter : (q + 1) * quarter]
        msg[q, quarter:, fold:] = branch[:, q * quarter : (q + 1) * quarter]


def expert_kernel(got, eg, eu, ed, msg):
    nt, rows, wide = got.shape
    quarter = rows - 16
    fold = wide // 2
    slots = quarter // 2
    gate_pre = up_pre = None
    for t in range(nt):
        x = jnp.concatenate([got[t, :slots, fold:], got[t, slots:quarter, fold:]], axis=1)
        g = jnp.dot(x, eg[0, t * wide : (t + 1) * wide], preferred_element_type=f32)
        u = jnp.dot(x, eu[0, t * wide : (t + 1) * wide], preferred_element_type=f32)
        gate_pre = g if gate_pre is None else gate_pre + g
        up_pre = u if up_pre is None else up_pre + u
    act = clamped_unit(gate_pre, up_pre).astype(bf16)
    out = jnp.dot(act, ed[0], preferred_element_type=f32).astype(bf16)
    pre = jnp.sum(got[:, :quarter, :fold].astype(f32), axis=0)
    cols = fold // 2
    branch = jnp.sum(got[:, quarter : quarter + 16, :fold].astype(f32), axis=0)[0:1]
    r = lax.broadcasted_iota(jnp.int32, (quarter, quarter), 0)
    c = lax.broadcasted_iota(jnp.int32, (quarter, quarter), 1)
    branch = jnp.sum(jnp.where(r == c, branch, 0.0), axis=1, keepdims=True)
    hidden = jax.nn.silu(pre[:, :cols]) * pre[:, cols:] * jax.nn.sigmoid(branch)
    hidden = hidden.astype(bf16)
    for t in range(nt):
        msg[t, :, :wide] = out[:, t * wide : (t + 1) * wide]
        msg[t, :, wide : wide + cols] = hidden[:slots]
        msg[t, :, wide + cols :] = hidden[slots:]


def block_kernel(which, got, dd, him, lom, out):
    nt, slots, wide = got.shape
    cols = dd.shape[0]
    wide = wide - 2 * cols
    rows = jnp.sum(got[:, :, :wide].astype(f32), axis=0).astype(bf16)
    half = out.shape[0] * out.shape[1]
    hidden = []
    for q in range(which * nt // 2, (which + 1) * nt // 2):
        hidden.append(got[q, :, wide : wide + cols])
        hidden.append(got[q, :, wide + cols :])
    left = jnp.concatenate(
        [
            jnp.concatenate(hidden, axis=0),
            him[which * half : (which + 1) * half],
            lom[which * half : (which + 1) * half],
        ],
        axis=1,
    )
    right = jnp.concatenate([dd[...], rows, rows], axis=0)
    full = jnp.dot(left, right, preferred_element_type=f32)
    out[...] = full.astype(out.dtype).reshape(out.shape)


def add_kernel(a, b, out):
    out[...] = (a[...] + b[...].astype(f32)).astype(bf16)


def final_kernel(got, res, out):
    out[...] = (jnp.sum(got[...].astype(f32), axis=0) + res[...]).astype(bf16)


def body(
    tokens,
    attn_gain,
    query_weight,
    key_weight,
    value_weight,
    break_bias,
    cache_keys,
    cache_values,
    lengths,
    out_weight,
    ffn_gain,
    branch_gate,
    dense_gate,
    dense_up,
    dense_down,
    route_ids,
    route_weights,
    expert_gate,
    expert_up,
    expert_down,
):
    nz, nt = lax.axis_size("z"), lax.axis_size("tp")
    nzx = nz * NX
    seqs, width = tokens.shape
    top = route_ids.shape[1]
    slice_width = width // nt
    all_rows = 2 * nzx * seqs
    slots = 2 * nzx * 2
    depth = query_weight.shape[0]
    heads = out_weight.shape[0]
    proj = query_weight.shape[1] + 2 * key_weight.shape[1]
    at = jnp.stack([lax.axis_index(a) for a in ("z", "x", "c", "tp")]).astype(jnp.int32)

    busy = pl.CostEstimate(flops=20_000_000_000, transcendentals=0, bytes_accessed=1 << 20)
    wcat, msg = local(
        functools.partial(prepare_kernel, nz),
        "prepare",
        [sds((depth, proj)), sds((nz, depth, heads + 256))],
        (
            tokens,
            attn_gain[None],
            query_weight,
            key_weight,
            value_weight,
            out_weight.T,
            route_ids,
            route_weights,
        ),
    )
    got = exchange(msg, "z")
    w_x = [wcat] + [along_x(wcat, k) for k in range(1, NX)]
    w_other = other_core(jnp.stack(w_x))
    part, owm = local(
        project_kernel,
        "project",
        [sds((nz, seqs, proj)), sds((nz, depth, heads + 128))],
        (at, got, *w_x, w_other),
        [pltpu.VMEM((2 * NX * depth, proj), bf16), pltpu.VMEM((nz * seqs, 2 * NX * depth), bf16)],
        smem=1,
        cost=busy,
    )
    part = exchange(part, "z")
    ow = [owm] + [along_x(owm, k) for k in range(1, NX)]
    ow_other = [other_core(piece) for piece in ow]

    head_dim = cache_keys.shape[3]
    attended, new_keys, new_values = local(
        functools.partial(attention_kernel, 4),
        "attention",
        [sds((seqs, heads)), sds((seqs, head_dim)), sds((seqs, head_dim))],
        (lengths, break_bias, part, cache_keys, cache_values),
        [pltpu.VMEM((seqs, 8, head_dim), f32)] * 2,
        smem=2,
    )

    msg = local(
        mix_kernel,
        "mix",
        sds((nt, seqs, width)),
        (at, attended, *ow, *ow_other),
        [pltpu.VMEM((width, heads), bf16)],
        smem=1,
    )
    mixed = exchange(msg, "tp")
    pickm, him, lom = local(
        functools.partial(slots_kernel, seqs, heads, top),
        "slots",
        [sds((all_rows, slots))] * 3,
        (at, *ow, *ow_other),
        [pltpu.VMEM((all_rows, 128), bf16)],
        smem=1,
    )
    msg, resid = local(
        norm_kernel,
        "norm",
        [sds((nzx, seqs, slice_width)), sds((seqs, slice_width), f32)],
        (at, mixed, tokens, ffn_gain[None]),
        smem=1,
    )
    mine = exchange(msg, ZX)
    other = other_core(mine)
    cols = dense_gate.shape[1]
    msg = local(
        spread_kernel,
        "spread",
        sds((nt, all_rows // nt + 16, slice_width)),
        (at, mine, other, dense_gate, dense_up, branch_gate[None], pickm),
        [pltpu.VMEM((all_rows, slice_width), bf16), pltpu.VMEM((slice_width, 2 * cols), bf16)],
        smem=1,
    )
    got = exchange(msg, "tp")
    msg = local(
        expert_kernel,
        "expert",
        sds((nt, slots, slice_width + 2 * cols)),
        (got, expert_gate, expert_up, expert_down),
    )
    got = exchange(msg, "tp")
    parts = (got, dense_down, him, lom)
    shape = (nzx, seqs, slice_width)
    sent = local(functools.partial(block_kernel, 1), "block_other", sds(shape), parts)
    arrived = other_core(sent)
    kept = local(functools.partial(block_kernel, 0), "block_mine", sds(shape, f32), parts)
    block = local(add_kernel, "add", sds(shape), (kept, arrived))
    got = exchange(block, ZX)
    out = local(final_kernel, "final", sds((seqs, slice_width)), (got, resid), keep=False)
    return out, new_keys, new_values


def solution(mesh):
    shape = (mesh.shape["ep"] // (2 * NX), NX, 2, mesh.shape["tp"])
    split = Mesh(mesh.devices.reshape(shape), ("z", "x", "c", "tp"))
    return jax.shard_map(
        body,
        mesh=split,
        in_specs=(
            P(EP, None),
            P(),
            P(EP, "tp"),
            P(EP, "tp"),
            P(EP, "tp"),
            P("tp"),
            P(EP, "tp", None, None),
            P(EP, "tp", None, None),
            P(EP),
            P("tp", EP),
            P(),
            P(),
            P("tp", EP),
            P("tp", EP),
            P(EP, "tp"),
            P(EP, None),
            P(EP, None),
            P(EP, None, "tp"),
            P(EP, None, "tp"),
            P(EP, "tp", None),
        ),
        out_specs=(P(EP, "tp"), P(EP, "tp"), P(EP, "tp")),
        check_vma=False,
    )
```

time: 364 us -> 161 us (0.44)
  waiting for transfers between devices: 148 us -> 28 us
  other arithmetic: 84.7 us -> 0.1 us
  blocking collectives: 33.2 us -> 60.3 us
  matrix products: 20.1 us -> 0 us
  Pallas kernels: 0 us -> 15.9 us
  between operations: 14.5 us -> 0.87 us
  starting transfers between devices: 48.4 us -> 42.8 us
    all_gather x2 -> x0, waiting for transfers between devices: 84.2 us -> none  [the longest x1 70.4 us: in_one_piece(): whole = lax.all_gather(both, axis, axis=dim, tiled=True)]
    another operation x3 -> x2, other arithmetic: 79.9 us -> 0.1 us  [the longest x1 0.08 us: body(): jnp.stack([lax.axis_index(a) for a in ('z', 'x', 'c', 'tp')])]
    all_to_all x0 -> x4, blocking collectives: none -> 60.3 us  [exchange(): return lax.all_to_all(blocks, axes, 0, 0, tiled=True)]
    all_to_all x7 -> x3, waiting for transfers between devices: 64.2 us -> 18.7 us  [exchange(): return lax.all_to_all(blocks, axes, 0, 0, tiled=True)]
    all_gather x2 -> x0, blocking collectives: 33.2 us -> none  [all_blocks(): blocks = lax.all_gather(blocks, axes[k], axis=0, tiled=True)]
    all_to_all x7 -> x3, starting transfers between devices: 48.3 us -> 17 us  [exchange(): return lax.all_to_all(blocks, axes, 0, 0, tiled=True)]
    ppermute x0 -> x13, starting transfers between devices: none -> 25.9 us  [the longest x7 18.6 us: other_core(): return lax.ppermute(values, 'c', [(0, 1), (1, 0)])]
    dot_general x13 -> x0, matrix products: 20.1 us -> none  [the longest x1 4.08 us: body(): jnp.einsum('sgrd,sgld->sgrl', query_heads, cache_keys, preferred_element_...]
  transfers between devices with their start and end apart: 9 -> 16, of which waited for: 6 -> 8; matrix products, arithmetic and copies ran while one was open for 31% -> 1% of each run, Pallas kernels for 0% -> 5%
where the time goes in v2:
time: 161 us; the launch traced here: 160 us
  blocking collectives  60.3 us (37%)
  starting transfers between devices  42.8 us (27%)
  waiting for transfers between devices  28 us (17%)
  Pallas kernels  15.9 us (10%)
  local copies, waits for them, and re-layouts  11.6 us (7%)
    all_to_all x4, blocking collectives, exchange(): return lax.all_to_all(blocks, axes, 0, 0, tiled=True)  60.3 us
    all_to_all x3, waiting for transfers between devices, exchange(): return lax.all_to_all(blocks, axes, 0, 0, tiled=True)  18.7 us
    ppermute x7, starting transfers between devices, other_core(): return lax.ppermute(values, 'c', [(0, 1), (1, 0)])  18.6 us
    all_to_all x3, starting transfers between devices, exchange(): return lax.all_to_all(blocks, axes, 0, 0, tiled=True)  17 us
    pallas_call x12, Pallas kernels, local(): pl.pallas_call(kernel, out_shape=outs, in_specs=[SM] * smem + [VM] * (len...  15.9 us
    unnamed x42, local copies, waits for them, and re-layouts  11.6 us
    ppermute x6, waiting for transfers between devices, along_x(): return lax.ppermute(values, 'x', [(i, (i + k) % NX) for i in range(NX)])  7.31 us
    ppermute x6, starting transfers between devices, along_x(): return lax.ppermute(values, 'x', [(i, (i + k) % NX) for i in range(NX)])  7.21 us
  transfers between devices with their start and end apart: 16, of which 8 were waited for; matrix products, arithmetic and copies ran while one was open for 1% of the time, Pallas kernels for 5%

profile of v2, /device:TPU:1, one launch (start us, length us, event | category | flops | bytes accessed | tf_op | source)
XLA Modules:
  0.0 159.6 jit_solution(12874565599634608162)
XLA Ops:
  0.6 0.8 copy.23.ids
  1.4 0.8 copy.24.rw
  2.1 0.8 copy-done.6
  3.0 0.8 copy-done.10
  3.7 0.8 copy-done.11
  4.5 0.7 copy-done.12
  5.2 0.7 copy-done.13
  5.9 0.7 copy-done.14
  6.6 0.9 prepare.1
  7.5 9.0 %all-to-all-start = ((bf16[8,32,768]{2,1,0:T(8,128)(2,1)}), bf16[8,32,768]{2,1,0:T(8,128)(2,1)S(1)}, u32[]{:S(2)}, u32[]{:S(2)}) async-start(bf16[8,32,768]{2,1,0:T(8,128)(2,1)} %get-tuple-element.15), calls=%async_computation | async-start | bytes 786432 | tf_op jit(solution)/shard_map/all_to_all | solution.py:35
  16.5 2.5 %collective-permute-start.2 = (bf16[32,768]{1,0:T(8,128)(2,1)S(1)}, bf16[32,768]{1,0:T(8,128)(2,1)S(1)}, u32[]{:S(2)}, u32[]{:S(2)}) collective-permute-start(bf16[32,768]{1,0:T(8,128)(2,1)S(1)} %get-tuple-element.16.w0), channel_id=1, source_target_pairs={{0,24},{8,0},{16,8},{24,16},{1,25},{9,1},{17,9},{25,17},{2,26},{10... | collective-permute-start | bytes 147464 | tf_op jit(solution)/shard_map/ppermute | solution.py:43
  19.0 0.5 collective-permute-start.1
  19.5 0.6 collective-permute-start
  20.1 3.3 %collective-permute-done.1.w2 = bf16[32,768]{1,0:T(8,128)(2,1)S(1)} collective-permute-done((bf16[32,768]{1,0:T(8,128)(2,1)S(1)}, bf16[32,768]{1,0:T(8,128)(2,1)S(1)}, u32[]{:S(2)}, u32[]{:S(2)}) %collective-permute-start.1) | collective-permute-done | bytes 49184 | tf_op jit(solution)/shard_map/ppermute | solution.py:43
  23.4 0.8 collective-permute-done.w1
  24.3 2.2 %collective-permute-start.3 = (bf16[4,32,768]{2,1,0:T(8,128)(2,1)S(1)}, bf16[4,32,768]{2,1,0:T(8,128)(2,1)S(1)}, u32[]{:S(2)}, u32[]{:S(2)}) collective-permute-start(bf16[4,32,768]{2,1,0:T(8,128)(2,1)S(1)} %pad_maximum_fusion), channel_id=1, source_target_pairs={{0,4},{4,0},{1,5},{5,1},{2,6},{6,2},{3,7},{7,3},{8,12},{12,8},{9,1... | collective-permute-start | bytes 589832 | tf_op jit(solution)/shard_map/ppermute | solution.py:39
  26.5 1.0 collective-permute-done.3.wo
  27.5 3.2 %all-to-all-done.got = bf16[8,32,768]{2,1,0:T(8,128)(2,1)S(1)} async-done(((bf16[8,32,768]{2,1,0:T(8,128)(2,1)}), bf16[8,32,768]{2,1,0:T(8,128)(2,1)S(1)}, u32[]{:S(2)}, u32[]{:S(2)}) %all-to-all-start) | async-done | bytes 393248 | tf_op jit(solution)/shard_map/all_to_all | solution.py:35
  30.7 1.5 project.1
  32.2 2.5 %collective-permute-start.6 = (bf16[8,32,640]{2,1,0:T(8,128)(2,1)S(1)}, bf16[8,32,640]{2,1,0:T(8,128)(2,1)S(1)}, u32[]{:S(2)}, u32[]{:S(2)}) collective-permute-start(bf16[8,32,640]{2,1,0:T(8,128)(2,1)S(1)} %get-tuple-element.19.refs_0_), channel_id=1, source_target_pairs={{0,24},{8,0},{16,8},{24,16},{1,25},{9,1},{17,9},{25,17},{2,26},{10... | collective-permute-start | bytes 983048 | tf_op jit(solution)/shard_map/ppermute | solution.py:43
  34.7 0.5 collective-permute-start.5
  35.2 0.6 collective-permute-start.4
  35.8 3.5 %all-to-all-start.1 = ((bf16[8,16,768]{2,1,0:T(8,128)(2,1)}), bf16[8,16,768]{2,1,0:T(8,128)(2,1)S(1)}, u32[]{:S(2)}, u32[]{:S(2)}) async-start(bf16[8,16,768]{2,1,0:T(8,128)(2,1)} %get-tuple-element.17), calls=%async_computation.1 | async-start | bytes 393216 | tf_op jit(solution)/shard_map/all_to_all | solution.py:35
  39.4 2.3 %collective-permute-start.7 = (bf16[8,32,640]{2,1,0:T(8,128)(2,1)S(1)}, bf16[8,32,640]{2,1,0:T(8,128)(2,1)S(1)}, u32[]{:S(2)}, u32[]{:S(2)}) collective-permute-start(bf16[8,32,640]{2,1,0:T(8,128)(2,1)S(1)} %get-tuple-element.19.refs_0_), channel_id=1, source_target_pairs={{0,4},{4,0},{1,5},{5,1},{2,6},{6,2},{3,7},{7,3},{8,12},{12,8},{9,1... | collective-permute-start | bytes 983048 | tf_op jit(solution)/shard_map/ppermute | solution.py:39
  41.7 8.0 %collective-permute-start.10 = (bf16[8,32,640]{2,1,0:T(8,128)(2,1)S(1)}, bf16[8,32,640]{2,1,0:T(8,128)(2,1)S(1)}, u32[]{:S(2)}, u32[]{:S(2)}) collective-permute-start(bf16[8,32,640]{2,1,0:T(8,128)(2,1)S(1)} %collective-permute-done.6.refs_3_), channel_id=1, source_target_pairs={{0,4},{4,0},{1,5},{5,1},{2,6},{6,2},{3,7},{7,3},{8,12},{12,8},{9,1... | collective-permute-start | bytes 983048 | tf_op jit(solution)/shard_map/ppermute | solution.py:39
  49.7 3.2 %collective-permute-done.4.refs_1_ = bf16[8,32,640]{2,1,0:T(8,128)(2,1)S(1)} collective-permute-done((bf16[8,32,640]{2,1,0:T(8,128)(2,1)S(1)}, bf16[8,32,640]{2,1,0:T(8,128)(2,1)S(1)}, u32[]{:S(2)}, u32[]{:S(2)}) %collective-permute-start.4) | collective-permute-done | bytes 327712 | tf_op jit(solution)/shard_map/ppermute | solution.py:43
  52.9 0.5 collective-permute-start.8
  53.4 2.2 %copy-done = bf16[16,1,1024,128]{3,2,1,0:T(8,128)(2,1)S(1)} copy-done((bf16[16,1,1024,128]{3,2,1,0:T(8,128)(2,1)S(1)}, bf16[16,1,1024,128]{3,2,1,0:T(8,128)(2,1)}, u32[]{:S(2)}) %copy-start) | copy-done | bytes 4194328
  55.6 2.2 %copy-done.1 = bf16[16,1,1024,128]{3,2,1,0:T(8,128)(2,1)S(1)} copy-done((bf16[16,1,1024,128]{3,2,1,0:T(8,128)(2,1)S(1)}, bf16[16,1,1024,128]{3,2,1,0:T(8,128)(2,1)}, u32[]{:S(2)}) %copy-start.1) | copy-done | bytes 4194328
  57.8 5.3 %attention.1 = (bf16[16,512]{1,0:T(8,128)(2,1)S(1)}, bf16[16,128]{1,0:T(8,128)(2,1)S(1)}, bf16[16,128]{1,0:T(8,128)(2,1)S(1)}) custom-call(s32[16]{0:T(128)S(1)} %copy-done.16, f32[4]{0:T(128)S(1)} %copy-done.17, bf16[8,16,768]{2,1,0:T(8,128)(2,1)S(1)} %all-to-all-done.1.part, bf16[16,1,1024,128]{3,2,1,0:T(8,128)(2,1)S(1)} %copy-done, ...), custom_call_target="tpu_custom_call" | custom-call | tf_op jit(solution)/shard_map/attention/pallas_call | solution.py:55
  63.1 1.3 mix.1
  64.5 10.5 %all_to_all.35.got = bf16[4,16,2048]{2,1,0:T(8,128)(2,1)S(1)} all-to-all(bf16[4,16,2048]{2,1,0:T(8,128)(2,1)S(1)} %mix.1), channel_id=1, replica_groups=mesh['z'=8,'x'=4,'c'=2,'tp'=4] {'tp'}, dimensions={0} | all-to-all | bytes 524288 | tf_op jit(solution)/shard_map/all_to_all | solution.py:35
  74.9 0.7 norm.1
  75.7 18.9 %all_to_all.36.mine = bf16[32,16,512]{2,1,0:T(8,128)(2,1)S(1)} all-to-all(bf16[32,16,512]{2,1,0:T(8,128)(2,1)S(1)} %get-tuple-element.20), channel_id=1, replica_groups=mesh['z'=8,'x'=4,'c'=2,'tp'=4] {'z','x'}, dimensions={0} | all-to-all | bytes 1048576 | tf_op jit(solution)/shard_map/all_to_all | solution.py:35
  94.6 3.0 %collective-permute-start.11 = (bf16[32,16,512]{2,1,0:T(8,128)(2,1)S(1)}, bf16[32,16,512]{2,1,0:T(8,128)(2,1)S(1)}, u32[]{:S(2)}, u32[]{:S(2)}) collective-permute-start(bf16[32,16,512]{2,1,0:T(8,128)(2,1)S(1)} %all_to_all.36.mine), channel_id=1, source_target_pairs={{0,4},{4,0},{1,5},{5,1},{2,6},{6,2},{3,7},{7,3},{8,12},{12,8},{9,1... | collective-permute-start | bytes 1572872 | tf_op jit(solution)/shard_map/ppermute | solution.py:39
  97.6 1.6 %slots.1 = (bf16[1024,128]{1,0:T(8,128)(2,1)S(1)}, bf16[1024,128]{1,0:T(8,128)(2,1)S(1)}, bf16[1024,128]{1,0:T(8,128)(2,1)S(1)}) custom-call(s32[4]{0:T(128)S(1)} %pad_add_fusion.at, bf16[8,32,640]{2,1,0:T(8,128)(2,1)S(1)} %get-tuple-element.19.refs_0_, bf16[8,32,640]{2,1,0:T(8,128)(2,1)S(1)} %collective-permute-done.4.refs_1_, ...), custom_call_target="tpu_custom_call" | custom-call | tf_op jit(solution)/shard_map/slots/pallas_call | solution.py:55
  99.2 1.4 spread.1
  100.7 17.9 %all_to_all.37.got = bf16[4,272,512]{2,1,0:T(8,128)(2,1)S(1)} all-to-all(bf16[4,272,512]{2,1,0:T(8,128)(2,1)S(1)} %spread.1), channel_id=1, replica_groups=mesh['z'=8,'x'=4,'c'=2,'tp'=4] {'tp'}, dimensions={0} | all-to-all | bytes 2228224 | tf_op jit(solution)/shard_map/all_to_all | solution.py:35
  118.5 0.7 expert.1
  119.3 13.1 %all_to_all.38.got = bf16[4,128,768]{2,1,0:T(8,128)(2,1)S(1)} all-to-all(bf16[4,128,768]{2,1,0:T(8,128)(2,1)S(1)} %expert.1), channel_id=1, replica_groups=mesh['z'=8,'x'=4,'c'=2,'tp'=4] {'tp'}, dimensions={0} | all-to-all | bytes 1572864 | tf_op jit(solution)/shard_map/all_to_all | solution.py:35
  132.8 2.7 %collective-permute-start.12 = (bf16[32,16,512]{2,1,0:T(8,128)(2,1)S(1)}, bf16[32,16,512]{2,1,0:T(8,128)(2,1)S(1)}, u32[]{:S(2)}, u32[]{:S(2)}) collective-permute-start(bf16[32,16,512]{2,1,0:T(8,128)(2,1)S(1)} %block_other.1), channel_id=1, source_target_pairs={{0,4},{4,0},{1,5},{5,1},{2,6},{6,2},{3,7},{7,3},{8,12},{12,8},{9,1... | collective-permute-start | bytes 1572872 | tf_op jit(solution)/shard_map/ppermute | solution.py:39
  136.0 1.1 collective-permute-done.12.b
  137.0 0.9 add.7
  137.9 4.4 %all-to-all-start.6 = ((bf16[32,16,512]{2,1,0:T(8,128)(2,1)}), bf16[32,16,512]{2,1,0:T(8,128)(2,1)S(1)}, u32[]{:S(2)}, u32[]{:S(2)}) async-start(bf16[32,16,512]{2,1,0:T(8,128)(2,1)} %add.7), calls=%async_computation.6 | async-start | bytes 1048576 | tf_op jit(solution)/shard_map/all_to_all | solution.py:35
  142.3 0.6 copy.25
  142.9 0.6 copy.26
  143.5 15.4 %all-to-all-done.6.got = bf16[32,16,512]{2,1,0:T(8,128)(2,1)S(1)} async-done(((bf16[32,16,512]{2,1,0:T(8,128)(2,1)}), bf16[32,16,512]{2,1,0:T(8,128)(2,1)S(1)}, u32[]{:S(2)}, u32[]{:S(2)}) %all-to-all-start.6) | async-done | bytes 524320 | tf_op jit(solution)/shard_map/all_to_all | solution.py:35
  159.0 0.7 final.1
  (45 shorter events, 1.2 us)
Async XLA Ops:
  2.1 0.8 copy-start.6
  3.0 0.8 copy-start.10
  3.7 0.8 copy-start.11
  4.5 0.7 copy-start.12
  5.2 0.7 copy-start.13
  5.9 0.7 copy-start.14
  7.5 23.3 %all-to-all-start = ((bf16[8,32,768]{2,1,0:T(8,128)(2,1)}), bf16[8,32,768]{2,1,0:T(8,128)(2,1)S(1)}, u32[]{:S(2)}, u32[]{:S(2)}) async-start(bf16[8,32,768]{2,1,0:T(8,128)(2,1)} %get-tuple-element.15), calls=%async_computation | async-start | bytes 786432 | tf_op jit(solution)/shard_map/all_to_all | solution.py:35
  16.5 3.7 %collective-permute-start.2 = (bf16[32,768]{1,0:T(8,128)(2,1)S(1)}, bf16[32,768]{1,0:T(8,128)(2,1)S(1)}, u32[]{:S(2)}, u32[]{:S(2)}) collective-permute-start(bf16[32,768]{1,0:T(8,128)(2,1)S(1)} %get-tuple-element.16.w0), channel_id=1, source_target_pairs={{0,24},{8,0},{16,8},{24,16},{1,25},{9,1},{17,9},{25,17},{2,26},{10... | collective-permute-start | bytes 147464 | tf_op jit(solution)/shard_map/ppermute | solution.py:43
  19.0 4.5 %collective-permute-start.1 = (bf16[32,768]{1,0:T(8,128)(2,1)S(1)}, bf16[32,768]{1,0:T(8,128)(2,1)S(1)}, u32[]{:S(2)}, u32[]{:S(2)}) collective-permute-start(bf16[32,768]{1,0:T(8,128)(2,1)S(1)} %get-tuple-element.16.w0), channel_id=1, source_target_pairs={{0,16},{8,24},{16,0},{24,8},{1,17},{9,25},{17,1},{25,9},{2,18},{10... | collective-permute-start | bytes 147464 | tf_op jit(solution)/shard_map/ppermute | solution.py:43
  19.5 4.7 %collective-permute-start = (bf16[32,768]{1,0:T(8,128)(2,1)S(1)}, bf16[32,768]{1,0:T(8,128)(2,1)S(1)}, u32[]{:S(2)}, u32[]{:S(2)}) collective-permute-start(bf16[32,768]{1,0:T(8,128)(2,1)S(1)} %get-tuple-element.16.w0), channel_id=1, source_target_pairs={{0,8},{8,16},{16,24},{24,0},{1,9},{9,17},{17,25},{25,1},{2,10},{10... | collective-permute-start | bytes 147464 | tf_op jit(solution)/shard_map/ppermute | solution.py:43
  24.3 3.2 %collective-permute-start.3 = (bf16[4,32,768]{2,1,0:T(8,128)(2,1)S(1)}, bf16[4,32,768]{2,1,0:T(8,128)(2,1)S(1)}, u32[]{:S(2)}, u32[]{:S(2)}) collective-permute-start(bf16[4,32,768]{2,1,0:T(8,128)(2,1)S(1)} %pad_maximum_fusion), channel_id=1, source_target_pairs={{0,4},{4,0},{1,5},{5,1},{2,6},{6,2},{3,7},{7,3},{8,12},{12,8},{9,1... | collective-permute-start | bytes 589832 | tf_op jit(solution)/shard_map/ppermute | solution.py:39
  26.5 26.9 %copy-start.16 = (s32[16]{0:T(128)S(1)}, s32[16]{0:T(128)}, u32[]{:S(2)}) copy-start(s32[16]{0:T(128)} %lengths.1) | copy-start | bytes 196
  26.5 26.9 %copy-start.17 = (f32[4]{0:T(128)S(1)}, f32[4]{0:T(128)}, u32[]{:S(2)}) copy-start(f32[4]{0:T(128)} %bias.1) | copy-start | bytes 52
  32.2 9.4 %collective-permute-start.6 = (bf16[8,32,640]{2,1,0:T(8,128)(2,1)S(1)}, bf16[8,32,640]{2,1,0:T(8,128)(2,1)S(1)}, u32[]{:S(2)}, u32[]{:S(2)}) collective-permute-start(bf16[8,32,640]{2,1,0:T(8,128)(2,1)S(1)} %get-tuple-element.19.refs_0_), channel_id=1, source_target_pairs={{0,24},{8,0},{16,8},{24,16},{1,25},{9,1},{17,9},{25,17},{2,26},{10... | collective-permute-start | bytes 983048 | tf_op jit(solution)/shard_map/ppermute | solution.py:43
  34.7 15.0 %collective-permute-start.5 = (bf16[8,32,640]{2,1,0:T(8,128)(2,1)S(1)}, bf16[8,32,640]{2,1,0:T(8,128)(2,1)S(1)}, u32[]{:S(2)}, u32[]{:S(2)}) collective-permute-start(bf16[8,32,640]{2,1,0:T(8,128)(2,1)S(1)} %get-tuple-element.19.refs_0_), channel_id=1, source_target_pairs={{0,16},{8,24},{16,0},{24,8},{1,17},{9,25},{17,1},{25,9},{2,18},{10... | collective-permute-start | bytes 983048 | tf_op jit(solution)/shard_map/ppermute | solution.py:43
  35.2 17.6 %collective-permute-start.4 = (bf16[8,32,640]{2,1,0:T(8,128)(2,1)S(1)}, bf16[8,32,640]{2,1,0:T(8,128)(2,1)S(1)}, u32[]{:S(2)}, u32[]{:S(2)}) collective-permute-start(bf16[8,32,640]{2,1,0:T(8,128)(2,1)S(1)} %get-tuple-element.19.refs_0_), channel_id=1, source_target_pairs={{0,8},{8,16},{16,24},{24,0},{1,9},{9,17},{17,25},{25,1},{2,10},{10... | collective-permute-start | bytes 983048 | tf_op jit(solution)/shard_map/ppermute | solution.py:43
  35.8 39.1 %copy-start.7 = (bf16[16,2048]{1,0:T(8,128)(2,1)S(1)}, bf16[16,2048]{1,0:T(8,128)(2,1)}, u32[]{:S(2)}) copy-start(bf16[16,2048]{1,0:T(8,128)(2,1)} %tok.3) | copy-start | bytes 196612
  35.8 39.1 %copy-start.15 = (f32[2048]{0:T(1024)S(1)}, f32[2048]{0:T(1024)}, u32[]{:S(2)}) copy-start(f32[2048]{0:T(1024)} %param.30) | copy-start | bytes 24580
  35.8 17.5 %all-to-all-start.1 = ((bf16[8,16,768]{2,1,0:T(8,128)(2,1)}), bf16[8,16,768]{2,1,0:T(8,128)(2,1)S(1)}, u32[]{:S(2)}, u32[]{:S(2)}) async-start(bf16[8,16,768]{2,1,0:T(8,128)(2,1)} %get-tuple-element.17), calls=%async_computation.1 | async-start | bytes 393216 | tf_op jit(solution)/shard_map/all_to_all | solution.py:35
  39.4 23.7 %collective-permute-start.7 = (bf16[8,32,640]{2,1,0:T(8,128)(2,1)S(1)}, bf16[8,32,640]{2,1,0:T(8,128)(2,1)S(1)}, u32[]{:S(2)}, u32[]{:S(2)}) collective-permute-start(bf16[8,32,640]{2,1,0:T(8,128)(2,1)S(1)} %get-tuple-element.19.refs_0_), channel_id=1, source_target_pairs={{0,4},{4,0},{1,5},{5,1},{2,6},{6,2},{3,7},{7,3},{8,12},{12,8},{9,1... | collective-permute-start | bytes 983048 | tf_op jit(solution)/shard_map/ppermute | solution.py:39
  41.7 21.4 %collective-permute-start.10 = (bf16[8,32,640]{2,1,0:T(8,128)(2,1)S(1)}, bf16[8,32,640]{2,1,0:T(8,128)(2,1)S(1)}, u32[]{:S(2)}, u32[]{:S(2)}) collective-permute-start(bf16[8,32,640]{2,1,0:T(8,128)(2,1)S(1)} %collective-permute-done.6.refs_3_), channel_id=1, source_target_pairs={{0,4},{4,0},{1,5},{5,1},{2,6},{6,2},{3,7},{7,3},{8,12},{12,8},{9,1... | collective-permute-start | bytes 983048 | tf_op jit(solution)/shard_map/ppermute | solution.py:39
  49.7 13.4 %collective-permute-start.9 = (bf16[8,32,640]{2,1,0:T(8,128)(2,1)S(1)}, bf16[8,32,640]{2,1,0:T(8,128)(2,1)S(1)}, u32[]{:S(2)}, u32[]{:S(2)}) collective-permute-start(bf16[8,32,640]{2,1,0:T(8,128)(2,1)S(1)} %collective-permute-done.5.refs_2_), channel_id=1, source_target_pairs={{0,4},{4,0},{1,5},{5,1},{2,6},{6,2},{3,7},{7,3},{8,12},{12,8},{9,1... | collective-permute-start | bytes 983048 | tf_op jit(solution)/shard_map/ppermute | solution.py:39
  52.9 10.3 %collective-permute-start.8 = (bf16[8,32,640]{2,1,0:T(8,128)(2,1)S(1)}, bf16[8,32,640]{2,1,0:T(8,128)(2,1)S(1)}, u32[]{:S(2)}, u32[]{:S(2)}) collective-permute-start(bf16[8,32,640]{2,1,0:T(8,128)(2,1)S(1)} %collective-permute-done.4.refs_1_), channel_id=1, source_target_pairs={{0,4},{4,0},{1,5},{5,1},{2,6},{6,2},{3,7},{7,3},{8,12},{12,8},{9,1... | collective-permute-start | bytes 983048 | tf_op jit(solution)/shard_map/ppermute | solution.py:39
  53.4 2.2 %copy-start = (bf16[16,1,1024,128]{3,2,1,0:T(8,128)(2,1)S(1)}, bf16[16,1,1024,128]{3,2,1,0:T(8,128)(2,1)}, u32[]{:S(2)}) copy-start(bf16[16,1,1024,128]{3,2,1,0:T(8,128)(2,1)} %k_ref.1) | copy-start | bytes 12582916
  55.6 2.2 %copy-start.1 = (bf16[16,1,1024,128]{3,2,1,0:T(8,128)(2,1)S(1)}, bf16[16,1,1024,128]{3,2,1,0:T(8,128)(2,1)}, u32[]{:S(2)}) copy-start(bf16[16,1,1024,128]{3,2,1,0:T(8,128)(2,1)} %v_ref.1) | copy-start | bytes 12582916
  63.1 34.5 %copy-start.18 = (bf16[2048]{0:T(1024)(128)(2,1)S(1)}, bf16[2048]{0:T(1024)(128)(2,1)}, u32[]{:S(2)}) copy-start(bf16[2048]{0:T(1024)(128)(2,1)} %param.31) | copy-start | bytes 12292
  63.1 36.1 %copy-start.8 = (bf16[512,128]{1,0:T(8,128)(2,1)S(1)}, bf16[512,128]{1,0:T(8,128)(2,1)}, u32[]{:S(2)}) copy-start(bf16[512,128]{1,0:T(8,128)(2,1)} %dg.1) | copy-start | bytes 393220
  63.1 36.1 %copy-start.9 = (bf16[512,128]{1,0:T(8,128)(2,1)S(1)}, bf16[512,128]{1,0:T(8,128)(2,1)}, u32[]{:S(2)}) copy-start(bf16[512,128]{1,0:T(8,128)(2,1)} %du.1) | copy-start | bytes 393220
  75.7 42.9 %copy-start.2 = (bf16[1,2048,256]{2,1,0:T(8,128)(2,1)S(1)}, bf16[1,2048,256]{2,1,0:T(8,128)(2,1)}, u32[]{:S(2)}) copy-start(bf16[1,2048,256]{2,1,0:T(8,128)(2,1)} %eg.1) | copy-start | bytes 3145732
  75.7 42.9 %copy-start.3 = (bf16[1,2048,256]{2,1,0:T(8,128)(2,1)S(1)}, bf16[1,2048,256]{2,1,0:T(8,128)(2,1)}, u32[]{:S(2)}) copy-start(bf16[1,2048,256]{2,1,0:T(8,128)(2,1)} %eu.1) | copy-start | bytes 3145732
  75.7 42.9 %copy-start.4 = (bf16[1,256,2048]{2,1,0:T(8,128)(2,1)S(1)}, bf16[1,256,2048]{2,1,0:T(8,128)(2,1)}, u32[]{:S(2)}) copy-start(bf16[1,256,2048]{2,1,0:T(8,128)(2,1)} %ed.1) | copy-start | bytes 3145732
  94.6 4.6 %collective-permute-start.11 = (bf16[32,16,512]{2,1,0:T(8,128)(2,1)S(1)}, bf16[32,16,512]{2,1,0:T(8,128)(2,1)S(1)}, u32[]{:S(2)}, u32[]{:S(2)}) collective-permute-start(bf16[32,16,512]{2,1,0:T(8,128)(2,1)S(1)} %all_to_all.36.mine), channel_id=1, source_target_pairs={{0,4},{4,0},{1,5},{5,1},{2,6},{6,2},{3,7},{7,3},{8,12},{12,8},{9,1... | collective-permute-start | bytes 1572872 | tf_op jit(solution)/shard_map/ppermute | solution.py:39
  100.7 31.7 %copy-start.5 = (bf16[128,512]{1,0:T(8,128)(2,1)S(1)}, bf16[128,512]{1,0:T(8,128)(2,1)}, u32[]{:S(2)}) copy-start(bf16[128,512]{1,0:T(8,128)(2,1)} %dd.3) | copy-start | bytes 393220
  132.8 4.2 %collective-permute-start.12 = (bf16[32,16,512]{2,1,0:T(8,128)(2,1)S(1)}, bf16[32,16,512]{2,1,0:T(8,128)(2,1)S(1)}, u32[]{:S(2)}, u32[]{:S(2)}) collective-permute-start(bf16[32,16,512]{2,1,0:T(8,128)(2,1)S(1)} %block_other.1), channel_id=1, source_target_pairs={{0,4},{4,0},{1,5},{5,1},{2,6},{6,2},{3,7},{7,3},{8,12},{12,8},{9,1... | collective-permute-start | bytes 1572872 | tf_op jit(solution)/shard_map/ppermute | solution.py:39
  137.9 21.0 %all-to-all-start.6 = ((bf16[32,16,512]{2,1,0:T(8,128)(2,1)}), bf16[32,16,512]{2,1,0:T(8,128)(2,1)S(1)}, u32[]{:S(2)}, u32[]{:S(2)}) async-start(bf16[32,16,512]{2,1,0:T(8,128)(2,1)} %add.7), calls=%async_computation.6 | async-start | bytes 1048576 | tf_op jit(solution)/shard_map/all_to_all | solution.py:35

commit v3 on v2

v3 whole, which is shorter than its diff:
```python
import functools
import jax
import jax.numpy as jnp
from jax import lax
from jax.experimental import pallas as pl
from jax.experimental.pallas import tpu as pltpu
from jax.sharding import Mesh
from jax.sharding import PartitionSpec as P

EP = ("z", "x", "c")
ZX = ("z", "x")

norm_eps = 1e-05
clamp_limit = 7.0
swish_alpha = 1.702
f32 = jnp.float32
bf16 = jnp.bfloat16
VM = pl.BlockSpec(memory_space=pltpu.VMEM)
SM = pl.BlockSpec(memory_space=pltpu.SMEM)

NX = 4


def rms_scale(values, gain):
    return values * lax.rsqrt(jnp.mean(values * values, axis=-1, keepdims=True) + norm_eps) * gain


def clamped_unit(gate_pre, up_pre):
    gate_c = jnp.minimum(gate_pre, clamp_limit)
    up_c = jnp.clip(up_pre, -clamp_limit, clamp_limit)
    return (up_c + 1.0) * gate_c * jax.nn.sigmoid(swish_alpha * gate_c)


def exchange(blocks, axes):
    return lax.all_to_all(blocks, axes, 0, 0, tiled=True)


def other_core(values):
    return lax.ppermute(values, "c", [(0, 1), (1, 0)])


def along_x(values, k):
    return lax.ppermute(values, "x", [(i, (i + k) % NX) for i in range(NX)])


def local(kernel, name, outs, args, scratch=(), smem=0, keep=True, pin=pltpu.VMEM):
    multi = isinstance(outs, (list, tuple))
    if keep:
        outs = jax.tree.map(lambda s: pltpu.VMEM(s.shape, s.dtype), outs)
    pins = pin if isinstance(pin, tuple) else (pin,) * (len(args) - smem)
    args = tuple(args[:smem]) + tuple(
        pltpu.with_memory_space_constraint(a, p) for a, p in zip(args[smem:], pins)
    )
    return pl.pallas_call(
        kernel,
        out_shape=outs,
        in_specs=[SM] * smem + [VM] * (len(args) - smem),
        out_specs=[VM] * len(outs) if multi else VM,
        scratch_shapes=list(scratch),
        compiler_params=pltpu.CompilerParams(vmem_limit_bytes=16 << 20),
        name=name,
    )(*args)


def sds(shape, dtype=bf16):
    return jax.ShapeDtypeStruct(tuple(shape), dtype)


def pick(parts, at):
    out = parts[0]
    for k in range(1, len(parts)):
        out = jnp.where(at == k, parts[k], out)
    return out


def prepare_kernel(nz, tok, gain, qw, kw, vw, owt, ids, rw, wcat, msg):
    qc, kc = qw.shape[1], kw.shape[1]
    proj = qc + 2 * kc
    wcat[:, :qc] = qw[...]
    wcat[:, qc : qc + kc] = kw[...]
    wcat[:, qc + kc : proj] = vw[...]
    normed = rms_scale(tok[...].astype(f32), gain[...]).astype(bf16)
    seqs = normed.shape[0]
    lane = lax.broadcasted_iota(jnp.int32, (seqs, 128), 1)
    row = lax.broadcasted_iota(jnp.int32, (seqs, seqs), 0)
    col = lax.broadcasted_iota(jnp.int32, (seqs, seqs), 1)
    hi = rw[...].astype(bf16).astype(f32)
    lo = rw[...] - hi
    idf = ids[...].astype(f32)
    top = idf.shape[0]
    meta = jnp.zeros((seqs, 128), f32)
    for j, values in enumerate((idf, hi, lo)):
        for k in range(top):
            down = jnp.sum(jnp.where(row == col, values[k : k + 1], 0.0), axis=1, keepdims=True)
            meta = jnp.where(lane == j * top + k, down, meta)
    meta = meta.astype(bf16)
    wcat[:seqs, proj:] = meta
    wcat[seqs:, proj:] = jnp.zeros((wcat.shape[0] - seqs, 128), bf16)
    heads = owt.shape[1]
    for z in range(nz):
        msg[z, :, :heads] = owt[...]
        msg[z, :seqs, heads:] = normed[:, z * 256 : z * 256 + 128]
        msg[z, seqs:, heads:] = normed[:, z * 256 + 128 : z * 256 + 256]


def project_kernel(at, got, w0, w1, w2, w3, wo, part, owm, w_s, f_s):
    x, c = at[1], at[2]
    nz, depth, wide = got.shape
    seqs = depth // 2
    proj = w_s.shape[1]
    table = jnp.zeros((seqs, 128), f32)
    for k, w in enumerate((w0, w1, w2, w3)):
        place = lax.rem(x + NX - k, NX) * 2
        w_s[pl.ds(pl.multiple_of((place + c) * depth, depth), depth)] = w[:, :proj]
        w_s[pl.ds(pl.multiple_of((place + 1 - c) * depth, depth), depth)] = wo[k, :, :proj]
        table += pltpu.roll(w[:seqs, proj:].astype(f32), k * 16, 1)
        table += pltpu.roll(wo[k, :seqs, proj:].astype(f32), (NX + k) * 16, 1)
    table = table.astype(bf16)
    for z in range(nz):
        f_s[z * seqs : (z + 1) * seqs, :128] = got[z, :seqs, wide - 128 :]
        f_s[z * seqs : (z + 1) * seqs, 128:] = got[z, seqs:, wide - 128 :]
        owm[z] = got[z, :, : wide - 128]
    out = jnp.dot(f_s[...], w_s[...], preferred_element_type=f32).astype(bf16)
    for z in range(nz):
        part[z, :, :proj] = out[z * seqs : (z + 1) * seqs]
        part[z, :, proj:] = table


def attention_kernel(
    block, lengths, bias, part, k_hbm, v_hbm, att, nk, nv, k_ref, v_ref, q_s, z_s, w_s, sems
):
    seqs, _, span, head_dim = k_ref.shape
    piece = 256
    steps = span // piece
    pairs = ((k_hbm, k_ref), (v_hbm, v_ref))

    def each_size(which, s, act):
        live = lax.div(lengths[s] + piece - 1, piece)
        for n in range(1, steps + 1):

            @pl.when(live == n)
            def _():
                place = (s, 0, pl.ds(0, n * piece))
                source, target = pairs[which]
                act(
                    pltpu.make_async_copy(source.at[place], target.at[place], sems.at[which, s]), n
                )

    def begin(copy, n):
        copy.start()

    @pl.loop(0, seqs)
    def _(s):
        each_size(0, s, begin)

    @pl.loop(0, seqs)
    def _(s):
        def clear(copy, n):
            copy.start()
            if n < steps:
                rest = (steps - n) * piece
                v_ref[s, 0, pl.ds(n * piece, rest)] = jnp.zeros((rest, head_dim), bf16)

        each_size(1, s, clear)

    heads = bias.shape[0]
    q_cols = heads * head_dim
    both = 2 * heads
    qkv = jnp.sum(part[:, :, : q_cols + 2 * head_dim].astype(f32), axis=0)
    nk[...] = qkv[:, q_cols : q_cols + head_dim].astype(bf16)
    nv[...] = qkv[:, q_cols + head_dim :].astype(bf16)
    for s in range(seqs):
        for h in range(heads):
            at_row = s * heads + h
            q_s[at_row : at_row + 1] = qkv[s : s + 1, h * head_dim : (h + 1) * head_dim]

    upper = lax.broadcasted_iota(jnp.int32, (both, 1), 0) < heads

    def wait(copy, n):
        copy.wait()

    @pl.loop(0, seqs // 2)
    def _(i):
        s = i * 2
        each_size(0, s, wait)
        each_size(0, s + 1, wait)
        here = pl.ds(pl.multiple_of(s * heads, both), both)
        q = q_s[here].astype(bf16)
        pair = [
            lax.dot_general(
                q, k_ref[s + j, 0], (((1,), (1,)), ((), ())), preferred_element_type=f32
            )
            for j in range(2)
        ]
        z_s[here] = jnp.where(upper, pair[0], pair[1])

    rows = block * heads
    row = lax.broadcasted_iota(jnp.int32, (rows, 1), 0)
    lane = lax.broadcasted_iota(jnp.int32, (rows, 128), 1)
    offset = jnp.zeros((rows, 1), f32)
    for h in range(heads):
        offset = jnp.where(row % heads == h, bias[h], offset)
    chunks = span // 128

    @pl.loop(0, seqs // block)
    def _(step):
        length = jnp.zeros((rows, 1), jnp.int32)
        for i in range(block):
            length = jnp.where(row // heads == i, lengths[step * block + i], length)
        here = pl.ds(pl.multiple_of(step * rows, rows), rows)
        after = jnp.zeros((rows, 1), f32)
        for c in range(chunks - 1, -1, -1):
            cols = slice(c * 128, (c + 1) * 128)
            z = z_s[here, cols] * head_dim ** (-0.5) + offset
            inside = lane + c * 128 < length
            tail = jnp.log1p(jnp.exp(-jnp.abs(z)))
            keep = jnp.where(inside, -jnp.maximum(z, 0.0) - tail, 0.0)
            total = keep
            shift = 1
            while shift < 128:
                moved = pltpu.roll(total, 128 - shift, 1)
                total = total + jnp.where(lane < 128 - shift, moved, 0.0)
                shift *= 2
            between = total - keep + after
            after = after + total[:, 0:1]
            power = jnp.exp(jnp.minimum(z, 0.0) - tail + between)
            w_s[here, cols] = jnp.where(inside, power, 0.0)

    @pl.loop(0, seqs // 2)
    def _(i):
        s = i * 2
        each_size(1, s, wait)
        each_size(1, s + 1, wait)
        here = pl.ds(pl.multiple_of(s * heads, both), both)
        w = w_s[here].astype(bf16)
        pair = [jnp.dot(w, v_ref[s + j, 0], preferred_element_type=f32) for j in range(2)]
        q_s[here] = jnp.where(upper, pair[0], pair[1])

    out = q_s[...].astype(bf16).astype(f32)
    for s in range(seqs):
        for h in range(heads):
            at_row = s * heads + h
            att[s : s + 1, h * head_dim : (h + 1) * head_dim] = out[at_row : at_row + 1].astype(
                bf16
            )


def attention(part, bias, keys, values, lengths):
    seqs, _, span, head_dim = keys.shape
    heads = bias.shape[0]
    outs = [sds((seqs, heads * head_dim)), sds((seqs, head_dim)), sds((seqs, head_dim))]
    hbm = pl.BlockSpec(memory_space=pltpu.HBM)
    pins = (pltpu.VMEM, pltpu.HBM, pltpu.HBM)
    args = [
        pltpu.with_memory_space_constraint(a, p) for a, p in zip((part, keys, values), pins)
    ]
    return pl.pallas_call(
        functools.partial(attention_kernel, 8),
        out_shape=outs,
        in_specs=[SM, SM, VM, hbm, hbm],
        out_specs=[VM] * 3,
        scratch_shapes=[pltpu.VMEM(keys.shape, bf16)] * 2
        + [pltpu.VMEM((seqs * heads, head_dim), f32)]
        + [pltpu.VMEM((seqs * heads, span), f32)] * 2
        + [pltpu.SemaphoreType.DMA((2, seqs))],
        compiler_params=pltpu.CompilerParams(vmem_limit_bytes=24 << 20),
        name="attention",
    )(*(pltpu.with_memory_space_constraint(a, pltpu.HBM) for a in (lengths, bias)), *args)


def mix_kernel(at, att, *refs):
    mine, others, msg, w_s = refs[:NX], refs[NX : 2 * NX], refs[2 * NX], refs[2 * NX + 1]
    x, c = at[1], at[2]
    nz, depth = mine[0].shape[:2]
    heads = att.shape[1]
    for k in range(NX):
        place = lax.rem(x + NX - k, NX) * 2
        for z in range(nz):
            base = z * NX * 2
            w_s[pl.ds(pl.multiple_of((base + place + c) * depth, depth), depth)] = mine[k][
                z, :, :heads
            ]
            w_s[pl.ds(pl.multiple_of((base + place + 1 - c) * depth, depth), depth)] = others[k][
                z, :, :heads
            ]
    out = lax.dot_general(
        att[...], w_s[...], (((1,), (1,)), ((), ())), preferred_element_type=f32
    ).astype(bf16)
    for t in range(msg.shape[0]):
        msg[t] = out


def slots_kernel(seqs, top, at, part, him, lom, m_s):
    x = at[1]
    nz, _, wide = part.shape
    half = nz * NX * seqs
    for z in range(nz):
        table = part[z, :, wide - 128 :].astype(f32)
        for r in range(2):
            for k in range(NX):
                place = lax.rem(x + NX - k, NX) * seqs
                start = pl.multiple_of(r * half + z * NX * seqs + place, seqs)
                shift = (r * NX + k) * 16
                m_s[pl.ds(start, seqs)] = pltpu.roll(table, (128 - shift) % 128, 1)
    expert = (at[0] * NX + x) * 2 + at[2]
    m = m_s[...]
    rows = m.shape[0]
    lane = lax.broadcasted_iota(jnp.int32, (rows, 128), 1)
    row = lax.broadcasted_iota(jnp.int32, (rows, 128), 0)
    hit = jnp.where((m == expert.astype(f32)) & (lane < top), 1.0, 0.0)
    hi = jnp.sum(hit * pltpu.roll(m, 128 - top, 1), axis=1, keepdims=True)
    lo = jnp.sum(hit * pltpu.roll(m, 128 - 2 * top, 1), axis=1, keepdims=True)
    own = jnp.broadcast_to(jnp.sum(hit, axis=1, keepdims=True), (rows, 128))
    upto = own
    shift = 1
    while shift < seqs:
        upto = upto + jnp.where(row % seqs >= shift, pltpu.roll(upto, shift, 0), 0.0)
        shift *= 2
    slot = (row // seqs) * 2 + (upto - own).astype(jnp.int32)
    here = jnp.where((lane == slot) & (own > 0.5), 1.0, 0.0)
    him[...] = (here * hi).astype(bf16)
    lom[...] = (here * lo).astype(bf16)


def norm_kernel(at, got, tok, gain, ids, msg, res):
    t = at[3]
    mixed = jnp.sum(got[...].astype(f32), axis=0).astype(bf16).astype(f32)
    resid = tok[...].astype(f32) + mixed
    normed = rms_scale(resid, gain[...]).astype(bf16)
    seqs, width = resid.shape
    nb, share, _ = msg.shape
    parts = got.shape[0]
    wide = width // parts
    own = share // 2
    res[...] = pick([resid[:, k * wide : (k + 1) * wide] for k in range(parts)], t)
    top = ids.shape[0]
    experts = 2 * nb
    expert = lax.broadcasted_iota(jnp.int32, (experts, seqs), 0)
    hit = jnp.zeros((experts, seqs), f32)
    for k in range(top):
        hit = jnp.where(ids[k : k + 1] == expert, 1.0, hit)
    lane = lax.broadcasted_iota(jnp.int32, (seqs, seqs), 1)
    before = jnp.where(lax.broadcasted_iota(jnp.int32, (seqs, seqs), 0) < lane, 1.0, 0.0)
    rank = jnp.dot(hit, before, preferred_element_type=f32)
    quarter = lax.broadcasted_iota(jnp.int32, (own, seqs), 0) + t * own
    quarter = jnp.where(quarter == lax.broadcasted_iota(jnp.int32, (own, seqs), 1), 1.0, 0.0)
    first = jnp.where(rank < 0.5, hit, 0.0)
    second = jnp.where(rank > 0.5, hit, 0.0)
    choose = []
    for b in range(nb):
        choose.append(quarter)
        for c in range(2):
            e = 2 * b + c
            choose.append(first[e : e + 1])
            choose.append(second[e : e + 1])
    choose = jnp.concatenate(choose, axis=0).astype(bf16)
    rows = jnp.dot(choose, normed, preferred_element_type=f32).astype(bf16)
    msg[...] = rows.reshape(msg.shape)


def expert_kernel(
    at, mine, other, w0, w1, w2, w3, bg, eg, eu, ed, msg, w_s, d_s, x_s, r_s, sems
):
    t = at[3]
    nb, share, width = mine.shape
    own = share // 2
    nt, slots, _ = msg.shape
    wide = width // nt
    cols = w0.shape[1] // 2
    copies = [pltpu.make_async_copy(ed.at[0], d_s, sems.at[nt])]
    for k, w in enumerate((w0, w1, w2, w3)):
        place = pl.multiple_of(lax.rem(t + nt - k, nt) * wide, wide)
        copies.append(pltpu.make_async_copy(w, w_s.at[pl.ds(place, wide)], sems.at[k]))
    for copy in copies:
        copy.start()
    core = at[2]
    half = nb * own
    for h, part in enumerate((mine, other)):
        block = part[...].astype(f32)
        routed = jnp.where(core == 0, block[:, own : own + 2], block[:, own + 2 :])
        r_s[h * 2 * nb : (h + 1) * 2 * nb] = routed.reshape(2 * nb, width).astype(bf16)
        x_s[h * half : (h + 1) * half] = block[:, :own].reshape(half, width).astype(bf16)
    rows = r_s[...]
    gate_pre = jnp.dot(rows, eg[0], preferred_element_type=f32)
    up_pre = jnp.dot(rows, eu[0], preferred_element_type=f32)
    act = clamped_unit(gate_pre, up_pre).astype(bf16)
    copies[0].wait()
    out = jnp.dot(act, d_s[...], preferred_element_type=f32).astype(bf16)
    for q in range(nt):
        msg[q, :, :wide] = out[:, q * wide : (q + 1) * wide]
    x = x_s[...]
    gate = jnp.broadcast_to(bg[...].astype(f32), (8, width)).astype(bf16)
    branch = lax.dot_general(x, gate, (((1,), (1,)), ((), ())), preferred_element_type=f32)
    for copy in copies[1:]:
        copy.wait()
    pre = jnp.dot(x, w_s[...], preferred_element_type=f32)
    hidden = jax.nn.silu(pre[:, :cols]) * pre[:, cols:] * jax.nn.sigmoid(branch[:, 0:1])
    hidden = hidden.astype(bf16)
    for q in range(nt):
        msg[q, :, wide : wide + cols] = hidden[:slots]
        msg[q, :, wide + cols :] = hidden[slots:]


def block_kernel(which, got, dd, him, lom, out, h_s):
    nt, slots, wide = got.shape
    cols = dd.shape[0]
    wide = wide - 2 * cols
    rows = jnp.sum(got[:, :, :wide].astype(f32), axis=0).astype(bf16)
    nb, seqs, _ = out.shape
    half = nb * seqs
    own = seqs // nt
    start = wide + which * cols
    for q in range(nt):
        part = got[q, :, start : start + cols].astype(f32)
        h_s[:, q * own : (q + 1) * own] = part.reshape(nb, own, cols)
    left = jnp.concatenate(
        [
            h_s[...].reshape(half, cols).astype(bf16),
            him[which * half : (which + 1) * half],
            lom[which * half : (which + 1) * half],
        ],
        axis=1,
    )
    right = jnp.concatenate([dd[...], rows, rows], axis=0)
    full = jnp.dot(left, right, preferred_element_type=f32)
    out[...] = full.astype(out.dtype).reshape(out.shape)


def add_kernel(a, b, out):
    out[...] = (a[...] + b[...].astype(f32)).astype(bf16)


def final_kernel(got, res, out):
    out[...] = (jnp.sum(got[...].astype(f32), axis=0) + res[...]).astype(bf16)


def body(
    tokens,
    attn_gain,
    query_weight,
    key_weight,
    value_weight,
    break_bias,
    cache_keys,
    cache_values,
    lengths,
    out_weight,
    ffn_gain,
    branch_gate,
    dense_gate,
    dense_up,
    dense_down,
    route_ids,
    route_weights,
    expert_gate,
    expert_up,
    expert_down,
):
    nz, nt = lax.axis_size("z"), lax.axis_size("tp")
    nzx = nz * NX
    seqs, width = tokens.shape
    top = route_ids.shape[1]
    slice_width = width // nt
    all_rows = 2 * nzx * seqs
    slots = 2 * nzx * 2
    depth = query_weight.shape[0]
    heads = out_weight.shape[0]
    proj = query_weight.shape[1] + 2 * key_weight.shape[1]
    at = jnp.stack([lax.axis_index(a) for a in ("z", "x", "c", "tp")]).astype(jnp.int32)

    wcat, msg = local(
        functools.partial(prepare_kernel, nz),
        "prepare",
        [sds((depth, proj + 128)), sds((nz, depth, heads + 128))],
        (
            tokens,
            attn_gain[None],
            query_weight,
            key_weight,
            value_weight,
            out_weight.T,
            route_ids.T,
            route_weights.T,
        ),
        pin=pltpu.HBM,
    )
    with jax.named_scope("over_z"):
        got = exchange(msg, "z")
    with jax.named_scope("weights_x"):
        w_x = [wcat] + [along_x(wcat, k) for k in range(1, NX)]
    w_other = other_core(jnp.stack(w_x))
    part, owm = local(
        project_kernel,
        "project",
        [sds((nz, seqs, proj + 128)), sds((nz, depth, heads))],
        (at, got, *w_x, w_other),
        [pltpu.VMEM((2 * NX * depth, proj), bf16), pltpu.VMEM((nz * seqs, 2 * NX * depth), bf16)],
        smem=1,
    )
    with jax.named_scope("partial_z"):
        part = exchange(part, "z")
    with jax.named_scope("mix_x"):
        ow = [owm] + [along_x(owm, k) for k in range(1, NX)]
    ow_other = [other_core(piece) for piece in ow]

    attended, new_keys, new_values = attention(
        part, break_bias, cache_keys, cache_values, lengths
    )

    msg = local(
        mix_kernel,
        "mix",
        sds((nt, seqs, width)),
        (at, attended, *ow, *ow_other),
        [pltpu.VMEM((width, heads), bf16)],
        smem=1,
    )
    mixed = exchange(msg, "tp")
    him, lom = local(
        functools.partial(slots_kernel, seqs, top),
        "slots",
        [sds((all_rows, slots))] * 2,
        (at, part),
        [pltpu.VMEM((all_rows, 128), f32)],
        smem=1,
    )
    own = seqs // nt
    cols = dense_gate.shape[1]
    msg, resid = local(
        norm_kernel,
        "norm",
        [sds((nzx, 2 * own, width)), sds((seqs, slice_width), f32)],
        (at, mixed, tokens, ffn_gain[None], route_ids.T),
        smem=1,
    )
    with jax.named_scope("rows_zx"):
        mine = exchange(msg, ZX)
    with jax.named_scope("dense_tp"):
        gu = jnp.concatenate([dense_gate, dense_up], axis=1)
        gu = [gu] + [
            lax.ppermute(gu, "tp", [(i, (i + k) % nt) for i in range(nt)]) for k in range(1, nt)
        ]
    mine, *gu = lax.optimization_barrier((mine, *gu))
    other, him, lom = lax.optimization_barrier((other_core(mine), him, lom))
    hbm = pl.BlockSpec(memory_space=pltpu.HBM)
    places = [pltpu.VMEM] * 2 + [pltpu.HBM] * nt + [pltpu.VMEM] * 3 + [pltpu.HBM]
    operands = (mine, other, *gu, branch_gate[None], expert_gate, expert_up, expert_down)
    msg = pl.pallas_call(
        expert_kernel,
        out_shape=pltpu.VMEM((nt, slots, slice_width + 2 * cols), bf16),
        in_specs=[SM] + [hbm if p == pltpu.HBM else VM for p in places],
        out_specs=VM,
        scratch_shapes=[
            pltpu.VMEM((width, 2 * cols), bf16),
            pltpu.VMEM(expert_down.shape[1:], bf16),
            pltpu.VMEM((2 * nzx * own, width), bf16),
            pltpu.VMEM((slots, width), bf16),
            pltpu.SemaphoreType.DMA((nt + 1,)),
        ],
        compiler_params=pltpu.CompilerParams(vmem_limit_bytes=16 << 20),
        name="expert",
    )(at, *(pltpu.with_memory_space_constraint(a, p) for a, p in zip(operands, places)))
    got = exchange(msg, "tp")
    parts = (got, dense_down, him, lom)
    shape = (nzx, seqs, slice_width)
    hold = [pltpu.VMEM((nzx, seqs, cols), f32)]
    sent = local(functools.partial(block_kernel, 1), "block_other", sds(shape), parts, hold)
    arrived = other_core(sent)
    kept = local(functools.partial(block_kernel, 0), "block_mine", sds(shape, f32), parts, hold)
    block = local(add_kernel, "add", sds(shape), (kept, arrived))
    got = exchange(block, ZX)
    out = local(final_kernel, "final", sds((seqs, slice_width)), (got, resid), keep=False)
    return out, new_keys, new_values


def solution(mesh):
    shape = (mesh.shape["ep"] // (2 * NX), NX, 2, mesh.shape["tp"])
    split = Mesh(mesh.devices.reshape(shape), ("z", "x", "c", "tp"))
    return jax.shard_map(
        body,
        mesh=split,
        in_specs=(
            P(EP, None),
            P(),
            P(EP, "tp"),
            P(EP, "tp"),
            P(EP, "tp"),
            P("tp"),
            P(EP, "tp", None, None),
            P(EP, "tp", None, None),
            P(EP),
            P("tp", EP),
            P(),
            P(),
            P("tp", EP),
            P("tp", EP),
            P(EP, "tp"),
            P(EP, None),
            P(EP, None),
            P(EP, None, "tp"),
            P(EP, None, "tp"),
            P(EP, "tp", None),
        ),
        out_specs=(P(EP, "tp"), P(EP, "tp"), P(EP, "tp")),
        check_vma=False,
    )
```

time: 161 us -> 145 us (0.901)
  blocking collectives: 60.3 us -> 45.6 us
  local copies, waits for them, and re-layouts: 11.6 us -> 1.73 us
  Pallas kernels: 15.9 us -> 21.7 us
  waiting for transfers between devices: 28 us -> 31 us
    all_to_all x4 -> x3, blocking collectives: 60.3 us -> 45.6 us  [exchange(): return lax.all_to_all(blocks, axes, 0, 0, tiled=True)]
    ppermute x0 -> x3, waiting for transfers between devices: none -> 12.2 us  [body(): lax.ppermute(gu, 'tp', [(i, (i + k) % nt) for i in range(nt)])]
    unnamed x42 -> x23, local copies, waits for them, and re-layouts: 11.6 us -> 0.78 us
    pallas_call x0 -> x2, Pallas kernels: none -> 10.6 us  [the longest x1 7.27 us: attention(): pl.pallas_call(functools.partial(attention_kernel, 8), out_shape=outs, in...]
    all_to_all x3, waiting for transfers between devices: 18.7 us -> 9.75 us  [exchange(): return lax.all_to_all(blocks, axes, 0, 0, tiled=True)]
    pallas_call x12 -> x9, Pallas kernels: 15.9 us -> 11.1 us  [local(): pl.pallas_call(kernel, out_shape=outs, in_specs=[SM] * smem + [VM] * (len...]
    ppermute x7, starting transfers between devices: 18.6 us -> 15.8 us  [other_core(): return lax.ppermute(values, 'c', [(0, 1), (1, 0)])]
    ppermute x0 -> x3, starting transfers between devices: none -> 2.15 us  [body(): lax.ppermute(gu, 'tp', [(i, (i + k) % nt) for i in range(nt)])]
  transfers between devices with their start and end apart: 16 -> 19, of which waited for: 8 -> 12; matrix products, arithmetic and copies ran while one was open for 1% -> 1% of each run, Pallas kernels for 5% -> 7%
where the time goes in v3:
time: 145 us
  blocking collectives  45.6 us (31%)
  starting transfers between devices  44 us (30%)
  waiting for transfers between devices  31 us (21%)
  Pallas kernels  21.7 us (15%)
  local copies, waits for them, and re-layouts  1.73 us (1%)
    all_to_all x3, blocking collectives, exchange(): return lax.all_to_all(blocks, axes, 0, 0, tiled=True)  45.6 us
    all_to_all x3, starting transfers between devices, exchange(): return lax.all_to_all(blocks, axes, 0, 0, tiled=True)  18.8 us
    ppermute x7, starting transfers between devices, other_core(): return lax.ppermute(values, 'c', [(0, 1), (1, 0)])  15.8 us
    ppermute x3, waiting for transfers between devices, body(): lax.ppermute(gu, 'tp', [(i, (i + k) % nt) for i in range(nt)])  12.2 us
    pallas_call x9, Pallas kernels, local(): pl.pallas_call(kernel, out_shape=outs, in_specs=[SM] * smem + [VM] * (len...  11.1 us
    all_to_all x3, waiting for transfers between devices, exchange(): return lax.all_to_all(blocks, axes, 0, 0, tiled=True)  9.75 us
    pallas_call x1, Pallas kernels, attention(): pl.pallas_call(functools.partial(attention_kernel, 8), out_shape=outs, in...  7.27 us
    ppermute x6, starting transfers between devices, along_x(): return lax.ppermute(values, 'x', [(i, (i + k) % NX) for i in range(NX)])  7.21 us
  transfers between devices with their start and end apart: 19, of which 12 were waited for; matrix products, arithmetic and copies ran while one was open for 1% of the time, Pallas kernels for 7%

profile of v3, /device:TPU:1, one launch (start us, length us, event | category | flops | bytes accessed | tf_op | source)
XLA Modules:
  0.0 144.9 jit_solution(12696414882734305202)
XLA Ops:
  0.6 1.8 %prepare.1 = (bf16[32,896]{1,0:T(8,128)(2,1)S(1)}, bf16[8,32,640]{2,1,0:T(8,128)(2,1)}) custom-call(bf16[16,2048]{1,0:T(8,128)(2,1)} %tok.3, f32[1,2048]{1,0:T(1,128)} %bitcast.21, bf16[32,512]{1,0:T(8,128)(2,1)} %qw.1, bf16[32,128]{1,0:T(8,128)(2,1)} %kw.1, bf16[32,128]{1,0:T(8,128)(2,1)} %vw.1, bf16[32,512]{1,0:T(8,128)(2,1)} %bitcast.20, ...), custom_call_target="tpu_custom_call" | custom-call | tf_op jit(solution)/shard_map/prepare/pallas_call | solution.py:54
  2.4 9.0 %all-to-all-start = ((bf16[8,32,640]{2,1,0:T(8,128)(2,1)}), bf16[8,32,640]{2,1,0:T(8,128)(2,1)S(1)}, u32[]{:S(2)}, u32[]{:S(2)}) async-start(bf16[8,32,640]{2,1,0:T(8,128)(2,1)} %get-tuple-element.22), calls=%async_computation | async-start | bytes 655360 | tf_op jit(solution)/shard_map/over_z/all_to_all | solution.py:35
  11.4 2.5 %collective-permute-start.2 = (bf16[32,896]{1,0:T(8,128)(2,1)S(1)}, bf16[32,896]{1,0:T(8,128)(2,1)S(1)}, u32[]{:S(2)}, u32[]{:S(2)}) collective-permute-start(bf16[32,896]{1,0:T(8,128)(2,1)S(1)} %get-tuple-element.23.w0), channel_id=1, source_target_pairs={{0,24},{8,0},{16,8},{24,16},{1,25},{9,1},{17,9},{25,17},{2,26},{10... | collective-permute-start | bytes 172040 | tf_op jit(solution)/shard_map/weights_x/ppermute | solution.py:43
  13.9 0.5 collective-permute-start.1
  14.4 0.6 collective-permute-start
  15.0 0.1 collective-permute-done.2.w3
  15.1 3.3 %collective-permute-done.1.w2 = bf16[32,896]{1,0:T(8,128)(2,1)S(1)} collective-permute-done((bf16[32,896]{1,0:T(8,128)(2,1)S(1)}, bf16[32,896]{1,0:T(8,128)(2,1)S(1)}, u32[]{:S(2)}, u32[]{:S(2)}) %collective-permute-start.1) | collective-permute-done | bytes 57376 | tf_op jit(solution)/shard_map/weights_x/ppermute | solution.py:43
  18.4 0.9 collective-permute-done.w1
  19.4 2.2 %collective-permute-start.3 = (bf16[4,32,896]{2,1,0:T(8,128)(2,1)S(1)}, bf16[4,32,896]{2,1,0:T(8,128)(2,1)S(1)}, u32[]{:S(2)}, u32[]{:S(2)}) collective-permute-start(bf16[4,32,896]{2,1,0:T(8,128)(2,1)S(1)} %pad_maximum_fusion), channel_id=1, source_target_pairs={{0,4},{4,0},{1,5},{5,1},{2,6},{6,2},{3,7},{7,3},{8,12},{12,8},{9,1... | collective-permute-start | bytes 688136 | tf_op jit(solution)/shard_map/ppermute | solution.py:39
  21.5 0.1 pad_add_fusion.at
  21.6 1.0 collective-permute-done.3.wo
  22.6 0.8 all-to-all-done.got
  23.5 1.5 %project.1 = (bf16[8,16,896]{2,1,0:T(8,128)(2,1)}, bf16[8,32,512]{2,1,0:T(8,128)(2,1)S(1)}) custom-call(s32[4]{0:T(128)S(1)} %pad_add_fusion.at, bf16[8,32,640]{2,1,0:T(8,128)(2,1)S(1)} %all-to-all-done.got, bf16[32,896]{1,0:T(8,128)(2,1)S(1)} %get-tuple-element.23.w0, bf16[32,896]{1,0:T(8,128)(2,1)S(1)} %collective-permute-done.w1, ...), custom_call_target="tpu_custom_call" | custom-call | tf_op jit(solution)/shard_map/project/pallas_call | solution.py:54
  25.0 2.5 %collective-permute-start.6 = (bf16[8,32,512]{2,1,0:T(8,128)(2,1)S(1)}, bf16[8,32,512]{2,1,0:T(8,128)(2,1)S(1)}, u32[]{:S(2)}, u32[]{:S(2)}) collective-permute-start(bf16[8,32,512]{2,1,0:T(8,128)(2,1)S(1)} %get-tuple-element.26.refs_0_), channel_id=1, source_target_pairs={{0,24},{8,0},{16,8},{24,16},{1,25},{9,1},{17,9},{25,17},{2,26},{10... | collective-permute-start | bytes 786440 | tf_op jit(solution)/shard_map/mix_x/ppermute | solution.py:43
  27.5 0.5 collective-permute-start.5
  28.0 0.6 collective-permute-start.4
  28.6 4.5 %all-to-all-start.1 = ((bf16[8,16,896]{2,1,0:T(8,128)(2,1)}), bf16[8,16,896]{2,1,0:T(8,128)(2,1)S(1)}, u32[]{:S(2)}, u32[]{:S(2)}) async-start(bf16[8,16,896]{2,1,0:T(8,128)(2,1)} %get-tuple-element.24), calls=%async_computation.1 | async-start | bytes 458752 | tf_op jit(solution)/shard_map/partial_z/all_to_all | solution.py:35
  33.1 0.0 copy-start.4
  33.1 2.0 %collective-permute-start.7 = (bf16[8,32,512]{2,1,0:T(8,128)(2,1)S(1)}, bf16[8,32,512]{2,1,0:T(8,128)(2,1)}, u32[]{:S(2)}, u32[]{:S(2)}) collective-permute-start(bf16[8,32,512]{2,1,0:T(8,128)(2,1)S(1)} %get-tuple-element.26.refs_0_), channel_id=1, source_target_pairs={{0,4},{4,0},{1,5},{5,1},{2,6},{6,2},{3,7},{7,3},{8,12},{12,8},{9,1... | collective-permute-start | bytes 786440 | tf_op jit(solution)/shard_map/ppermute | solution.py:39
  35.1 4.5 %collective-permute-start.10 = (bf16[8,32,512]{2,1,0:T(8,128)(2,1)S(1)}, bf16[8,32,512]{2,1,0:T(8,128)(2,1)}, u32[]{:S(2)}, u32[]{:S(2)}) collective-permute-start(bf16[8,32,512]{2,1,0:T(8,128)(2,1)S(1)} %collective-permute-done.6.refs_3_), channel_id=1, source_target_pairs={{0,4},{4,0},{1,5},{5,1},{2,6},{6,2},{3,7},{7,3},{8,12},{12,8},{9,1... | collective-permute-start | bytes 786440 | tf_op jit(solution)/shard_map/ppermute | solution.py:39
  39.6 0.9 collective-permute-start.9
  40.5 2.1 %collective-permute-done.4.refs_1_ = bf16[8,32,512]{2,1,0:T(8,128)(2,1)} collective-permute-done((bf16[8,32,512]{2,1,0:T(8,128)(2,1)S(1)}, bf16[8,32,512]{2,1,0:T(8,128)(2,1)}, u32[]{:S(2)}, u32[]{:S(2)}) %collective-permute-start.4) | collective-permute-done | bytes 262176 | tf_op jit(solution)/shard_map/mix_x/ppermute | solution.py:43
  42.7 0.7 collective-permute-start.8
  43.4 7.3 %attention.1 = (bf16[16,512]{1,0:T(8,128)(2,1)S(1)}, bf16[16,128]{1,0:T(8,128)(2,1)}, bf16[16,128]{1,0:T(8,128)(2,1)}) custom-call(s32[16]{0:T(128)} %lengths.1, f32[4]{0:T(128)} %bias.1, bf16[8,16,896]{2,1,0:T(8,128)(2,1)S(1)} %all-to-all-done.1.part, bf16[16,1,1024,128]{3,2,1,0:T(8,128)(2,1)} %k_hbm.1, bf16[16,1,1024,128]{3,2,1,0:T(8,128)(2,1)} %v_hbm.1), custom_call_target="tpu_custom_call" | custom-call | tf_op jit(solution)/shard_map/attention/pallas_call | solution.py:257
  50.8 2.2 %mix.1 = bf16[4,16,2048]{2,1,0:T(8,128)(2,1)S(1)} custom-call(s32[4]{0:T(128)S(1)} %pad_add_fusion.at, bf16[16,512]{1,0:T(8,128)(2,1)S(1)} %get-tuple-element.25.att, bf16[8,32,512]{2,1,0:T(8,128)(2,1)S(1)} %get-tuple-element.26.refs_0_, bf16[8,32,512]{2,1,0:T(8,128)(2,1)} %collective-permute-done.4.refs_1_, ...), custom_call_target="tpu_custom_call" | custom-call | tf_op jit(solution)/shard_map/mix/pallas_call | solution.py:54
  53.0 9.5 %all_to_all.30.got = bf16[4,16,2048]{2,1,0:T(8,128)(2,1)S(1)} all-to-all(bf16[4,16,2048]{2,1,0:T(8,128)(2,1)S(1)} %mix.1), channel_id=1, replica_groups=mesh['z'=8,'x'=4,'c'=2,'tp'=4] {'tp'}, dimensions={0} | all-to-all | bytes 524288 | tf_op jit(solution)/shard_map/all_to_all | solution.py:35
  62.5 2.1 %norm.1 = (bf16[32,8,2048]{2,1,0:T(8,128)(2,1)}, f32[16,512]{1,0:T(8,128)S(1)}) custom-call(s32[4]{0:T(128)S(1)} %pad_add_fusion.at, bf16[4,16,2048]{2,1,0:T(8,128)(2,1)S(1)} %all_to_all.30.got, bf16[16,2048]{1,0:T(8,128)(2,1)S(1)} %copy-done.3, f32[1,2048]{1,0:T(1,128)S(1)} %bitcast.19, s32[4,16]{1,0:T(4,128)S(1)} %bitcast.18), custom_call_target="tpu_custom_call" | custom-call | tf_op jit(solution)/shard_map/norm/pallas_call | solution.py:54
  64.6 5.3 %all-to-all-start.3 = ((bf16[32,8,2048]{2,1,0:T(8,128)(2,1)}), bf16[32,8,2048]{2,1,0:T(8,128)(2,1)S(1)}, u32[]{:S(2)}, u32[]{:S(2)}) async-start(bf16[32,8,2048]{2,1,0:T(8,128)(2,1)} %get-tuple-element.27), calls=%async_computation.3 | async-start | bytes 2097152 | tf_op jit(solution)/shard_map/rows_zx/all_to_all | solution.py:35
  70.0 0.9 constant_dynamic-update-slice_fusion.w0
  70.9 1.0 collective-permute-start.13
  71.9 1.2 collective-permute-start.12
  73.1 3.1 %collective-permute-done.13.w3 = bf16[512,256]{1,0:T(8,128)(2,1)S(1)} collective-permute-done((bf16[512,256]{1,0:T(8,128)(2,1)S(1)}, bf16[512,256]{1,0:T(8,128)(2,1)S(1)}, u32[]{:S(2)}, u32[]{:S(2)}) %collective-permute-start.13) | collective-permute-done | bytes 262176 | tf_op jit(solution)/shard_map/dense_tp/ppermute | solution.py:541
  76.2 2.7 %collective-permute-done.12.w2 = bf16[512,256]{1,0:T(8,128)(2,1)S(1)} collective-permute-done((bf16[512,256]{1,0:T(8,128)(2,1)S(1)}, bf16[512,256]{1,0:T(8,128)(2,1)S(1)}, u32[]{:S(2)}, u32[]{:S(2)}) %collective-permute-start.12) | collective-permute-done | bytes 262176 | tf_op jit(solution)/shard_map/dense_tp/ppermute | solution.py:541
  78.9 0.7 copy-done.8
  79.6 6.3 %collective-permute-done.11.w1 = bf16[512,256]{1,0:T(8,128)(2,1)} collective-permute-done((bf16[512,256]{1,0:T(8,128)(2,1)S(1)}, bf16[512,256]{1,0:T(8,128)(2,1)}, u32[]{:S(2)}, u32[]{:S(2)}) %collective-permute-start.11) | collective-permute-done | bytes 262176 | tf_op jit(solution)/shard_map/dense_tp/ppermute | solution.py:541
  86.0 8.9 %all-to-all-done.3.mine = bf16[32,8,2048]{2,1,0:T(8,128)(2,1)S(1)} async-done(((bf16[32,8,2048]{2,1,0:T(8,128)(2,1)}), bf16[32,8,2048]{2,1,0:T(8,128)(2,1)S(1)}, u32[]{:S(2)}, u32[]{:S(2)}) %all-to-all-start.3) | async-done | bytes 1048608 | tf_op jit(solution)/shard_map/rows_zx/all_to_all | solution.py:35
  94.9 4.2 %collective-permute-start.14 = (bf16[32,8,2048]{2,1,0:T(8,128)(2,1)S(1)}, bf16[32,8,2048]{2,1,0:T(8,128)(2,1)S(1)}, u32[]{:S(2)}, u32[]{:S(2)}) collective-permute-start(bf16[32,8,2048]{2,1,0:T(8,128)(2,1)S(1)} %all-to-all-done.3.mine), channel_id=1, source_target_pairs={{0,4},{4,0},{1,5},{5,1},{2,6},{6,2},{3,7},{7,3},{8,12},{12,8},{9,1... | collective-permute-start | bytes 3145736 | tf_op jit(solution)/shard_map/ppermute | solution.py:39
  99.1 1.8 %slots.1 = (bf16[1024,128]{1,0:T(8,128)(2,1)S(1)}, bf16[1024,128]{1,0:T(8,128)(2,1)S(1)}) custom-call(s32[4]{0:T(128)S(1)} %pad_add_fusion.at, bf16[8,16,896]{2,1,0:T(8,128)(2,1)S(1)} %all-to-all-done.1.part), custom_call_target="tpu_custom_call" | custom-call | tf_op jit(solution)/shard_map/slots/pallas_call | solution.py:54
  100.8 0.5 collective-permute-done.14.other
  101.3 3.4 %expert.1 = bf16[4,128,768]{2,1,0:T(8,128)(2,1)S(1)} custom-call(s32[4]{0:T(128)S(1)} %pad_add_fusion.at, bf16[32,8,2048]{2,1,0:T(8,128)(2,1)S(1)} %all-to-all-done.3.mine, bf16[32,8,2048]{2,1,0:T(8,128)(2,1)S(1)} %collective-permute-done.14.other, bf16[512,256]{1,0:T(8,128)(2,1)} %copy-done.6, bf16[512,256]{1,0:T(8,128)(2,1)} %collective-permute-done.11.w1, ...), custom_call_target="tpu_custom_call" | custom-call | tf_op jit(solution)/shard_map/expert/pallas_call | solution.py:548
  104.7 14.4 %all_to_all.31.got = bf16[4,128,768]{2,1,0:T(8,128)(2,1)S(1)} all-to-all(bf16[4,128,768]{2,1,0:T(8,128)(2,1)S(1)} %expert.1), channel_id=1, replica_groups=mesh['z'=8,'x'=4,'c'=2,'tp'=4] {'tp'}, dimensions={0} | all-to-all | bytes 1572864 | tf_op jit(solution)/shard_map/all_to_all | solution.py:35
  119.1 0.5 block_other.1
  119.6 1.3 collective-permute-start.15
  120.9 0.5 block_mine.1.a
  121.4 1.1 collective-permute-done.15.b
  122.5 0.1 add.7
  122.6 21.6 %all_to_all.32.got = bf16[32,16,512]{2,1,0:T(8,128)(2,1)S(1)} all-to-all(bf16[32,16,512]{2,1,0:T(8,128)(2,1)S(1)} %add.7), channel_id=1, replica_groups=mesh['z'=8,'x'=4,'c'=2,'tp'=4] {'z','x'}, dimensions={0} | all-to-all | bytes 1048576 | tf_op jit(solution)/shard_map/all_to_all | solution.py:35
  144.2 0.7 final.1
  (31 shorter events, 0.1 us)
Async XLA Ops:
  2.4 21.1 %all-to-all-start = ((bf16[8,32,640]{2,1,0:T(8,128)(2,1)}), bf16[8,32,640]{2,1,0:T(8,128)(2,1)S(1)}, u32[]{:S(2)}, u32[]{:S(2)}) async-start(bf16[8,32,640]{2,1,0:T(8,128)(2,1)} %get-tuple-element.22), calls=%async_computation | async-start | bytes 655360 | tf_op jit(solution)/shard_map/over_z/all_to_all | solution.py:35
  11.4 3.7 %collective-permute-start.2 = (bf16[32,896]{1,0:T(8,128)(2,1)S(1)}, bf16[32,896]{1,0:T(8,128)(2,1)S(1)}, u32[]{:S(2)}, u32[]{:S(2)}) collective-permute-start(bf16[32,896]{1,0:T(8,128)(2,1)S(1)} %get-tuple-element.23.w0), channel_id=1, source_target_pairs={{0,24},{8,0},{16,8},{24,16},{1,25},{9,1},{17,9},{25,17},{2,26},{10... | collective-permute-start | bytes 172040 | tf_op jit(solution)/shard_map/weights_x/ppermute | solution.py:43
  13.9 4.6 %collective-permute-start.1 = (bf16[32,896]{1,0:T(8,128)(2,1)S(1)}, bf16[32,896]{1,0:T(8,128)(2,1)S(1)}, u32[]{:S(2)}, u32[]{:S(2)}) collective-permute-start(bf16[32,896]{1,0:T(8,128)(2,1)S(1)} %get-tuple-element.23.w0), channel_id=1, source_target_pairs={{0,16},{8,24},{16,0},{24,8},{1,17},{9,25},{17,1},{25,9},{2,18},{10... | collective-permute-start | bytes 172040 | tf_op jit(solution)/shard_map/weights_x/ppermute | solution.py:43
  14.4 4.9 %collective-permute-start = (bf16[32,896]{1,0:T(8,128)(2,1)S(1)}, bf16[32,896]{1,0:T(8,128)(2,1)S(1)}, u32[]{:S(2)}, u32[]{:S(2)}) collective-permute-start(bf16[32,896]{1,0:T(8,128)(2,1)S(1)} %get-tuple-element.23.w0), channel_id=1, source_target_pairs={{0,8},{8,16},{16,24},{24,0},{1,9},{9,17},{17,25},{25,1},{2,10},{10... | collective-permute-start | bytes 172040 | tf_op jit(solution)/shard_map/weights_x/ppermute | solution.py:43
  19.4 3.3 %collective-permute-start.3 = (bf16[4,32,896]{2,1,0:T(8,128)(2,1)S(1)}, bf16[4,32,896]{2,1,0:T(8,128)(2,1)S(1)}, u32[]{:S(2)}, u32[]{:S(2)}) collective-permute-start(bf16[4,32,896]{2,1,0:T(8,128)(2,1)S(1)} %pad_maximum_fusion), channel_id=1, source_target_pairs={{0,4},{4,0},{1,5},{5,1},{2,6},{6,2},{3,7},{7,3},{8,12},{12,8},{9,1... | collective-permute-start | bytes 688136 | tf_op jit(solution)/shard_map/ppermute | solution.py:39
  25.0 10.1 %collective-permute-start.6 = (bf16[8,32,512]{2,1,0:T(8,128)(2,1)S(1)}, bf16[8,32,512]{2,1,0:T(8,128)(2,1)S(1)}, u32[]{:S(2)}, u32[]{:S(2)}) collective-permute-start(bf16[8,32,512]{2,1,0:T(8,128)(2,1)S(1)} %get-tuple-element.26.refs_0_), channel_id=1, source_target_pairs={{0,24},{8,0},{16,8},{24,16},{1,25},{9,1},{17,9},{25,17},{2,26},{10... | collective-permute-start | bytes 786440 | tf_op jit(solution)/shard_map/mix_x/ppermute | solution.py:43
  27.5 12.2 %collective-permute-start.5 = (bf16[8,32,512]{2,1,0:T(8,128)(2,1)S(1)}, bf16[8,32,512]{2,1,0:T(8,128)(2,1)S(1)}, u32[]{:S(2)}, u32[]{:S(2)}) collective-permute-start(bf16[8,32,512]{2,1,0:T(8,128)(2,1)S(1)} %get-tuple-element.26.refs_0_), channel_id=1, source_target_pairs={{0,16},{8,24},{16,0},{24,8},{1,17},{9,25},{17,1},{25,9},{2,18},{10... | collective-permute-start | bytes 786440 | tf_op jit(solution)/shard_map/mix_x/ppermute | solution.py:43
  28.0 14.7 %collective-permute-start.4 = (bf16[8,32,512]{2,1,0:T(8,128)(2,1)S(1)}, bf16[8,32,512]{2,1,0:T(8,128)(2,1)}, u32[]{:S(2)}, u32[]{:S(2)}) collective-permute-start(bf16[8,32,512]{2,1,0:T(8,128)(2,1)S(1)} %get-tuple-element.26.refs_0_), channel_id=1, source_target_pairs={{0,8},{8,16},{16,24},{24,0},{1,9},{9,17},{17,25},{25,1},{2,10},{10... | collective-permute-start | bytes 786440 | tf_op jit(solution)/shard_map/mix_x/ppermute | solution.py:43
  28.6 14.8 %all-to-all-start.1 = ((bf16[8,16,896]{2,1,0:T(8,128)(2,1)}), bf16[8,16,896]{2,1,0:T(8,128)(2,1)S(1)}, u32[]{:S(2)}, u32[]{:S(2)}) async-start(bf16[8,16,896]{2,1,0:T(8,128)(2,1)} %get-tuple-element.24), calls=%async_computation.1 | async-start | bytes 458752 | tf_op jit(solution)/shard_map/partial_z/all_to_all | solution.py:35
  33.1 29.5 %copy-start.3 = (bf16[16,2048]{1,0:T(8,128)(2,1)S(1)}, bf16[16,2048]{1,0:T(8,128)(2,1)}, u32[]{:S(2)}) copy-start(bf16[16,2048]{1,0:T(8,128)(2,1)} %tok.3) | copy-start | bytes 196612
  33.1 29.5 %copy-start.4 = (s32[16,4]{0,1:T(4,128)S(1)}, s32[16,4]{0,1:T(4,128)}, u32[]{:S(2)}) copy-start(s32[16,4]{0,1:T(4,128)} %param.35) | copy-start | bytes 772
  33.1 29.4 %copy-start.5 = (f32[2048]{0:T(1024)S(1)}, f32[2048]{0:T(1024)}, u32[]{:S(2)}) copy-start(f32[2048]{0:T(1024)} %param.30) | copy-start | bytes 24580
  33.1 17.6 %collective-permute-start.7 = (bf16[8,32,512]{2,1,0:T(8,128)(2,1)S(1)}, bf16[8,32,512]{2,1,0:T(8,128)(2,1)}, u32[]{:S(2)}, u32[]{:S(2)}) collective-permute-start(bf16[8,32,512]{2,1,0:T(8,128)(2,1)S(1)} %get-tuple-element.26.refs_0_), channel_id=1, source_target_pairs={{0,4},{4,0},{1,5},{5,1},{2,6},{6,2},{3,7},{7,3},{8,12},{12,8},{9,1... | collective-permute-start | bytes 786440 | tf_op jit(solution)/shard_map/ppermute | solution.py:39
  35.1 15.6 %collective-permute-start.10 = (bf16[8,32,512]{2,1,0:T(8,128)(2,1)S(1)}, bf16[8,32,512]{2,1,0:T(8,128)(2,1)}, u32[]{:S(2)}, u32[]{:S(2)}) collective-permute-start(bf16[8,32,512]{2,1,0:T(8,128)(2,1)S(1)} %collective-permute-done.6.refs_3_), channel_id=1, source_target_pairs={{0,4},{4,0},{1,5},{5,1},{2,6},{6,2},{3,7},{7,3},{8,12},{12,8},{9,1... | collective-permute-start | bytes 786440 | tf_op jit(solution)/shard_map/ppermute | solution.py:39
  39.6 11.1 %collective-permute-start.9 = (bf16[8,32,512]{2,1,0:T(8,128)(2,1)S(1)}, bf16[8,32,512]{2,1,0:T(8,128)(2,1)}, u32[]{:S(2)}, u32[]{:S(2)}) collective-permute-start(bf16[8,32,512]{2,1,0:T(8,128)(2,1)S(1)} %collective-permute-done.5.refs_2_), channel_id=1, source_target_pairs={{0,4},{4,0},{1,5},{5,1},{2,6},{6,2},{3,7},{7,3},{8,12},{12,8},{9,1... | collective-permute-start | bytes 786440 | tf_op jit(solution)/shard_map/ppermute | solution.py:39
  42.7 8.1 %collective-permute-start.8 = (bf16[8,32,512]{2,1,0:T(8,128)(2,1)}, bf16[8,32,512]{2,1,0:T(8,128)(2,1)}, u32[]{:S(2)}, u32[]{:S(2)}) collective-permute-start(bf16[8,32,512]{2,1,0:T(8,128)(2,1)} %collective-permute-done.4.refs_1_), channel_id=1, source_target_pairs={{0,4},{4,0},{1,5},{5,1},{2,6},{6,2},{3,7},{7,3},{8,12},{12,8},{9,1... | collective-permute-start | bytes 786440 | tf_op jit(solution)/shard_map/ppermute | solution.py:39
  50.7 19.2 %copy-start.9 = (bf16[512,128]{1,0:T(8,128)(2,1)S(1)}, bf16[512,128]{1,0:T(8,128)(2,1)}, u32[]{:S(2)}) copy-start(bf16[512,128]{1,0:T(8,128)(2,1)} %param.32) | copy-start | bytes 393220
  50.7 48.3 %copy-start.10 = (bf16[2048]{0:T(1024)(128)(2,1)S(1)}, bf16[2048]{0:T(1024)(128)(2,1)}, u32[]{:S(2)}) copy-start(bf16[2048]{0:T(1024)(128)(2,1)} %param.31) | copy-start | bytes 12292
  50.7 50.6 %copy-start = (bf16[1,2048,256]{2,1,0:T(8,128)(2,1)S(1)}, bf16[1,2048,256]{2,1,0:T(8,128)(2,1)}, u32[]{:S(2)}) copy-start(bf16[1,2048,256]{2,1,0:T(8,128)(2,1)} %eg.1) | copy-start | bytes 3145732
  50.7 50.6 %copy-start.1 = (bf16[1,2048,256]{2,1,0:T(8,128)(2,1)S(1)}, bf16[1,2048,256]{2,1,0:T(8,128)(2,1)}, u32[]{:S(2)}) copy-start(bf16[1,2048,256]{2,1,0:T(8,128)(2,1)} %eu.1) | copy-start | bytes 3145732
  64.6 30.2 %all-to-all-start.3 = ((bf16[32,8,2048]{2,1,0:T(8,128)(2,1)}), bf16[32,8,2048]{2,1,0:T(8,128)(2,1)S(1)}, u32[]{:S(2)}, u32[]{:S(2)}) async-start(bf16[32,8,2048]{2,1,0:T(8,128)(2,1)} %get-tuple-element.27), calls=%async_computation.3 | async-start | bytes 2097152 | tf_op jit(solution)/shard_map/rows_zx/all_to_all | solution.py:35
  70.9 8.0 %copy-start.6 = (bf16[512,256]{1,0:T(8,128)(2,1)}, bf16[512,256]{1,0:T(8,128)(2,1)S(1)}, u32[]{:S(2)}) copy-start(bf16[512,256]{1,0:T(8,128)(2,1)S(1)} %constant_dynamic-update-slice_fusion.w0) | copy-start | bytes 786436
  70.9 5.3 %collective-permute-start.13 = (bf16[512,256]{1,0:T(8,128)(2,1)S(1)}, bf16[512,256]{1,0:T(8,128)(2,1)S(1)}, u32[]{:S(2)}, u32[]{:S(2)}) collective-permute-start(bf16[512,256]{1,0:T(8,128)(2,1)S(1)} %constant_dynamic-update-slice_fusion.w0), channel_id=1, source_target_pairs={{0,3},{1,0},{2,1},{3,2},{4,7},{5,4},{6,5},{7,6},{8,11},{9,8},{10,9... | collective-permute-start | bytes 786440 | tf_op jit(solution)/shard_map/dense_tp/ppermute | solution.py:541
  71.9 7.0 %collective-permute-start.12 = (bf16[512,256]{1,0:T(8,128)(2,1)S(1)}, bf16[512,256]{1,0:T(8,128)(2,1)S(1)}, u32[]{:S(2)}, u32[]{:S(2)}) collective-permute-start(bf16[512,256]{1,0:T(8,128)(2,1)S(1)} %constant_dynamic-update-slice_fusion.w0), channel_id=1, source_target_pairs={{0,2},{1,3},{2,0},{3,1},{4,6},{5,7},{6,4},{7,5},{8,10},{9,11},{10,... | collective-permute-start | bytes 786440 | tf_op jit(solution)/shard_map/dense_tp/ppermute | solution.py:541
  73.1 12.9 %collective-permute-start.11 = (bf16[512,256]{1,0:T(8,128)(2,1)S(1)}, bf16[512,256]{1,0:T(8,128)(2,1)}, u32[]{:S(2)}, u32[]{:S(2)}) collective-permute-start(bf16[512,256]{1,0:T(8,128)(2,1)S(1)} %constant_dynamic-update-slice_fusion.w0), channel_id=1, source_target_pairs={{0,1},{1,2},{2,3},{3,0},{4,5},{5,6},{6,7},{7,4},{8,9},{9,10},{10,1... | collective-permute-start | bytes 786440 | tf_op jit(solution)/shard_map/dense_tp/ppermute | solution.py:541
  76.2 2.7 %copy-start.7 = (bf16[512,256]{1,0:T(8,128)(2,1)}, bf16[512,256]{1,0:T(8,128)(2,1)S(1)}, u32[]{:S(2)}) copy-start(bf16[512,256]{1,0:T(8,128)(2,1)S(1)} %collective-permute-done.13.w3) | copy-start | bytes 786436
  78.9 0.7 copy-start.8
  94.9 6.5 %collective-permute-start.14 = (bf16[32,8,2048]{2,1,0:T(8,128)(2,1)S(1)}, bf16[32,8,2048]{2,1,0:T(8,128)(2,1)S(1)}, u32[]{:S(2)}, u32[]{:S(2)}) collective-permute-start(bf16[32,8,2048]{2,1,0:T(8,128)(2,1)S(1)} %all-to-all-done.3.mine), channel_id=1, source_target_pairs={{0,4},{4,0},{1,5},{5,1},{2,6},{6,2},{3,7},{7,3},{8,12},{12,8},{9,1... | collective-permute-start | bytes 3145736 | tf_op jit(solution)/shard_map/ppermute | solution.py:39
  101.3 17.8 %copy-start.2 = (bf16[128,512]{1,0:T(8,128)(2,1)S(1)}, bf16[128,512]{1,0:T(8,128)(2,1)}, u32[]{:S(2)}) copy-start(bf16[128,512]{1,0:T(8,128)(2,1)} %dd.3) | copy-start | bytes 393220
  119.6 2.9 %collective-permute-start.15 = (bf16[32,16,512]{2,1,0:T(8,128)(2,1)S(1)}, bf16[32,16,512]{2,1,0:T(8,128)(2,1)S(1)}, u32[]{:S(2)}, u32[]{:S(2)}) collective-permute-start(bf16[32,16,512]{2,1,0:T(8,128)(2,1)S(1)} %block_other.1), channel_id=1, source_target_pairs={{0,4},{4,0},{1,5},{5,1},{2,6},{6,2},{3,7},{7,3},{8,12},{12,8},{9,1... | collective-permute-start | bytes 1572872 | tf_op jit(solution)/shard_map/ppermute | solution.py:39

commit v4 on v3

--- a/solution.py
+++ b/solution.py
@@ -293,33 +293,37 @@
 def slots_kernel(seqs, top, at, part, him, lom, m_s):
     x = at[1]
     nz, _, wide = part.shape
-    half = nz * NX * seqs
     for z in range(nz):
         table = part[z, :, wide - 128 :].astype(f32)
-        for r in range(2):
-            for k in range(NX):
-                place = lax.rem(x + NX - k, NX) * seqs
-                start = pl.multiple_of(r * half + z * NX * seqs + place, seqs)
-                shift = (r * NX + k) * 16
-                m_s[pl.ds(start, seqs)] = pltpu.roll(table, (128 - shift) % 128, 1)
-    expert = (at[0] * NX + x) * 2 + at[2]
+        for k in range(NX):
+            place = lax.rem(x + NX - k, NX) * seqs
+            start = pl.multiple_of(z * NX * seqs + place, seqs)
+            m_s[pl.ds(start, seqs)] = pltpu.roll(table, (128 - k * 16) % 128, 1)
     m = m_s[...]
     rows = m.shape[0]
     lane = lax.broadcasted_iota(jnp.int32, (rows, 128), 1)
     row = lax.broadcasted_iota(jnp.int32, (rows, 128), 0)
-    hit = jnp.where((m == expert.astype(f32)) & (lane < top), 1.0, 0.0)
-    hi = jnp.sum(hit * pltpu.roll(m, 128 - top, 1), axis=1, keepdims=True)
-    lo = jnp.sum(hit * pltpu.roll(m, 128 - 2 * top, 1), axis=1, keepdims=True)
-    own = jnp.broadcast_to(jnp.sum(hit, axis=1, keepdims=True), (rows, 128))
-    upto = own
-    shift = 1
-    while shift < seqs:
-        upto = upto + jnp.where(row % seqs >= shift, pltpu.roll(upto, shift, 0), 0.0)
-        shift *= 2
-    slot = (row // seqs) * 2 + (upto - own).astype(jnp.int32)
-    here = jnp.where((lane == slot) & (own > 0.5), 1.0, 0.0)
-    him[...] = (here * hi).astype(bf16)
-    lom[...] = (here * lo).astype(bf16)
+    highs = pltpu.roll(m, 128 - top, 1)
+    lows = pltpu.roll(m, 128 - 2 * top, 1)
+    him_all = jnp.zeros((rows, 128), f32)
+    lom_all = jnp.zeros((rows, 128), f32)
+    for c in range(2):
+        expert = (at[0] * NX + x) * 2 + c
+        hit = jnp.where((m == expert.astype(f32)) & (lane < top), 1.0, 0.0)
+        hi = jnp.sum(hit * highs, axis=1, keepdims=True)
+        lo = jnp.sum(hit * lows, axis=1, keepdims=True)
+        own = jnp.broadcast_to(jnp.sum(hit, axis=1, keepdims=True), (rows, 128))
+        upto = own
+        shift = 1
+        while shift < seqs:
+            upto = upto + jnp.where(row % seqs >= shift, pltpu.roll(upto, shift, 0), 0.0)
+            shift *= 2
+        slot = c * 64 + (row // seqs) * 2 + (upto - own).astype(jnp.int32)
+        here = jnp.where((lane == slot) & (own > 0.5), 1.0, 0.0)
+        him_all += here * hi
+        lom_all += here * lo
+    him[...] = him_all.astype(bf16)
+    lom[...] = lom_all.astype(bf16)
 
 
 def norm_kernel(at, got, tok, gain, ids, msg, res):
@@ -364,7 +368,8 @@
     t = at[3]
     nb, share, width = mine.shape
     own = share // 2
-    nt, slots, _ = msg.shape
+    nt = msg.shape[0] // 2
+    slots = 2 * msg.shape[1]
     wide = width // nt
     cols = w0.shape[1] // 2
     copies = [pltpu.make_async_copy(ed.at[0], d_s, sems.at[nt])]
@@ -386,8 +391,11 @@
     act = clamped_unit(gate_pre, up_pre).astype(bf16)
     copies[0].wait()
     out = jnp.dot(act, d_s[...], preferred_element_type=f32).astype(bf16)
-    for q in range(nt):
-        msg[q, :, :wide] = out[:, q * wide : (q + 1) * wide]
+    some = slots // 2
+    for r in range(2):
+        to = lax.rem(core + r, 2) * nt
+        for q in range(nt):
+            msg[to + q, :, :wide] = out[r * some : (r + 1) * some, q * wide : (q + 1) * wide]
     x = x_s[...]
     gate = jnp.broadcast_to(bg[...].astype(f32), (8, width)).astype(bf16)
     branch = lax.dot_general(x, gate, (((1,), (1,)), ((), ())), preferred_element_type=f32)
@@ -396,38 +404,47 @@
     pre = jnp.dot(x, w_s[...], preferred_element_type=f32)
     hidden = jax.nn.silu(pre[:, :cols]) * pre[:, cols:] * jax.nn.sigmoid(branch[:, 0:1])
     hidden = hidden.astype(bf16)
-    for q in range(nt):
-        msg[q, :, wide : wide + cols] = hidden[:slots]
-        msg[q, :, wide + cols :] = hidden[slots:]
-
-
-def block_kernel(which, got, dd, him, lom, out, h_s):
-    nt, slots, wide = got.shape
+    for r in range(2):
+        to = lax.rem(core + r, 2) * nt
+        for q in range(nt):
+            msg[to + q, :, wide : wide + cols] = hidden[r * half : r * half + some]
+            msg[to + q, :, wide + cols :] = hidden[r * half + some : (r + 1) * half]
+
+
+def block_kernel(at, got, dd, dd_other, him, lom, out, h_s):
+    nt = got.shape[0] // 2
+    some = got.shape[1]
     cols = dd.shape[0]
-    wide = wide - 2 * cols
-    rows = jnp.sum(got[:, :, :wide].astype(f32), axis=0).astype(bf16)
+    wide = dd.shape[1]
     nb, seqs, _ = out.shape
-    half = nb * seqs
     own = seqs // nt
-    start = wide + which * cols
-    for q in range(nt):
-        part = got[q, :, start : start + cols].astype(f32)
-        h_s[:, q * own : (q + 1) * own] = part.reshape(nb, own, cols)
-    left = jnp.concatenate(
+    rows = []
+    for c in range(2):
+        part = jnp.sum(got[c * nt : (c + 1) * nt, :, :wide].astype(f32), axis=0)
+        rows.append(part.astype(bf16))
+        for q in range(nt):
+            for f in range(2):
+                start = wide + f * cols
+                part = got[c * nt + q, :, start : start + cols].astype(f32)
+                h_s[
+                    f * nb // 2 : (f + 1) * nb // 2,
+                    q * own : (q + 1) * own,
+                    c * cols : (c + 1) * cols,
+                ] = part.reshape(nb // 2, own, cols)
+    hidden = h_s[...].reshape(nb * seqs, 2 * cols).astype(bf16)
+    left = jnp.concatenate([hidden, him[...], lom[...]], axis=1)
+    zero = at[2] == 0
+    right = jnp.concatenate(
         [
-            h_s[...].reshape(half, cols).astype(bf16),
-            him[which * half : (which + 1) * half],
-            lom[which * half : (which + 1) * half],
+            jnp.where(zero, dd[...], dd_other[...]),
+            jnp.where(zero, dd_other[...], dd[...]),
+            *rows,
+            *rows,
         ],
-        axis=1,
-    )
-    right = jnp.concatenate([dd[...], rows, rows], axis=0)
+        axis=0,
+    )
     full = jnp.dot(left, right, preferred_element_type=f32)
-    out[...] = full.astype(out.dtype).reshape(out.shape)
-
-
-def add_kernel(a, b, out):
-    out[...] = (a[...] + b[...].astype(f32)).astype(bf16)
+    out[...] = full.astype(bf16).reshape(out.shape)
 
 
 def final_kernel(got, res, out):
@@ -519,9 +536,9 @@
     him, lom = local(
         functools.partial(slots_kernel, seqs, top),
         "slots",
-        [sds((all_rows, slots))] * 2,
+        [sds((all_rows // 2, slots))] * 2,
         (at, part),
-        [pltpu.VMEM((all_rows, 128), f32)],
+        [pltpu.VMEM((all_rows // 2, 128), f32)],
         smem=1,
     )
     own = seqs // nt
@@ -540,14 +557,15 @@
         gu = [gu] + [
             lax.ppermute(gu, "tp", [(i, (i + k) % nt) for i in range(nt)]) for k in range(1, nt)
         ]
-    mine, *gu = lax.optimization_barrier((mine, *gu))
+        down = other_core(dense_down)
+    mine, down, *gu = lax.optimization_barrier((mine, down, *gu))
     other, him, lom = lax.optimization_barrier((other_core(mine), him, lom))
     hbm = pl.BlockSpec(memory_space=pltpu.HBM)
     places = [pltpu.VMEM] * 2 + [pltpu.HBM] * nt + [pltpu.VMEM] * 3 + [pltpu.HBM]
     operands = (mine, other, *gu, branch_gate[None], expert_gate, expert_up, expert_down)
     msg = pl.pallas_call(
         expert_kernel,
-        out_shape=pltpu.VMEM((nt, slots, slice_width + 2 * cols), bf16),
+        out_shape=pltpu.VMEM((2 * nt, slots // 2, slice_width + 2 * cols), bf16),
         in_specs=[SM] + [hbm if p == pltpu.HBM else VM for p in places],
         out_specs=VM,
         scratch_shapes=[
@@ -560,14 +578,15 @@
         compiler_params=pltpu.CompilerParams(vmem_limit_bytes=16 << 20),
         name="expert",
     )(at, *(pltpu.with_memory_space_constraint(a, p) for a, p in zip(operands, places)))
-    got = exchange(msg, "tp")
-    parts = (got, dense_down, him, lom)
-    shape = (nzx, seqs, slice_width)
-    hold = [pltpu.VMEM((nzx, seqs, cols), f32)]
-    sent = local(functools.partial(block_kernel, 1), "block_other", sds(shape), parts, hold)
-    arrived = other_core(sent)
-    kept = local(functools.partial(block_kernel, 0), "block_mine", sds(shape, f32), parts, hold)
-    block = local(add_kernel, "add", sds(shape), (kept, arrived))
+    got = exchange(msg, ("c", "tp"))
+    block = local(
+        block_kernel,
+        "block",
+        sds((nzx, seqs, slice_width)),
+        (at, got, dense_down, down, him, lom),
+        [pltpu.VMEM((nzx, seqs, 2 * cols), f32)],
+        smem=1,
+    )
     got = exchange(block, ZX)
     out = local(final_kernel, "final", sds((seqs, slice_width)), (got, resid), keep=False)
     return out, new_keys, new_values

time: 145 us -> 143 us (0.986)
  waiting for transfers between devices: 31 us -> 24.7 us
  starting transfers between devices: 44 us -> 46.1 us
  local copies, waits for them, and re-layouts: 1.73 us -> 3.65 us
    ppermute x3, waiting for transfers between devices: 12.2 us -> 6.42 us  [body(): lax.ppermute(gu, 'tp', [(i, (i + k) % nt) for i in range(nt)])]
    ppermute x7, starting transfers between devices: 15.8 us -> 18.1 us  [other_core(): return lax.ppermute(values, 'c', [(0, 1), (1, 0)])]
    unnamed x23 -> x25, local copies, waits for them, and re-layouts: 0.78 us -> 2.7 us
    pallas_call x9 -> x7, Pallas kernels: 11.1 us -> 10.8 us  [local(): pl.pallas_call(kernel, out_shape=outs, in_specs=[SM] * smem + [VM] * (len...]
  transfers between devices with their start and end apart: 19 -> 19, of which waited for: 12 -> 11; matrix products, arithmetic and copies ran while one was open for 1% -> 1% of each run, Pallas kernels for 7% -> 6%
where the time goes in v4:
time: 143 us
  starting transfers between devices  46.1 us (32%)
  blocking collectives  46 us (32%)
  waiting for transfers between devices  24.7 us (17%)
  Pallas kernels  21.4 us (15%)
  local copies, waits for them, and re-layouts  3.65 us (3%)
    all_to_all x3, blocking collectives, exchange(): return lax.all_to_all(blocks, axes, 0, 0, tiled=True)  46 us
    all_to_all x3, starting transfers between devices, exchange(): return lax.all_to_all(blocks, axes, 0, 0, tiled=True)  18.6 us
    ppermute x7, starting transfers between devices, other_core(): return lax.ppermute(values, 'c', [(0, 1), (1, 0)])  18.1 us
    pallas_call x7, Pallas kernels, local(): pl.pallas_call(kernel, out_shape=outs, in_specs=[SM] * smem + [VM] * (len...  10.8 us
    all_to_all x3, waiting for transfers between devices, exchange(): return lax.all_to_all(blocks, axes, 0, 0, tiled=True)  9 us
    pallas_call x1, Pallas kernels, attention(): pl.pallas_call(functools.partial(attention_kernel, 8), out_shape=outs, in...  7.29 us
    ppermute x6, starting transfers between devices, along_x(): return lax.ppermute(values, 'x', [(i, (i + k) % NX) for i in range(NX)])  7.21 us
    ppermute x6, waiting for transfers between devices, along_x(): return lax.ppermute(values, 'x', [(i, (i + k) % NX) for i in range(NX)])  6.46 us
  transfers between devices with their start and end apart: 19, of which 11 were waited for; matrix products, arithmetic and copies ran while one was open for 1% of the time, Pallas kernels for 6%

profile of v4, /device:TPU:1, one launch (start us, length us, event | category | flops | bytes accessed | tf_op | source)
XLA Modules:
  0.0 142.8 jit_solution(6336517727854517831)
XLA Ops:
  0.6 1.8 %prepare.1 = (bf16[32,896]{1,0:T(8,128)(2,1)S(1)}, bf16[8,32,640]{2,1,0:T(8,128)(2,1)}) custom-call(bf16[16,2048]{1,0:T(8,128)(2,1)} %tok.3, f32[1,2048]{1,0:T(1,128)} %bitcast.21, bf16[32,512]{1,0:T(8,128)(2,1)} %qw.1, bf16[32,128]{1,0:T(8,128)(2,1)} %kw.1, bf16[32,128]{1,0:T(8,128)(2,1)} %vw.1, bf16[32,512]{1,0:T(8,128)(2,1)} %bitcast.20, ...), custom_call_target="tpu_custom_call" | custom-call | tf_op jit(solution)/shard_map/prepare/pallas_call | solution.py:54
  2.4 9.0 %all-to-all-start = ((bf16[8,32,640]{2,1,0:T(8,128)(2,1)}), bf16[8,32,640]{2,1,0:T(8,128)(2,1)S(1)}, u32[]{:S(2)}, u32[]{:S(2)}) async-start(bf16[8,32,640]{2,1,0:T(8,128)(2,1)} %get-tuple-element.23), calls=%async_computation | async-start | bytes 655360 | tf_op jit(solution)/shard_map/over_z/all_to_all | solution.py:35
  11.4 2.5 %collective-permute-start.2 = (bf16[32,896]{1,0:T(8,128)(2,1)S(1)}, bf16[32,896]{1,0:T(8,128)(2,1)S(1)}, u32[]{:S(2)}, u32[]{:S(2)}) collective-permute-start(bf16[32,896]{1,0:T(8,128)(2,1)S(1)} %get-tuple-element.24.w0), channel_id=1, source_target_pairs={{0,24},{8,0},{16,8},{24,16},{1,25},{9,1},{17,9},{25,17},{2,26},{10... | collective-permute-start | bytes 172040 | tf_op jit(solution)/shard_map/weights_x/ppermute | solution.py:43
  13.9 0.5 collective-permute-start.1
  14.4 0.6 collective-permute-start
  15.0 0.1 collective-permute-done.2.w3
  15.1 3.3 %collective-permute-done.1.w2 = bf16[32,896]{1,0:T(8,128)(2,1)S(1)} collective-permute-done((bf16[32,896]{1,0:T(8,128)(2,1)S(1)}, bf16[32,896]{1,0:T(8,128)(2,1)S(1)}, u32[]{:S(2)}, u32[]{:S(2)}) %collective-permute-start.1) | collective-permute-done | bytes 57376 | tf_op jit(solution)/shard_map/weights_x/ppermute | solution.py:43
  18.4 0.9 collective-permute-done.w1
  19.3 2.2 %collective-permute-start.3 = (bf16[4,32,896]{2,1,0:T(8,128)(2,1)S(1)}, bf16[4,32,896]{2,1,0:T(8,128)(2,1)S(1)}, u32[]{:S(2)}, u32[]{:S(2)}) collective-permute-start(bf16[4,32,896]{2,1,0:T(8,128)(2,1)S(1)} %pad_maximum_fusion), channel_id=1, source_target_pairs={{0,4},{4,0},{1,5},{5,1},{2,6},{6,2},{3,7},{7,3},{8,12},{12,8},{9,1... | collective-permute-start | bytes 688136 | tf_op jit(solution)/shard_map/ppermute | solution.py:39
  21.5 0.1 pad_add_fusion.at
  21.6 1.0 collective-permute-done.3.wo
  22.6 0.8 all-to-all-done.got
  23.5 1.5 %project.1 = (bf16[8,16,896]{2,1,0:T(8,128)(2,1)}, bf16[8,32,512]{2,1,0:T(8,128)(2,1)S(1)}) custom-call(s32[4]{0:T(128)S(1)} %pad_add_fusion.at, bf16[8,32,640]{2,1,0:T(8,128)(2,1)S(1)} %all-to-all-done.got, bf16[32,896]{1,0:T(8,128)(2,1)S(1)} %get-tuple-element.24.w0, bf16[32,896]{1,0:T(8,128)(2,1)S(1)} %collective-permute-done.w1, ...), custom_call_target="tpu_custom_call" | custom-call | tf_op jit(solution)/shard_map/project/pallas_call | solution.py:54
  25.0 2.5 %collective-permute-start.6 = (bf16[8,32,512]{2,1,0:T(8,128)(2,1)S(1)}, bf16[8,32,512]{2,1,0:T(8,128)(2,1)S(1)}, u32[]{:S(2)}, u32[]{:S(2)}) collective-permute-start(bf16[8,32,512]{2,1,0:T(8,128)(2,1)S(1)} %get-tuple-element.27.refs_0_), channel_id=1, source_target_pairs={{0,24},{8,0},{16,8},{24,16},{1,25},{9,1},{17,9},{25,17},{2,26},{10... | collective-permute-start | bytes 786440 | tf_op jit(solution)/shard_map/mix_x/ppermute | solution.py:43
  27.5 0.5 collective-permute-start.5
  28.0 0.6 collective-permute-start.4
  28.6 4.5 %all-to-all-start.1 = ((bf16[8,16,896]{2,1,0:T(8,128)(2,1)}), bf16[8,16,896]{2,1,0:T(8,128)(2,1)S(1)}, u32[]{:S(2)}, u32[]{:S(2)}) async-start(bf16[8,16,896]{2,1,0:T(8,128)(2,1)} %get-tuple-element.25), calls=%async_computation.1 | async-start | bytes 458752 | tf_op jit(solution)/shard_map/partial_z/all_to_all | solution.py:35
  33.1 0.0 copy-start.6
  33.1 2.0 %collective-permute-start.7 = (bf16[8,32,512]{2,1,0:T(8,128)(2,1)S(1)}, bf16[8,32,512]{2,1,0:T(8,128)(2,1)}, u32[]{:S(2)}, u32[]{:S(2)}) collective-permute-start(bf16[8,32,512]{2,1,0:T(8,128)(2,1)S(1)} %get-tuple-element.27.refs_0_), channel_id=1, source_target_pairs={{0,4},{4,0},{1,5},{5,1},{2,6},{6,2},{3,7},{7,3},{8,12},{12,8},{9,1... | collective-permute-start | bytes 786440 | tf_op jit(solution)/shard_map/ppermute | solution.py:39
  35.1 4.5 %collective-permute-start.10 = (bf16[8,32,512]{2,1,0:T(8,128)(2,1)S(1)}, bf16[8,32,512]{2,1,0:T(8,128)(2,1)}, u32[]{:S(2)}, u32[]{:S(2)}) collective-permute-start(bf16[8,32,512]{2,1,0:T(8,128)(2,1)S(1)} %collective-permute-done.6.refs_3_), channel_id=1, source_target_pairs={{0,4},{4,0},{1,5},{5,1},{2,6},{6,2},{3,7},{7,3},{8,12},{12,8},{9,1... | collective-permute-start | bytes 786440 | tf_op jit(solution)/shard_map/ppermute | solution.py:39
  39.6 0.9 collective-permute-start.9
  40.5 2.1 %collective-permute-done.4.refs_1_ = bf16[8,32,512]{2,1,0:T(8,128)(2,1)} collective-permute-done((bf16[8,32,512]{2,1,0:T(8,128)(2,1)S(1)}, bf16[8,32,512]{2,1,0:T(8,128)(2,1)}, u32[]{:S(2)}, u32[]{:S(2)}) %collective-permute-start.4) | collective-permute-done | bytes 262176 | tf_op jit(solution)/shard_map/mix_x/ppermute | solution.py:43
  42.7 0.7 collective-permute-start.8
  43.4 7.3 %attention.1 = (bf16[16,512]{1,0:T(8,128)(2,1)S(1)}, bf16[16,128]{1,0:T(8,128)(2,1)}, bf16[16,128]{1,0:T(8,128)(2,1)}) custom-call(s32[16]{0:T(128)} %lengths.1, f32[4]{0:T(128)} %bias.1, bf16[8,16,896]{2,1,0:T(8,128)(2,1)S(1)} %all-to-all-done.1.part, bf16[16,1,1024,128]{3,2,1,0:T(8,128)(2,1)} %k_hbm.1, bf16[16,1,1024,128]{3,2,1,0:T(8,128)(2,1)} %v_hbm.1), custom_call_target="tpu_custom_call" | custom-call | tf_op jit(solution)/shard_map/attention/pallas_call | solution.py:257
  50.8 2.2 %mix.1 = bf16[4,16,2048]{2,1,0:T(8,128)(2,1)S(1)} custom-call(s32[4]{0:T(128)S(1)} %pad_add_fusion.at, bf16[16,512]{1,0:T(8,128)(2,1)S(1)} %get-tuple-element.26.att, bf16[8,32,512]{2,1,0:T(8,128)(2,1)S(1)} %get-tuple-element.27.refs_0_, bf16[8,32,512]{2,1,0:T(8,128)(2,1)} %collective-permute-done.4.refs_1_, ...), custom_call_target="tpu_custom_call" | custom-call | tf_op jit(solution)/shard_map/mix/pallas_call | solution.py:54
  53.0 9.5 %all_to_all.30.got = bf16[4,16,2048]{2,1,0:T(8,128)(2,1)S(1)} all-to-all(bf16[4,16,2048]{2,1,0:T(8,128)(2,1)S(1)} %mix.1), channel_id=1, replica_groups=mesh['z'=8,'x'=4,'c'=2,'tp'=4] {'tp'}, dimensions={0} | all-to-all | bytes 524288 | tf_op jit(solution)/shard_map/all_to_all | solution.py:35
  62.5 2.1 %norm.1 = (bf16[32,8,2048]{2,1,0:T(8,128)(2,1)}, f32[16,512]{1,0:T(8,128)S(1)}) custom-call(s32[4]{0:T(128)S(1)} %pad_add_fusion.at, bf16[4,16,2048]{2,1,0:T(8,128)(2,1)S(1)} %all_to_all.30.got, bf16[16,2048]{1,0:T(8,128)(2,1)S(1)} %copy-done.2, f32[1,2048]{1,0:T(1,128)S(1)} %bitcast.19, s32[4,16]{1,0:T(4,128)S(1)} %bitcast.18), custom_call_target="tpu_custom_call" | custom-call | tf_op jit(solution)/shard_map/norm/pallas_call | solution.py:54
  64.6 5.1 %all-to-all-start.3 = ((bf16[32,8,2048]{2,1,0:T(8,128)(2,1)}), bf16[32,8,2048]{2,1,0:T(8,128)(2,1)S(1)}, u32[]{:S(2)}, u32[]{:S(2)}) async-start(bf16[32,8,2048]{2,1,0:T(8,128)(2,1)} %get-tuple-element.28), calls=%async_computation.3 | async-start | bytes 2097152 | tf_op jit(solution)/shard_map/rows_zx/all_to_all | solution.py:35
  69.8 0.9 constant_dynamic-update-slice_fusion.1
  70.7 0.9 constant_dynamic-update-slice_fusion.w0
  71.7 1.0 collective-permute-start.14
  72.6 1.2 collective-permute-start.13
  73.8 3.6 %collective-permute-start.11 = (bf16[128,512]{1,0:T(8,128)(2,1)S(1)}, bf16[128,512]{1,0:T(8,128)(2,1)S(1)}, u32[]{:S(2)}, u32[]{:S(2)}) collective-permute-start(bf16[128,512]{1,0:T(8,128)(2,1)S(1)} %copy-done.3), channel_id=1, source_target_pairs={{0,4},{4,0},{1,5},{5,1},{2,6},{6,2},{3,7},{7,3},{8,12},{12,8},{9,1... | collective-permute-start | bytes 393224 | tf_op jit(solution)/shard_map/dense_tp/ppermute | solution.py:39
  77.5 1.0 collective-permute-done.11.dd_other
  78.4 0.7 copy-done.4
  79.1 0.3 collective-permute-done.13.w2
  79.5 0.4 copy-done.9
  79.8 0.7 copy-done.10
  80.5 6.1 %collective-permute-done.12.w1 = bf16[512,256]{1,0:T(8,128)(2,1)} collective-permute-done((bf16[512,256]{1,0:T(8,128)(2,1)S(1)}, bf16[512,256]{1,0:T(8,128)(2,1)}, u32[]{:S(2)}, u32[]{:S(2)}) %collective-permute-start.12) | collective-permute-done | bytes 262176 | tf_op jit(solution)/shard_map/dense_tp/ppermute | solution.py:558
  86.6 8.2 %all-to-all-done.3.mine = bf16[32,8,2048]{2,1,0:T(8,128)(2,1)S(1)} async-done(((bf16[32,8,2048]{2,1,0:T(8,128)(2,1)}), bf16[32,8,2048]{2,1,0:T(8,128)(2,1)S(1)}, u32[]{:S(2)}, u32[]{:S(2)}) %all-to-all-start.3) | async-done | bytes 1048608 | tf_op jit(solution)/shard_map/rows_zx/all_to_all | solution.py:35
  94.8 4.1 %collective-permute-start.15 = (bf16[32,8,2048]{2,1,0:T(8,128)(2,1)S(1)}, bf16[32,8,2048]{2,1,0:T(8,128)(2,1)S(1)}, u32[]{:S(2)}, u32[]{:S(2)}) collective-permute-start(bf16[32,8,2048]{2,1,0:T(8,128)(2,1)S(1)} %all-to-all-done.3.mine), channel_id=1, source_target_pairs={{0,4},{4,0},{1,5},{5,1},{2,6},{6,2},{3,7},{7,3},{8,12},{12,8},{9,1... | collective-permute-start | bytes 3145736 | tf_op jit(solution)/shard_map/ppermute | solution.py:39
  98.9 1.5 %slots.1 = (bf16[512,128]{1,0:T(8,128)(2,1)S(1)}, bf16[512,128]{1,0:T(8,128)(2,1)S(1)}) custom-call(s32[4]{0:T(128)S(1)} %pad_add_fusion.at, bf16[8,16,896]{2,1,0:T(8,128)(2,1)S(1)} %all-to-all-done.1.part), custom_call_target="tpu_custom_call" | custom-call | tf_op jit(solution)/shard_map/slots/pallas_call | solution.py:54
  100.4 0.8 collective-permute-done.15.other
  101.2 3.4 %expert.1 = bf16[8,64,768]{2,1,0:T(8,128)(2,1)S(1)} custom-call(s32[4]{0:T(128)S(1)} %pad_add_fusion.at, bf16[32,8,2048]{2,1,0:T(8,128)(2,1)S(1)} %all-to-all-done.3.mine, bf16[32,8,2048]{2,1,0:T(8,128)(2,1)S(1)} %collective-permute-done.15.other, bf16[512,256]{1,0:T(8,128)(2,1)} %copy-done.8, bf16[512,256]{1,0:T(8,128)(2,1)} %collective-permute-done.12.w1, ...), custom_call_target="tpu_custom_call" | custom-call | tf_op jit(solution)/shard_map/expert/pallas_call | solution.py:566
  104.5 14.9 %all_to_all.31.got = bf16[8,64,768]{2,1,0:T(8,128)(2,1)S(1)} all-to-all(bf16[8,64,768]{2,1,0:T(8,128)(2,1)S(1)} %expert.1), channel_id=1, replica_groups=mesh['z'=8,'x'=4,'c'=2,'tp'=4] {'c','tp'}, dimensions={0} | all-to-all | bytes 1572864 | tf_op jit(solution)/shard_map/all_to_all | solution.py:35
  119.5 1.0 block.1
  120.5 21.6 %all_to_all.32.got = bf16[32,16,512]{2,1,0:T(8,128)(2,1)S(1)} all-to-all(bf16[32,16,512]{2,1,0:T(8,128)(2,1)S(1)} %block.1), channel_id=1, replica_groups=mesh['z'=8,'x'=4,'c'=2,'tp'=4] {'z','x'}, dimensions={0} | all-to-all | bytes 1048576 | tf_op jit(solution)/shard_map/all_to_all | solution.py:35
  142.1 0.7 final.1
  (31 shorter events, 0.1 us)
Async XLA Ops:
  2.4 21.1 %all-to-all-start = ((bf16[8,32,640]{2,1,0:T(8,128)(2,1)}), bf16[8,32,640]{2,1,0:T(8,128)(2,1)S(1)}, u32[]{:S(2)}, u32[]{:S(2)}) async-start(bf16[8,32,640]{2,1,0:T(8,128)(2,1)} %get-tuple-element.23), calls=%async_computation | async-start | bytes 655360 | tf_op jit(solution)/shard_map/over_z/all_to_all | solution.py:35
  11.4 3.7 %collective-permute-start.2 = (bf16[32,896]{1,0:T(8,128)(2,1)S(1)}, bf16[32,896]{1,0:T(8,128)(2,1)S(1)}, u32[]{:S(2)}, u32[]{:S(2)}) collective-permute-start(bf16[32,896]{1,0:T(8,128)(2,1)S(1)} %get-tuple-element.24.w0), channel_id=1, source_target_pairs={{0,24},{8,0},{16,8},{24,16},{1,25},{9,1},{17,9},{25,17},{2,26},{10... | collective-permute-start | bytes 172040 | tf_op jit(solution)/shard_map/weights_x/ppermute | solution.py:43
  13.9 4.6 %collective-permute-start.1 = (bf16[32,896]{1,0:T(8,128)(2,1)S(1)}, bf16[32,896]{1,0:T(8,128)(2,1)S(1)}, u32[]{:S(2)}, u32[]{:S(2)}) collective-permute-start(bf16[32,896]{1,0:T(8,128)(2,1)S(1)} %get-tuple-element.24.w0), channel_id=1, source_target_pairs={{0,16},{8,24},{16,0},{24,8},{1,17},{9,25},{17,1},{25,9},{2,18},{10... | collective-permute-start | bytes 172040 | tf_op jit(solution)/shard_map/weights_x/ppermute | solution.py:43
  14.4 4.9 %collective-permute-start = (bf16[32,896]{1,0:T(8,128)(2,1)S(1)}, bf16[32,896]{1,0:T(8,128)(2,1)S(1)}, u32[]{:S(2)}, u32[]{:S(2)}) collective-permute-start(bf16[32,896]{1,0:T(8,128)(2,1)S(1)} %get-tuple-element.24.w0), channel_id=1, source_target_pairs={{0,8},{8,16},{16,24},{24,0},{1,9},{9,17},{17,25},{25,1},{2,10},{10... | collective-permute-start | bytes 172040 | tf_op jit(solution)/shard_map/weights_x/ppermute | solution.py:43
  19.3 3.3 %collective-permute-start.3 = (bf16[4,32,896]{2,1,0:T(8,128)(2,1)S(1)}, bf16[4,32,896]{2,1,0:T(8,128)(2,1)S(1)}, u32[]{:S(2)}, u32[]{:S(2)}) collective-permute-start(bf16[4,32,896]{2,1,0:T(8,128)(2,1)S(1)} %pad_maximum_fusion), channel_id=1, source_target_pairs={{0,4},{4,0},{1,5},{5,1},{2,6},{6,2},{3,7},{7,3},{8,12},{12,8},{9,1... | collective-permute-start | bytes 688136 | tf_op jit(solution)/shard_map/ppermute | solution.py:39
  25.0 10.1 %collective-permute-start.6 = (bf16[8,32,512]{2,1,0:T(8,128)(2,1)S(1)}, bf16[8,32,512]{2,1,0:T(8,128)(2,1)S(1)}, u32[]{:S(2)}, u32[]{:S(2)}) collective-permute-start(bf16[8,32,512]{2,1,0:T(8,128)(2,1)S(1)} %get-tuple-element.27.refs_0_), channel_id=1, source_target_pairs={{0,24},{8,0},{16,8},{24,16},{1,25},{9,1},{17,9},{25,17},{2,26},{10... | collective-permute-start | bytes 786440 | tf_op jit(solution)/shard_map/mix_x/ppermute | solution.py:43
  27.5 12.2 %collective-permute-start.5 = (bf16[8,32,512]{2,1,0:T(8,128)(2,1)S(1)}, bf16[8,32,512]{2,1,0:T(8,128)(2,1)S(1)}, u32[]{:S(2)}, u32[]{:S(2)}) collective-permute-start(bf16[8,32,512]{2,1,0:T(8,128)(2,1)S(1)} %get-tuple-element.27.refs_0_), channel_id=1, source_target_pairs={{0,16},{8,24},{16,0},{24,8},{1,17},{9,25},{17,1},{25,9},{2,18},{10... | collective-permute-start | bytes 786440 | tf_op jit(solution)/shard_map/mix_x/ppermute | solution.py:43
  28.0 14.7 %collective-permute-start.4 = (bf16[8,32,512]{2,1,0:T(8,128)(2,1)S(1)}, bf16[8,32,512]{2,1,0:T(8,128)(2,1)}, u32[]{:S(2)}, u32[]{:S(2)}) collective-permute-start(bf16[8,32,512]{2,1,0:T(8,128)(2,1)S(1)} %get-tuple-element.27.refs_0_), channel_id=1, source_target_pairs={{0,8},{8,16},{16,24},{24,0},{1,9},{9,17},{17,25},{25,1},{2,10},{10... | collective-permute-start | bytes 786440 | tf_op jit(solution)/shard_map/mix_x/ppermute | solution.py:43
  28.6 14.8 %all-to-all-start.1 = ((bf16[8,16,896]{2,1,0:T(8,128)(2,1)}), bf16[8,16,896]{2,1,0:T(8,128)(2,1)S(1)}, u32[]{:S(2)}, u32[]{:S(2)}) async-start(bf16[8,16,896]{2,1,0:T(8,128)(2,1)} %get-tuple-element.25), calls=%async_computation.1 | async-start | bytes 458752 | tf_op jit(solution)/shard_map/partial_z/all_to_all | solution.py:35
  33.1 29.5 %copy-start.2 = (bf16[16,2048]{1,0:T(8,128)(2,1)S(1)}, bf16[16,2048]{1,0:T(8,128)(2,1)}, u32[]{:S(2)}) copy-start(bf16[16,2048]{1,0:T(8,128)(2,1)} %tok.3) | copy-start | bytes 196612
  33.1 29.5 %copy-start.6 = (s32[16,4]{0,1:T(4,128)S(1)}, s32[16,4]{0,1:T(4,128)}, u32[]{:S(2)}) copy-start(s32[16,4]{0,1:T(4,128)} %param.35) | copy-start | bytes 772
  33.1 29.5 %copy-start.7 = (f32[2048]{0:T(1024)S(1)}, f32[2048]{0:T(1024)}, u32[]{:S(2)}) copy-start(f32[2048]{0:T(1024)} %param.30) | copy-start | bytes 24580
  33.1 17.7 %collective-permute-start.7 = (bf16[8,32,512]{2,1,0:T(8,128)(2,1)S(1)}, bf16[8,32,512]{2,1,0:T(8,128)(2,1)}, u32[]{:S(2)}, u32[]{:S(2)}) collective-permute-start(bf16[8,32,512]{2,1,0:T(8,128)(2,1)S(1)} %get-tuple-element.27.refs_0_), channel_id=1, source_target_pairs={{0,4},{4,0},{1,5},{5,1},{2,6},{6,2},{3,7},{7,3},{8,12},{12,8},{9,1... | collective-permute-start | bytes 786440 | tf_op jit(solution)/shard_map/ppermute | solution.py:39
  35.1 15.7 %collective-permute-start.10 = (bf16[8,32,512]{2,1,0:T(8,128)(2,1)S(1)}, bf16[8,32,512]{2,1,0:T(8,128)(2,1)}, u32[]{:S(2)}, u32[]{:S(2)}) collective-permute-start(bf16[8,32,512]{2,1,0:T(8,128)(2,1)S(1)} %collective-permute-done.6.refs_3_), channel_id=1, source_target_pairs={{0,4},{4,0},{1,5},{5,1},{2,6},{6,2},{3,7},{7,3},{8,12},{12,8},{9,1... | collective-permute-start | bytes 786440 | tf_op jit(solution)/shard_map/ppermute | solution.py:39
  39.6 11.2 %collective-permute-start.9 = (bf16[8,32,512]{2,1,0:T(8,128)(2,1)S(1)}, bf16[8,32,512]{2,1,0:T(8,128)(2,1)}, u32[]{:S(2)}, u32[]{:S(2)}) collective-permute-start(bf16[8,32,512]{2,1,0:T(8,128)(2,1)S(1)} %collective-permute-done.5.refs_2_), channel_id=1, source_target_pairs={{0,4},{4,0},{1,5},{5,1},{2,6},{6,2},{3,7},{7,3},{8,12},{12,8},{9,1... | collective-permute-start | bytes 786440 | tf_op jit(solution)/shard_map/ppermute | solution.py:39
  42.7 8.1 %collective-permute-start.8 = (bf16[8,32,512]{2,1,0:T(8,128)(2,1)}, bf16[8,32,512]{2,1,0:T(8,128)(2,1)}, u32[]{:S(2)}, u32[]{:S(2)}) collective-permute-start(bf16[8,32,512]{2,1,0:T(8,128)(2,1)} %collective-permute-done.4.refs_1_), channel_id=1, source_target_pairs={{0,4},{4,0},{1,5},{5,1},{2,6},{6,2},{3,7},{7,3},{8,12},{12,8},{9,1... | collective-permute-start | bytes 786440 | tf_op jit(solution)/shard_map/ppermute | solution.py:39
  50.7 23.1 %copy-start.3 = (bf16[128,512]{1,0:T(8,128)(2,1)S(1)}, bf16[128,512]{1,0:T(8,128)(2,1)}, u32[]{:S(2)}) copy-start(bf16[128,512]{1,0:T(8,128)(2,1)} %dd.1) | copy-start | bytes 393220
  50.7 48.2 %copy-start.11 = (bf16[2048]{0:T(1024)(128)(2,1)S(1)}, bf16[2048]{0:T(1024)(128)(2,1)}, u32[]{:S(2)}) copy-start(bf16[2048]{0:T(1024)(128)(2,1)} %param.31) | copy-start | bytes 12292
  50.7 50.4 %copy-start = (bf16[1,2048,256]{2,1,0:T(8,128)(2,1)S(1)}, bf16[1,2048,256]{2,1,0:T(8,128)(2,1)}, u32[]{:S(2)}) copy-start(bf16[1,2048,256]{2,1,0:T(8,128)(2,1)} %eg.1) | copy-start | bytes 3145732
  50.7 50.4 %copy-start.1 = (bf16[1,2048,256]{2,1,0:T(8,128)(2,1)S(1)}, bf16[1,2048,256]{2,1,0:T(8,128)(2,1)}, u32[]{:S(2)}) copy-start(bf16[1,2048,256]{2,1,0:T(8,128)(2,1)} %eu.1) | copy-start | bytes 3145732
  64.6 30.1 %all-to-all-start.3 = ((bf16[32,8,2048]{2,1,0:T(8,128)(2,1)}), bf16[32,8,2048]{2,1,0:T(8,128)(2,1)S(1)}, u32[]{:S(2)}, u32[]{:S(2)}) async-start(bf16[32,8,2048]{2,1,0:T(8,128)(2,1)} %get-tuple-element.28), calls=%async_computation.3 | async-start | bytes 2097152 | tf_op jit(solution)/shard_map/rows_zx/all_to_all | solution.py:35
  71.7 7.8 %copy-start.8 = (bf16[512,256]{1,0:T(8,128)(2,1)}, bf16[512,256]{1,0:T(8,128)(2,1)S(1)}, u32[]{:S(2)}) copy-start(bf16[512,256]{1,0:T(8,128)(2,1)S(1)} %constant_dynamic-update-slice_fusion.w0) | copy-start | bytes 786436
  71.7 7.4 %collective-permute-start.14 = (bf16[512,256]{1,0:T(8,128)(2,1)S(1)}, bf16[512,256]{1,0:T(8,128)(2,1)S(1)}, u32[]{:S(2)}, u32[]{:S(2)}) collective-permute-start(bf16[512,256]{1,0:T(8,128)(2,1)S(1)} %constant_dynamic-update-slice_fusion.w0), channel_id=1, source_target_pairs={{0,3},{1,0},{2,1},{3,2},{4,7},{5,4},{6,5},{7,6},{8,11},{9,8},{10,9... | collective-permute-start | bytes 786440 | tf_op jit(solution)/shard_map/dense_tp/ppermute | solution.py:558
  72.6 6.8 %collective-permute-start.13 = (bf16[512,256]{1,0:T(8,128)(2,1)S(1)}, bf16[512,256]{1,0:T(8,128)(2,1)S(1)}, u32[]{:S(2)}, u32[]{:S(2)}) collective-permute-start(bf16[512,256]{1,0:T(8,128)(2,1)S(1)} %constant_dynamic-update-slice_fusion.w0), channel_id=1, source_target_pairs={{0,2},{1,3},{2,0},{3,1},{4,6},{5,7},{6,4},{7,5},{8,10},{9,11},{10,... | collective-permute-start | bytes 786440 | tf_op jit(solution)/shard_map/dense_tp/ppermute | solution.py:558
  73.8 12.8 %collective-permute-start.12 = (bf16[512,256]{1,0:T(8,128)(2,1)S(1)}, bf16[512,256]{1,0:T(8,128)(2,1)}, u32[]{:S(2)}, u32[]{:S(2)}) collective-permute-start(bf16[512,256]{1,0:T(8,128)(2,1)S(1)} %constant_dynamic-update-slice_fusion.w0), channel_id=1, source_target_pairs={{0,1},{1,2},{2,3},{3,0},{4,5},{5,6},{6,7},{7,4},{8,9},{9,10},{10,1... | collective-permute-start | bytes 786440 | tf_op jit(solution)/shard_map/dense_tp/ppermute | solution.py:558
  73.8 4.6 %collective-permute-start.11 = (bf16[128,512]{1,0:T(8,128)(2,1)S(1)}, bf16[128,512]{1,0:T(8,128)(2,1)S(1)}, u32[]{:S(2)}, u32[]{:S(2)}) collective-permute-start(bf16[128,512]{1,0:T(8,128)(2,1)S(1)} %copy-done.3), channel_id=1, source_target_pairs={{0,4},{4,0},{1,5},{5,1},{2,6},{6,2},{3,7},{7,3},{8,12},{12,8},{9,1... | collective-permute-start | bytes 393224 | tf_op jit(solution)/shard_map/dense_tp/ppermute | solution.py:39
  78.4 0.7 copy-start.4
  79.1 0.7 copy-start.9
  79.8 0.7 copy-start.10
  94.8 6.4 %collective-permute-start.15 = (bf16[32,8,2048]{2,1,0:T(8,128)(2,1)S(1)}, bf16[32,8,2048]{2,1,0:T(8,128)(2,1)S(1)}, u32[]{:S(2)}, u32[]{:S(2)}) collective-permute-start(bf16[32,8,2048]{2,1,0:T(8,128)(2,1)S(1)} %all-to-all-done.3.mine), channel_id=1, source_target_pairs={{0,4},{4,0},{1,5},{5,1},{2,6},{6,2},{3,7},{7,3},{8,12},{12,8},{9,1... | collective-permute-start | bytes 3145736 | tf_op jit(solution)/shard_map/ppermute | solution.py:39
  101.2 18.3 %copy-start.5 = (bf16[128,512]{1,0:T(8,128)(2,1)S(1)}, bf16[128,512]{1,0:T(8,128)(2,1)}, u32[]{:S(2)}) copy-start(bf16[128,512]{1,0:T(8,128)(2,1)} %copy-done.4) | copy-start | bytes 393220

commit v5 on v4

--- a/solution.py
+++ b/solution.py
@@ -179,7 +179,7 @@
     def wait(copy, n):
         copy.wait()
 
-    @pl.loop(0, seqs // 2)
+    @pl.loop(0, seqs // 2, unroll=4)
     def _(i):
         s = i * 2
         each_size(0, s, wait)
@@ -226,7 +226,7 @@
             power = jnp.exp(jnp.minimum(z, 0.0) - tail + between)
             w_s[here, cols] = jnp.where(inside, power, 0.0)
 
-    @pl.loop(0, seqs // 2)
+    @pl.loop(0, seqs // 2, unroll=4)
     def _(i):
         s = i * 2
         each_size(1, s, wait)
@@ -255,7 +255,7 @@
         pltpu.with_memory_space_constraint(a, p) for a, p in zip((part, keys, values), pins)
     ]
     return pl.pallas_call(
-        functools.partial(attention_kernel, 8),
+        functools.partial(attention_kernel, 16),
         out_shape=outs,
         in_specs=[SM, SM, VM, hbm, hbm],
         out_specs=[VM] * 3,

time: 143 us -> 143 us (level)
  no operation moved by 1% of the time
where the time goes in v5:
time: 143 us; the launch traced here: 142 us
  starting transfers between devices  46.1 us (32%)
  blocking collectives  46 us (32%)
  waiting for transfers between devices  24.6 us (17%)
  Pallas kernels  21 us (15%)
  local copies, waits for them, and re-layouts  3.7 us (3%)
    all_to_all x3, blocking collectives, exchange(): return lax.all_to_all(blocks, axes, 0, 0, tiled=True)  46 us
    all_to_all x3, starting transfers between devices, exchange(): return lax.all_to_all(blocks, axes, 0, 0, tiled=True)  18.6 us
    ppermute x7, starting transfers between devices, other_core(): return lax.ppermute(values, 'c', [(0, 1), (1, 0)])  18.1 us
    pallas_call x7, Pallas kernels, local(): pl.pallas_call(kernel, out_shape=outs, in_specs=[SM] * smem + [VM] * (len...  10.8 us
    all_to_all x3, waiting for transfers between devices, exchange(): return lax.all_to_all(blocks, axes, 0, 0, tiled=True)  9.08 us
    ppermute x6, starting transfers between devices, along_x(): return lax.ppermute(values, 'x', [(i, (i + k) % NX) for i in range(NX)])  7.21 us
    pallas_call x1, Pallas kernels, attention(): pl.pallas_call(functools.partial(attention_kernel, 16), out_shape=outs, i...  6.91 us
    ppermute x6, waiting for transfers between devices, along_x(): return lax.ppermute(values, 'x', [(i, (i + k) % NX) for i in range(NX)])  6.46 us
  transfers between devices with their start and end apart: 19, of which 11 were waited for; matrix products, arithmetic and copies ran while one was open for 1% of the time, Pallas kernels for 6%

profile of v5, /device:TPU:1, one launch (start us, length us, event | category | flops | bytes accessed | tf_op | source)
XLA Modules:
  0.0 142.4 jit_solution(6800014771811259971)
XLA Ops:
  0.6 1.8 %prepare.1 = (bf16[32,896]{1,0:T(8,128)(2,1)S(1)}, bf16[8,32,640]{2,1,0:T(8,128)(2,1)}) custom-call(bf16[16,2048]{1,0:T(8,128)(2,1)} %tok.3, f32[1,2048]{1,0:T(1,128)} %bitcast.21, bf16[32,512]{1,0:T(8,128)(2,1)} %qw.1, bf16[32,128]{1,0:T(8,128)(2,1)} %kw.1, bf16[32,128]{1,0:T(8,128)(2,1)} %vw.1, bf16[32,512]{1,0:T(8,128)(2,1)} %bitcast.20, ...), custom_call_target="tpu_custom_call" | custom-call | tf_op jit(solution)/shard_map/prepare/pallas_call | solution.py:54
  2.4 9.0 %all-to-all-start = ((bf16[8,32,640]{2,1,0:T(8,128)(2,1)}), bf16[8,32,640]{2,1,0:T(8,128)(2,1)S(1)}, u32[]{:S(2)}, u32[]{:S(2)}) async-start(bf16[8,32,640]{2,1,0:T(8,128)(2,1)} %get-tuple-element.23), calls=%async_computation | async-start | bytes 655360 | tf_op jit(solution)/shard_map/over_z/all_to_all | solution.py:35
  11.4 2.5 %collective-permute-start.2 = (bf16[32,896]{1,0:T(8,128)(2,1)S(1)}, bf16[32,896]{1,0:T(8,128)(2,1)S(1)}, u32[]{:S(2)}, u32[]{:S(2)}) collective-permute-start(bf16[32,896]{1,0:T(8,128)(2,1)S(1)} %get-tuple-element.24.w0), channel_id=1, source_target_pairs={{0,24},{8,0},{16,8},{24,16},{1,25},{9,1},{17,9},{25,17},{2,26},{10... | collective-permute-start | bytes 172040 | tf_op jit(solution)/shard_map/weights_x/ppermute | solution.py:43
  13.9 0.5 collective-permute-start.1
  14.4 0.6 collective-permute-start
  15.0 0.1 collective-permute-done.2.w3
  15.1 3.3 %collective-permute-done.1.w2 = bf16[32,896]{1,0:T(8,128)(2,1)S(1)} collective-permute-done((bf16[32,896]{1,0:T(8,128)(2,1)S(1)}, bf16[32,896]{1,0:T(8,128)(2,1)S(1)}, u32[]{:S(2)}, u32[]{:S(2)}) %collective-permute-start.1) | collective-permute-done | bytes 57376 | tf_op jit(solution)/shard_map/weights_x/ppermute | solution.py:43
  18.4 0.9 collective-permute-done.w1
  19.3 2.2 %collective-permute-start.3 = (bf16[4,32,896]{2,1,0:T(8,128)(2,1)S(1)}, bf16[4,32,896]{2,1,0:T(8,128)(2,1)S(1)}, u32[]{:S(2)}, u32[]{:S(2)}) collective-permute-start(bf16[4,32,896]{2,1,0:T(8,128)(2,1)S(1)} %pad_maximum_fusion), channel_id=1, source_target_pairs={{0,4},{4,0},{1,5},{5,1},{2,6},{6,2},{3,7},{7,3},{8,12},{12,8},{9,1... | collective-permute-start | bytes 688136 | tf_op jit(solution)/shard_map/ppermute | solution.py:39
  21.5 0.1 pad_add_fusion.at
  21.6 1.0 collective-permute-done.3.wo
  22.6 0.8 all-to-all-done.got
  23.5 1.5 %project.1 = (bf16[8,16,896]{2,1,0:T(8,128)(2,1)}, bf16[8,32,512]{2,1,0:T(8,128)(2,1)S(1)}) custom-call(s32[4]{0:T(128)S(1)} %pad_add_fusion.at, bf16[8,32,640]{2,1,0:T(8,128)(2,1)S(1)} %all-to-all-done.got, bf16[32,896]{1,0:T(8,128)(2,1)S(1)} %get-tuple-element.24.w0, bf16[32,896]{1,0:T(8,128)(2,1)S(1)} %collective-permute-done.w1, ...), custom_call_target="tpu_custom_call" | custom-call | tf_op jit(solution)/shard_map/project/pallas_call | solution.py:54
  25.0 2.5 %collective-permute-start.6 = (bf16[8,32,512]{2,1,0:T(8,128)(2,1)S(1)}, bf16[8,32,512]{2,1,0:T(8,128)(2,1)S(1)}, u32[]{:S(2)}, u32[]{:S(2)}) collective-permute-start(bf16[8,32,512]{2,1,0:T(8,128)(2,1)S(1)} %get-tuple-element.27.refs_0_), channel_id=1, source_target_pairs={{0,24},{8,0},{16,8},{24,16},{1,25},{9,1},{17,9},{25,17},{2,26},{10... | collective-permute-start | bytes 786440 | tf_op jit(solution)/shard_map/mix_x/ppermute | solution.py:43
  27.5 0.5 collective-permute-start.5
  28.0 0.6 collective-permute-start.4
  28.6 4.5 %all-to-all-start.1 = ((bf16[8,16,896]{2,1,0:T(8,128)(2,1)}), bf16[8,16,896]{2,1,0:T(8,128)(2,1)S(1)}, u32[]{:S(2)}, u32[]{:S(2)}) async-start(bf16[8,16,896]{2,1,0:T(8,128)(2,1)} %get-tuple-element.25), calls=%async_computation.1 | async-start | bytes 458752 | tf_op jit(solution)/shard_map/partial_z/all_to_all | solution.py:35
  33.1 0.0 copy-start.6
  33.1 2.0 %collective-permute-start.7 = (bf16[8,32,512]{2,1,0:T(8,128)(2,1)S(1)}, bf16[8,32,512]{2,1,0:T(8,128)(2,1)}, u32[]{:S(2)}, u32[]{:S(2)}) collective-permute-start(bf16[8,32,512]{2,1,0:T(8,128)(2,1)S(1)} %get-tuple-element.27.refs_0_), channel_id=1, source_target_pairs={{0,4},{4,0},{1,5},{5,1},{2,6},{6,2},{3,7},{7,3},{8,12},{12,8},{9,1... | collective-permute-start | bytes 786440 | tf_op jit(solution)/shard_map/ppermute | solution.py:39
  35.1 4.5 %collective-permute-start.10 = (bf16[8,32,512]{2,1,0:T(8,128)(2,1)S(1)}, bf16[8,32,512]{2,1,0:T(8,128)(2,1)}, u32[]{:S(2)}, u32[]{:S(2)}) collective-permute-start(bf16[8,32,512]{2,1,0:T(8,128)(2,1)S(1)} %collective-permute-done.6.refs_3_), channel_id=1, source_target_pairs={{0,4},{4,0},{1,5},{5,1},{2,6},{6,2},{3,7},{7,3},{8,12},{12,8},{9,1... | collective-permute-start | bytes 786440 | tf_op jit(solution)/shard_map/ppermute | solution.py:39
  39.6 0.9 collective-permute-start.9
  40.5 2.1 %collective-permute-done.4.refs_1_ = bf16[8,32,512]{2,1,0:T(8,128)(2,1)} collective-permute-done((bf16[8,32,512]{2,1,0:T(8,128)(2,1)S(1)}, bf16[8,32,512]{2,1,0:T(8,128)(2,1)}, u32[]{:S(2)}, u32[]{:S(2)}) %collective-permute-start.4) | collective-permute-done | bytes 262176 | tf_op jit(solution)/shard_map/mix_x/ppermute | solution.py:43
  42.7 0.7 collective-permute-start.8
  43.4 6.9 %attention.1 = (bf16[16,512]{1,0:T(8,128)(2,1)S(1)}, bf16[16,128]{1,0:T(8,128)(2,1)}, bf16[16,128]{1,0:T(8,128)(2,1)}) custom-call(s32[16]{0:T(128)} %lengths.1, f32[4]{0:T(128)} %bias.1, bf16[8,16,896]{2,1,0:T(8,128)(2,1)S(1)} %all-to-all-done.1.part, bf16[16,1,1024,128]{3,2,1,0:T(8,128)(2,1)} %k_hbm.1, bf16[16,1,1024,128]{3,2,1,0:T(8,128)(2,1)} %v_hbm.1), custom_call_target="tpu_custom_call" | custom-call | tf_op jit(solution)/shard_map/attention/pallas_call | solution.py:257
  50.4 2.2 %mix.1 = bf16[4,16,2048]{2,1,0:T(8,128)(2,1)S(1)} custom-call(s32[4]{0:T(128)S(1)} %pad_add_fusion.at, bf16[16,512]{1,0:T(8,128)(2,1)S(1)} %get-tuple-element.26.att, bf16[8,32,512]{2,1,0:T(8,128)(2,1)S(1)} %get-tuple-element.27.refs_0_, bf16[8,32,512]{2,1,0:T(8,128)(2,1)} %collective-permute-done.4.refs_1_, ...), custom_call_target="tpu_custom_call" | custom-call | tf_op jit(solution)/shard_map/mix/pallas_call | solution.py:54
  52.6 9.5 %all_to_all.30.got = bf16[4,16,2048]{2,1,0:T(8,128)(2,1)S(1)} all-to-all(bf16[4,16,2048]{2,1,0:T(8,128)(2,1)S(1)} %mix.1), channel_id=1, replica_groups=mesh['z'=8,'x'=4,'c'=2,'tp'=4] {'tp'}, dimensions={0} | all-to-all | bytes 524288 | tf_op jit(solution)/shard_map/all_to_all | solution.py:35
  62.2 2.1 %norm.1 = (bf16[32,8,2048]{2,1,0:T(8,128)(2,1)}, f32[16,512]{1,0:T(8,128)S(1)}) custom-call(s32[4]{0:T(128)S(1)} %pad_add_fusion.at, bf16[4,16,2048]{2,1,0:T(8,128)(2,1)S(1)} %all_to_all.30.got, bf16[16,2048]{1,0:T(8,128)(2,1)S(1)} %copy-done.2, f32[1,2048]{1,0:T(1,128)S(1)} %bitcast.19, s32[4,16]{1,0:T(4,128)S(1)} %bitcast.18), custom_call_target="tpu_custom_call" | custom-call | tf_op jit(solution)/shard_map/norm/pallas_call | solution.py:54
  64.2 5.1 %all-to-all-start.3 = ((bf16[32,8,2048]{2,1,0:T(8,128)(2,1)}), bf16[32,8,2048]{2,1,0:T(8,128)(2,1)S(1)}, u32[]{:S(2)}, u32[]{:S(2)}) async-start(bf16[32,8,2048]{2,1,0:T(8,128)(2,1)} %get-tuple-element.28), calls=%async_computation.3 | async-start | bytes 2097152 | tf_op jit(solution)/shard_map/rows_zx/all_to_all | solution.py:35
  69.4 0.9 constant_dynamic-update-slice_fusion.1
  70.3 0.9 constant_dynamic-update-slice_fusion.w0
  71.2 1.0 collective-permute-start.14
  72.2 1.2 collective-permute-start.13
  73.4 3.7 %collective-permute-start.11 = (bf16[128,512]{1,0:T(8,128)(2,1)S(1)}, bf16[128,512]{1,0:T(8,128)(2,1)S(1)}, u32[]{:S(2)}, u32[]{:S(2)}) collective-permute-start(bf16[128,512]{1,0:T(8,128)(2,1)S(1)} %copy-done.3), channel_id=1, source_target_pairs={{0,4},{4,0},{1,5},{5,1},{2,6},{6,2},{3,7},{7,3},{8,12},{12,8},{9,1... | collective-permute-start | bytes 393224 | tf_op jit(solution)/shard_map/dense_tp/ppermute | solution.py:39
  77.1 1.0 collective-permute-done.11.dd_other
  78.1 0.7 copy-done.4
  78.7 0.3 collective-permute-done.13.w2
  79.0 0.4 copy-done.9
  79.5 0.7 copy-done.10
  80.1 6.0 %collective-permute-done.12.w1 = bf16[512,256]{1,0:T(8,128)(2,1)} collective-permute-done((bf16[512,256]{1,0:T(8,128)(2,1)S(1)}, bf16[512,256]{1,0:T(8,128)(2,1)}, u32[]{:S(2)}, u32[]{:S(2)}) %collective-permute-start.12) | collective-permute-done | bytes 262176 | tf_op jit(solution)/shard_map/dense_tp/ppermute | solution.py:558
  86.1 8.2 %all-to-all-done.3.mine = bf16[32,8,2048]{2,1,0:T(8,128)(2,1)S(1)} async-done(((bf16[32,8,2048]{2,1,0:T(8,128)(2,1)}), bf16[32,8,2048]{2,1,0:T(8,128)(2,1)S(1)}, u32[]{:S(2)}, u32[]{:S(2)}) %all-to-all-start.3) | async-done | bytes 1048608 | tf_op jit(solution)/shard_map/rows_zx/all_to_all | solution.py:35
  94.3 4.1 %collective-permute-start.15 = (bf16[32,8,2048]{2,1,0:T(8,128)(2,1)S(1)}, bf16[32,8,2048]{2,1,0:T(8,128)(2,1)S(1)}, u32[]{:S(2)}, u32[]{:S(2)}) collective-permute-start(bf16[32,8,2048]{2,1,0:T(8,128)(2,1)S(1)} %all-to-all-done.3.mine), channel_id=1, source_target_pairs={{0,4},{4,0},{1,5},{5,1},{2,6},{6,2},{3,7},{7,3},{8,12},{12,8},{9,1... | collective-permute-start | bytes 3145736 | tf_op jit(solution)/shard_map/ppermute | solution.py:39
  98.5 1.5 %slots.1 = (bf16[512,128]{1,0:T(8,128)(2,1)S(1)}, bf16[512,128]{1,0:T(8,128)(2,1)S(1)}) custom-call(s32[4]{0:T(128)S(1)} %pad_add_fusion.at, bf16[8,16,896]{2,1,0:T(8,128)(2,1)S(1)} %all-to-all-done.1.part), custom_call_target="tpu_custom_call" | custom-call | tf_op jit(solution)/shard_map/slots/pallas_call | solution.py:54
  100.0 0.8 collective-permute-done.15.other
  100.8 3.4 %expert.1 = bf16[8,64,768]{2,1,0:T(8,128)(2,1)S(1)} custom-call(s32[4]{0:T(128)S(1)} %pad_add_fusion.at, bf16[32,8,2048]{2,1,0:T(8,128)(2,1)S(1)} %all-to-all-done.3.mine, bf16[32,8,2048]{2,1,0:T(8,128)(2,1)S(1)} %collective-permute-done.15.other, bf16[512,256]{1,0:T(8,128)(2,1)} %copy-done.8, bf16[512,256]{1,0:T(8,128)(2,1)} %collective-permute-done.12.w1, ...), custom_call_target="tpu_custom_call" | custom-call | tf_op jit(solution)/shard_map/expert/pallas_call | solution.py:566
  104.1 14.9 %all_to_all.31.got = bf16[8,64,768]{2,1,0:T(8,128)(2,1)S(1)} all-to-all(bf16[8,64,768]{2,1,0:T(8,128)(2,1)S(1)} %expert.1), channel_id=1, replica_groups=mesh['z'=8,'x'=4,'c'=2,'tp'=4] {'c','tp'}, dimensions={0} | all-to-all | bytes 1572864 | tf_op jit(solution)/shard_map/all_to_all | solution.py:35
  119.1 1.0 block.1
  120.1 21.6 %all_to_all.32.got = bf16[32,16,512]{2,1,0:T(8,128)(2,1)S(1)} all-to-all(bf16[32,16,512]{2,1,0:T(8,128)(2,1)S(1)} %block.1), channel_id=1, replica_groups=mesh['z'=8,'x'=4,'c'=2,'tp'=4] {'z','x'}, dimensions={0} | all-to-all | bytes 1048576 | tf_op jit(solution)/shard_map/all_to_all | solution.py:35
  141.7 0.7 final.1
  (31 shorter events, 0.1 us)
Async XLA Ops:
  2.4 21.1 %all-to-all-start = ((bf16[8,32,640]{2,1,0:T(8,128)(2,1)}), bf16[8,32,640]{2,1,0:T(8,128)(2,1)S(1)}, u32[]{:S(2)}, u32[]{:S(2)}) async-start(bf16[8,32,640]{2,1,0:T(8,128)(2,1)} %get-tuple-element.23), calls=%async_computation | async-start | bytes 655360 | tf_op jit(solution)/shard_map/over_z/all_to_all | solution.py:35
  11.4 3.7 %collective-permute-start.2 = (bf16[32,896]{1,0:T(8,128)(2,1)S(1)}, bf16[32,896]{1,0:T(8,128)(2,1)S(1)}, u32[]{:S(2)}, u32[]{:S(2)}) collective-permute-start(bf16[32,896]{1,0:T(8,128)(2,1)S(1)} %get-tuple-element.24.w0), channel_id=1, source_target_pairs={{0,24},{8,0},{16,8},{24,16},{1,25},{9,1},{17,9},{25,17},{2,26},{10... | collective-permute-start | bytes 172040 | tf_op jit(solution)/shard_map/weights_x/ppermute | solution.py:43
  13.9 4.6 %collective-permute-start.1 = (bf16[32,896]{1,0:T(8,128)(2,1)S(1)}, bf16[32,896]{1,0:T(8,128)(2,1)S(1)}, u32[]{:S(2)}, u32[]{:S(2)}) collective-permute-start(bf16[32,896]{1,0:T(8,128)(2,1)S(1)} %get-tuple-element.24.w0), channel_id=1, source_target_pairs={{0,16},{8,24},{16,0},{24,8},{1,17},{9,25},{17,1},{25,9},{2,18},{10... | collective-permute-start | bytes 172040 | tf_op jit(solution)/shard_map/weights_x/ppermute | solution.py:43
  14.4 4.9 %collective-permute-start = (bf16[32,896]{1,0:T(8,128)(2,1)S(1)}, bf16[32,896]{1,0:T(8,128)(2,1)S(1)}, u32[]{:S(2)}, u32[]{:S(2)}) collective-permute-start(bf16[32,896]{1,0:T(8,128)(2,1)S(1)} %get-tuple-element.24.w0), channel_id=1, source_target_pairs={{0,8},{8,16},{16,24},{24,0},{1,9},{9,17},{17,25},{25,1},{2,10},{10... | collective-permute-start | bytes 172040 | tf_op jit(solution)/shard_map/weights_x/ppermute | solution.py:43
  19.3 3.3 %collective-permute-start.3 = (bf16[4,32,896]{2,1,0:T(8,128)(2,1)S(1)}, bf16[4,32,896]{2,1,0:T(8,128)(2,1)S(1)}, u32[]{:S(2)}, u32[]{:S(2)}) collective-permute-start(bf16[4,32,896]{2,1,0:T(8,128)(2,1)S(1)} %pad_maximum_fusion), channel_id=1, source_target_pairs={{0,4},{4,0},{1,5},{5,1},{2,6},{6,2},{3,7},{7,3},{8,12},{12,8},{9,1... | collective-permute-start | bytes 688136 | tf_op jit(solution)/shard_map/ppermute | solution.py:39
  25.0 10.1 %collective-permute-start.6 = (bf16[8,32,512]{2,1,0:T(8,128)(2,1)S(1)}, bf16[8,32,512]{2,1,0:T(8,128)(2,1)S(1)}, u32[]{:S(2)}, u32[]{:S(2)}) collective-permute-start(bf16[8,32,512]{2,1,0:T(8,128)(2,1)S(1)} %get-tuple-element.27.refs_0_), channel_id=1, source_target_pairs={{0,24},{8,0},{16,8},{24,16},{1,25},{9,1},{17,9},{25,17},{2,26},{10... | collective-permute-start | bytes 786440 | tf_op jit(solution)/shard_map/mix_x/ppermute | solution.py:43
  27.5 12.2 %collective-permute-start.5 = (bf16[8,32,512]{2,1,0:T(8,128)(2,1)S(1)}, bf16[8,32,512]{2,1,0:T(8,128)(2,1)S(1)}, u32[]{:S(2)}, u32[]{:S(2)}) collective-permute-start(bf16[8,32,512]{2,1,0:T(8,128)(2,1)S(1)} %get-tuple-element.27.refs_0_), channel_id=1, source_target_pairs={{0,16},{8,24},{16,0},{24,8},{1,17},{9,25},{17,1},{25,9},{2,18},{10... | collective-permute-start | bytes 786440 | tf_op jit(solution)/shard_map/mix_x/ppermute | solution.py:43
  28.0 14.7 %collective-permute-start.4 = (bf16[8,32,512]{2,1,0:T(8,128)(2,1)S(1)}, bf16[8,32,512]{2,1,0:T(8,128)(2,1)}, u32[]{:S(2)}, u32[]{:S(2)}) collective-permute-start(bf16[8,32,512]{2,1,0:T(8,128)(2,1)S(1)} %get-tuple-element.27.refs_0_), channel_id=1, source_target_pairs={{0,8},{8,16},{16,24},{24,0},{1,9},{9,17},{17,25},{25,1},{2,10},{10... | collective-permute-start | bytes 786440 | tf_op jit(solution)/shard_map/mix_x/ppermute | solution.py:43
  28.6 14.8 %all-to-all-start.1 = ((bf16[8,16,896]{2,1,0:T(8,128)(2,1)}), bf16[8,16,896]{2,1,0:T(8,128)(2,1)S(1)}, u32[]{:S(2)}, u32[]{:S(2)}) async-start(bf16[8,16,896]{2,1,0:T(8,128)(2,1)} %get-tuple-element.25), calls=%async_computation.1 | async-start | bytes 458752 | tf_op jit(solution)/shard_map/partial_z/all_to_all | solution.py:35
  33.1 29.1 %copy-start.2 = (bf16[16,2048]{1,0:T(8,128)(2,1)S(1)}, bf16[16,2048]{1,0:T(8,128)(2,1)}, u32[]{:S(2)}) copy-start(bf16[16,2048]{1,0:T(8,128)(2,1)} %tok.3) | copy-start | bytes 196612
  33.1 29.1 %copy-start.6 = (s32[16,4]{0,1:T(4,128)S(1)}, s32[16,4]{0,1:T(4,128)}, u32[]{:S(2)}) copy-start(s32[16,4]{0,1:T(4,128)} %param.35) | copy-start | bytes 772
  33.1 29.1 %copy-start.7 = (f32[2048]{0:T(1024)S(1)}, f32[2048]{0:T(1024)}, u32[]{:S(2)}) copy-start(f32[2048]{0:T(1024)} %param.30) | copy-start | bytes 24580
  33.1 17.3 %collective-permute-start.7 = (bf16[8,32,512]{2,1,0:T(8,128)(2,1)S(1)}, bf16[8,32,512]{2,1,0:T(8,128)(2,1)}, u32[]{:S(2)}, u32[]{:S(2)}) collective-permute-start(bf16[8,32,512]{2,1,0:T(8,128)(2,1)S(1)} %get-tuple-element.27.refs_0_), channel_id=1, source_target_pairs={{0,4},{4,0},{1,5},{5,1},{2,6},{6,2},{3,7},{7,3},{8,12},{12,8},{9,1... | collective-permute-start | bytes 786440 | tf_op jit(solution)/shard_map/ppermute | solution.py:39
  35.1 15.3 %collective-permute-start.10 = (bf16[8,32,512]{2,1,0:T(8,128)(2,1)S(1)}, bf16[8,32,512]{2,1,0:T(8,128)(2,1)}, u32[]{:S(2)}, u32[]{:S(2)}) collective-permute-start(bf16[8,32,512]{2,1,0:T(8,128)(2,1)S(1)} %collective-permute-done.6.refs_3_), channel_id=1, source_target_pairs={{0,4},{4,0},{1,5},{5,1},{2,6},{6,2},{3,7},{7,3},{8,12},{12,8},{9,1... | collective-permute-start | bytes 786440 | tf_op jit(solution)/shard_map/ppermute | solution.py:39
  39.6 10.8 %collective-permute-start.9 = (bf16[8,32,512]{2,1,0:T(8,128)(2,1)S(1)}, bf16[8,32,512]{2,1,0:T(8,128)(2,1)}, u32[]{:S(2)}, u32[]{:S(2)}) collective-permute-start(bf16[8,32,512]{2,1,0:T(8,128)(2,1)S(1)} %collective-permute-done.5.refs_2_), channel_id=1, source_target_pairs={{0,4},{4,0},{1,5},{5,1},{2,6},{6,2},{3,7},{7,3},{8,12},{12,8},{9,1... | collective-permute-start | bytes 786440 | tf_op jit(solution)/shard_map/ppermute | solution.py:39
  42.7 7.7 %collective-permute-start.8 = (bf16[8,32,512]{2,1,0:T(8,128)(2,1)}, bf16[8,32,512]{2,1,0:T(8,128)(2,1)}, u32[]{:S(2)}, u32[]{:S(2)}) collective-permute-start(bf16[8,32,512]{2,1,0:T(8,128)(2,1)} %collective-permute-done.4.refs_1_), channel_id=1, source_target_pairs={{0,4},{4,0},{1,5},{5,1},{2,6},{6,2},{3,7},{7,3},{8,12},{12,8},{9,1... | collective-permute-start | bytes 786440 | tf_op jit(solution)/shard_map/ppermute | solution.py:39
  50.3 23.1 %copy-start.3 = (bf16[128,512]{1,0:T(8,128)(2,1)S(1)}, bf16[128,512]{1,0:T(8,128)(2,1)}, u32[]{:S(2)}) copy-start(bf16[128,512]{1,0:T(8,128)(2,1)} %dd.1) | copy-start | bytes 393220
  50.3 48.1 %copy-start.11 = (bf16[2048]{0:T(1024)(128)(2,1)S(1)}, bf16[2048]{0:T(1024)(128)(2,1)}, u32[]{:S(2)}) copy-start(bf16[2048]{0:T(1024)(128)(2,1)} %param.31) | copy-start | bytes 12292
  50.4 50.4 %copy-start = (bf16[1,2048,256]{2,1,0:T(8,128)(2,1)S(1)}, bf16[1,2048,256]{2,1,0:T(8,128)(2,1)}, u32[]{:S(2)}) copy-start(bf16[1,2048,256]{2,1,0:T(8,128)(2,1)} %eg.1) | copy-start | bytes 3145732
  50.4 50.4 %copy-start.1 = (bf16[1,2048,256]{2,1,0:T(8,128)(2,1)S(1)}, bf16[1,2048,256]{2,1,0:T(8,128)(2,1)}, u32[]{:S(2)}) copy-start(bf16[1,2048,256]{2,1,0:T(8,128)(2,1)} %eu.1) | copy-start | bytes 3145732
  64.2 30.1 %all-to-all-start.3 = ((bf16[32,8,2048]{2,1,0:T(8,128)(2,1)}), bf16[32,8,2048]{2,1,0:T(8,128)(2,1)S(1)}, u32[]{:S(2)}, u32[]{:S(2)}) async-start(bf16[32,8,2048]{2,1,0:T(8,128)(2,1)} %get-tuple-element.28), calls=%async_computation.3 | async-start | bytes 2097152 | tf_op jit(solution)/shard_map/rows_zx/all_to_all | solution.py:35
  71.2 7.8 %copy-start.8 = (bf16[512,256]{1,0:T(8,128)(2,1)}, bf16[512,256]{1,0:T(8,128)(2,1)S(1)}, u32[]{:S(2)}) copy-start(bf16[512,256]{1,0:T(8,128)(2,1)S(1)} %constant_dynamic-update-slice_fusion.w0) | copy-start | bytes 786436
  71.2 7.5 %collective-permute-start.14 = (bf16[512,256]{1,0:T(8,128)(2,1)S(1)}, bf16[512,256]{1,0:T(8,128)(2,1)S(1)}, u32[]{:S(2)}, u32[]{:S(2)}) collective-permute-start(bf16[512,256]{1,0:T(8,128)(2,1)S(1)} %constant_dynamic-update-slice_fusion.w0), channel_id=1, source_target_pairs={{0,3},{1,0},{2,1},{3,2},{4,7},{5,4},{6,5},{7,6},{8,11},{9,8},{10,9... | collective-permute-start | bytes 786440 | tf_op jit(solution)/shard_map/dense_tp/ppermute | solution.py:558
  72.2 6.8 %collective-permute-start.13 = (bf16[512,256]{1,0:T(8,128)(2,1)S(1)}, bf16[512,256]{1,0:T(8,128)(2,1)S(1)}, u32[]{:S(2)}, u32[]{:S(2)}) collective-permute-start(bf16[512,256]{1,0:T(8,128)(2,1)S(1)} %constant_dynamic-update-slice_fusion.w0), channel_id=1, source_target_pairs={{0,2},{1,3},{2,0},{3,1},{4,6},{5,7},{6,4},{7,5},{8,10},{9,11},{10,... | collective-permute-start | bytes 786440 | tf_op jit(solution)/shard_map/dense_tp/ppermute | solution.py:558
  73.4 12.7 %collective-permute-start.12 = (bf16[512,256]{1,0:T(8,128)(2,1)S(1)}, bf16[512,256]{1,0:T(8,128)(2,1)}, u32[]{:S(2)}, u32[]{:S(2)}) collective-permute-start(bf16[512,256]{1,0:T(8,128)(2,1)S(1)} %constant_dynamic-update-slice_fusion.w0), channel_id=1, source_target_pairs={{0,1},{1,2},{2,3},{3,0},{4,5},{5,6},{6,7},{7,4},{8,9},{9,10},{10,1... | collective-permute-start | bytes 786440 | tf_op jit(solution)/shard_map/dense_tp/ppermute | solution.py:558
  73.4 4.7 %collective-permute-start.11 = (bf16[128,512]{1,0:T(8,128)(2,1)S(1)}, bf16[128,512]{1,0:T(8,128)(2,1)S(1)}, u32[]{:S(2)}, u32[]{:S(2)}) collective-permute-start(bf16[128,512]{1,0:T(8,128)(2,1)S(1)} %copy-done.3), channel_id=1, source_target_pairs={{0,4},{4,0},{1,5},{5,1},{2,6},{6,2},{3,7},{7,3},{8,12},{12,8},{9,1... | collective-permute-start | bytes 393224 | tf_op jit(solution)/shard_map/dense_tp/ppermute | solution.py:39
  78.1 0.7 copy-start.4
  78.7 0.7 copy-start.9
  79.5 0.7 copy-start.10
  94.3 6.4 %collective-permute-start.15 = (bf16[32,8,2048]{2,1,0:T(8,128)(2,1)S(1)}, bf16[32,8,2048]{2,1,0:T(8,128)(2,1)S(1)}, u32[]{:S(2)}, u32[]{:S(2)}) collective-permute-start(bf16[32,8,2048]{2,1,0:T(8,128)(2,1)S(1)} %all-to-all-done.3.mine), channel_id=1, source_target_pairs={{0,4},{4,0},{1,5},{5,1},{2,6},{6,2},{3,7},{7,3},{8,12},{12,8},{9,1... | collective-permute-start | bytes 3145736 | tf_op jit(solution)/shard_map/ppermute | solution.py:39
  100.8 18.3 %copy-start.5 = (bf16[128,512]{1,0:T(8,128)(2,1)S(1)}, bf16[128,512]{1,0:T(8,128)(2,1)}, u32[]{:S(2)}) copy-start(bf16[128,512]{1,0:T(8,128)(2,1)} %copy-done.4) | copy-start | bytes 393220
